TPU v7x, 512 devices: a whole 4x4x16 slice. The times are simulated.
512 devices in a mesh: ep: 32 (over z, core), tp: 16 (over y, x).
Axes of the slice: x: 4, y: 4, z: 16, core: 2. Of those that a mesh axis runs over, the one named last changes fastest.
Arguments:
- query_rows: bfloat16 [16384, 2048], P('ep', 'tp'), may hold values from -6 to 6
- key_rows: bfloat16 [16384, 2048], P('ep', 'tp'), may hold values from -6 to 6
- value_rows: bfloat16 [16384, 4096], P('ep', 'tp'), may hold values from -6 to 6
- in_gate: float32 [16, 16384], P('tp', 'ep'), may hold values from -120 to 120
- forget_gate: float32 [16, 16384], P('tp', 'ep'), may hold values from -2 to 20
- out_gate: bfloat16 [16384, 4096], P('ep', 'tp'), may hold values from -6 to 6
- head_gain: float32 [4096], P('tp'), may hold values from 0.1 to 1.9
- mix_weight: bfloat16 [4096, 4096], P(None, 'tp'), may hold values from -0.09375 to 0.09375
- expert_input: bfloat16 [8192, 4096], P('ep', 'tp'), may hold values from -30 to 30
- routes: int32 [8192, 2], P('ep'), may hold values from 0 to 31, all different within a row; in each aligned block of 256 rows (0 to 255, 256 to 511, ...) at most 32 rows name the same one
- route_weight: float32 [8192, 2], P('ep'), may hold values from 0.25 to 1.25
- gate_weight: bfloat16 [32, 1024, 4096], P('ep', 'tp'), may hold values from -0.09375 to 0.09375
- up_weight: bfloat16 [32, 1024, 4096], P('ep', 'tp'), may hold values from -0.09375 to 0.09375
- down_weight: bfloat16 [32, 1024, 4096], P('ep', None, 'tp'), may hold values from -0.1875 to 0.1875
Outputs:
- mixer_out: bfloat16 [16384, 4096], P('ep', 'tp')
- expert_out: bfloat16 [8192, 4096], P('ep', 'tp')
Inputs may be any that keep to these rules, and one draw needn't show every extreme that they name: `routes`: each row names 2 different experts. In the rows of one device no expert is named by more than 32 rows, and in the rows of some device an expert is named by exactly 32 rows.
All inputs are finite; a program needn't handle non-finite values.
Results may differ from a plain program's by a relative error of at most 0.0057.
Values may be sent and summed in bfloat16 or wider, within the bound.
No kernel may reach another device: no remote copies, remote signals or barrier semaphores. Data moves between devices by JAX's collectives and lax.ppermute only.
A program may use at most 128 MiB of HBM per device.

v0:
```python
import jax
import jax.numpy as jnp
from jax import lax
from jax.experimental import pallas as pl
from jax.experimental.pallas import tpu as pltpu
from jax.sharding import Mesh
from jax.sharding import PartitionSpec as P


EP = ("z", "c")
TP = ("y", "x")
EPSILON = 1e-06
LOG_FLOOR = -1e30
MASKED = -1e38
HIGHEST = lax.Precision.HIGHEST
F32 = jnp.float32
BF16 = jnp.bfloat16


def dot(a, b):
    return jnp.dot(a, b, preferred_element_type=F32)


def dot_t(a, b):
    return lax.dot_general(a, b, (((1,), (1,)), ((), ())), preferred_element_type=F32)


def iota(shape, dim):
    return lax.broadcasted_iota(jnp.int32, shape, dim)


def call(kernel, out, args, scratch=(), grid=None, in_specs=None, out_specs=None):
    vmem = pl.BlockSpec(memory_space=pltpu.VMEM)
    smem = pl.BlockSpec(memory_space=pltpu.SMEM)
    if in_specs is None:
        in_specs = [smem if a.dtype == jnp.int32 and a.ndim == 1 else vmem for a in args]
    kw = {} if grid is None else {"grid": grid}
    if out_specs is None:
        out_specs = jax.tree.map(lambda _: vmem, out)
    return pl.pallas_call(
        kernel,
        out_shape=out,
        in_specs=in_specs,
        out_specs=out_specs,
        scratch_shapes=list(scratch),
        **kw,
    )(*args)


def log_sigmoid(f):
    return jnp.minimum(f, 0.0) - jnp.log1p(jnp.exp(-jnp.abs(f)))


def cumulative_forms(forget_row):
    n = forget_row.shape[1]
    logs = jnp.broadcast_to(log_sigmoid(forget_row), (n, n))
    at_row, at_col = iota((n, n), 0), iota((n, n), 1)
    column = jnp.sum(jnp.where(at_col <= at_row, logs, 0.0), axis=1, keepdims=True)
    own = jnp.sum(jnp.where(at_col == at_row, logs, 0.0), axis=1, keepdims=True)
    row = jnp.sum(jnp.where(at_row <= at_col, own, 0.0), axis=0, keepdims=True)
    return column, row


def summary_kernel(k_ref, v_ref, in_ref, forget_ref, out_ref):
    n = k_ref.shape[0]
    dk = k_ref.shape[1]
    column, _ = cumulative_forms(forget_ref[...])
    diagonal = iota((n, n), 0) == iota((n, n), 1)
    log_in = jnp.sum(
        jnp.where(diagonal, jnp.broadcast_to(in_ref[...], (n, n)), 0.0), axis=1, keepdims=True
    )
    total = column[n - 1 :, :]
    weight_log = total - column + log_in
    top = jnp.max(weight_log, axis=0, keepdims=True)
    weighted = k_ref[...].astype(F32) * jnp.exp(weight_log - top)
    memory = lax.dot_general(
        weighted.astype(BF16), v_ref[...], (((0,), (0,)), ((), ())), preferred_element_type=F32
    )
    normal = jnp.sum(weighted, axis=0, keepdims=True)
    width = out_ref.shape[1]
    out_ref[0:dk, :] = memory
    out_ref[dk : dk + 1, 0:dk] = normal
    out_ref[dk : dk + 1, dk:] = normal
    out_ref[dk + 1 : dk + 2, :] = jnp.broadcast_to(total, (1, width))
    out_ref[dk + 2 : dk + 3, :] = jnp.broadcast_to(top, (1, width))
    out_ref[dk + 3 :, :] = jnp.zeros((out_ref.shape[0] - dk - 3, width), F32)


def parts_of(x, dk):
    return x[0:dk, :], x[dk : dk + 1, :], x[dk + 1 : dk + 2, :], x[dk + 2 : dk + 3, :]


def fold(first, second):
    memory_1, normal_1, decay_1, max_1 = first
    memory_2, normal_2, decay_2, max_2 = second
    top = jnp.maximum(decay_2 + max_1, max_2)
    keep_1 = jnp.exp(decay_2 + max_1 - top)
    keep_2 = jnp.exp(max_2 - top)
    return (
        keep_1 * memory_1 + keep_2 * memory_2,
        keep_1 * normal_1 + keep_2 * normal_2,
        decay_1 + decay_2,
        top,
    )


def split3(x):
    high = x.astype(BF16)
    rest = x - high.astype(F32)
    middle = rest.astype(BF16)
    low = (rest - middle.astype(F32)).astype(BF16)
    return high, middle, low


def pack(out_ref, memory, normal, decay, top):
    dk, width = memory.shape
    out_ref[0:dk, :] = memory.astype(BF16)
    rows = []
    for value in (normal, decay, top):
        rows += [part.astype(F32) for part in split3(value)]
    rows.append(jnp.zeros((out_ref.shape[0] - dk - len(rows), width), F32))
    out_ref[dk:, :] = jnp.concatenate(rows, axis=0).astype(BF16)


def unpack(item, dk):
    item = item.astype(F32)
    rows = [
        item[dk + i : dk + i + 1] + item[dk + i + 1 : dk + i + 2] + item[dk + i + 2 : dk + i + 3]
        for i in (0, 3, 6)
    ]
    return (item[0:dk], *rows)


def first_state(dk, width):
    return (
        jnp.zeros((dk, width), F32),
        jnp.zeros((1, width), F32),
        jnp.zeros((1, width), F32),
        jnp.full((1, width), LOG_FLOOR, F32),
    )


def fold_earlier(all_ref, here, dk):
    state = before = first_state(dk, all_ref.shape[2])
    for k in range(all_ref.shape[0]):
        state = fold(state, unpack(all_ref[k], dk))
        before = tuple(jnp.where(k < here, new, old) for new, old in zip(state, before))
    return before, state


def store_state(out_ref, state):
    memory, normal, decay, top = state
    dk, width = memory.shape
    out_ref[0:dk, :] = memory
    out_ref[dk:, :] = jnp.concatenate(
        [normal, decay, top, jnp.zeros((out_ref.shape[0] - dk - 3, width), F32)], axis=0
    )


def chip_kernel(at_ref, mine_ref, other_ref, packed_ref):
    dk = 128
    south = at_ref[0] == 0
    mine, other = mine_ref[...], other_ref[...]
    first = parts_of(jnp.where(south, mine, other), dk)
    second = parts_of(jnp.where(south, other, mine), dk)
    total = fold(first, second)
    half = mine.shape[1] // 2
    pack(packed_ref, *[jnp.where(south, v[:, :half], v[:, half:]) for v in total])


def prior_kernel(at_ref, all_ref, out_ref):
    before, _ = fold_earlier(all_ref, at_ref[1], 128)
    store_state(out_ref, before)


def output_kernel(
    at_ref, q_ref, k_ref, v_ref, in_ref, forget_ref, gate_ref, gain_ref,
    prior_ref, prior_other_ref, other_ref, out_ref,
):
    n, dk = q_ref.shape
    scale = dk ** (-0.5)
    south = at_ref[0] == 0
    column, row = cumulative_forms(forget_ref[...])
    left = jnp.where(south, prior_ref[...], prior_other_ref[...])
    right = jnp.where(south, prior_other_ref[...], prior_ref[...])
    before = parts_of(jnp.concatenate([left, right], axis=1), dk)
    joined = fold(before, parts_of(other_ref[...], dk))
    memory, normal, _, top_before = [jnp.where(south, b, j) for b, j in zip(before, joined)]
    normal = normal[:, :dk]
    top_before = top_before[:, 0:1]
    log_in = in_ref[...]
    step = n // 4
    for start in range(0, n, step):
        rows, seen = slice(start, start + step), start + step
        q = q_ref[rows, :]
        at = column[rows, :]
        causal = iota((step, seen), 1) <= iota((step, seen), 0) + start
        log_decay = jnp.where(causal, at - row[:, :seen] + log_in[:, :seen], MASKED)
        log_inter = at + top_before
        top = jnp.maximum(log_inter, jnp.max(log_decay, axis=1, keepdims=True))
        scores = dot_t(q, k_ref[0:seen, :]) * scale * jnp.exp(log_decay - top)
        carried = jnp.exp(log_inter - top) * scale
        wide = q.astype(F32)
        numerator = carried * jnp.dot(
            wide, memory, precision=HIGHEST, preferred_element_type=F32
        ) + dot(scores.astype(BF16), v_ref[0:seen, :])
        denominator = carried * jnp.sum(wide * normal, axis=1, keepdims=True) + jnp.sum(
            scores, axis=1, keepdims=True
        )
        values = numerator / jnp.maximum(jnp.abs(denominator), jnp.exp(-top))
        values = values * lax.rsqrt(jnp.mean(values * values, axis=1, keepdims=True) + EPSILON)
        gate = gate_ref[rows, :].astype(F32)
        values = values * gain_ref[...] * (1.0 / (1.0 + jnp.exp(-gate)))
        side, inner = divmod(start, n // 2)
        out_ref[lax.rem(at_ref[2] + side, 2), inner : inner + step, :] = values.astype(BF16)


def dispatch_kernel(routes_ref, x_ref, out_ref):
    tokens = x_ref.shape[0]
    slots = out_ref.shape[0]
    experts, room = 32, slots // 32
    expert = iota((experts, tokens), 0)
    named = jnp.zeros((experts, tokens), F32)
    for r in range(routes_ref.shape[0]):
        named = named + (routes_ref[r : r + 1, :] == expert).astype(F32)
    earlier = (iota((tokens, tokens), 0) < iota((tokens, tokens), 1)).astype(F32).astype(BF16)
    place = dot(named.astype(BF16), earlier)
    key = jnp.where(named > 0.5, place, -1.0).astype(BF16)
    slot = iota((slots, experts), 0)
    spread = (slot // room == iota((slots, experts), 1)).astype(F32).astype(BF16)
    wanted = (iota((slots, tokens), 0) % room).astype(F32)
    chosen = (dot(spread, key) == wanted).astype(F32).astype(BF16)
    out_ref[...] = dot(chosen, x_ref[...]).astype(BF16)


def pair_kernel(gate_ref, up_ref, out_ref):
    width = gate_ref.shape[0]
    out_ref[0:width, :] = gate_ref[...]
    out_ref[width:, :] = up_ref[...]


def collect_kernel(routes_ref, weight_ref, back_ref, out_ref):
    tokens = out_ref.shape[0]
    slots = back_ref.shape[0]
    experts, room = 32, slots // 32
    expert = iota((tokens, experts), 1)
    named = jnp.zeros((tokens, experts), F32)
    weight = jnp.zeros((tokens, experts), F32)
    for r in range(routes_ref.shape[1]):
        hit = routes_ref[:, r : r + 1] == expert
        named = named + hit.astype(F32)
        weight = weight + jnp.where(hit, weight_ref[:, r : r + 1], 0.0)
    earlier = (iota((tokens, tokens), 1) < iota((tokens, tokens), 0)).astype(F32).astype(BF16)
    place = dot(earlier, named.astype(BF16))
    key = jnp.where(named > 0.5, place, -1.0).astype(BF16)
    slot = iota((experts, slots), 1)
    spread = (slot // room == iota((experts, slots), 0)).astype(F32).astype(BF16)
    wanted = (iota((tokens, slots), 1) % room).astype(F32)
    chosen = dot(key, spread) == wanted
    total = jnp.zeros(out_ref.shape, F32)
    for part in split3(weight):
        share = jnp.where(chosen, dot(part, spread), 0.0).astype(BF16)
        total = total + dot(share, back_ref[...])
    out_ref[...] = total.astype(BF16)


def hidden_kernel(
    x_ref, gate_ref, up_ref, w1_ref, w2_ref, w3_ref, out_ref, gate_acc, up_acc, squares
):
    step = pl.program_id(0)
    width = gate_ref.shape[0]
    far = (w1_ref, w2_ref, w3_ref)
    senders, _, columns = x_ref.shape
    x = jnp.concatenate([x_ref[i] for i in range(senders)], axis=1)
    gate = jnp.concatenate([gate_ref[...]] + [w[0:width] for w in far], axis=0)
    up = jnp.concatenate([up_ref[...]] + [w[width:] for w in far], axis=0)
    gate_part, up_part = dot_t(x, gate), dot_t(x, up)
    square = jnp.zeros(squares.shape, F32)
    for i in range(senders):
        wide = x_ref[i].astype(F32)
        square = square + wide * wide

    @pl.when(step == 0)
    def _():
        gate_acc[...] = gate_part
        up_acc[...] = up_part
        squares[...] = square

    @pl.when(step > 0)
    def _():
        gate_acc[...] += gate_part
        up_acc[...] += up_part
        squares[...] += square

    @pl.when(step == pl.num_programs(0) - 1)
    def _():
        total = jnp.sum(squares[...], axis=1, keepdims=True)
        inverse = lax.rsqrt(total * (1.0 / (columns * out_ref.shape[0])) + EPSILON)
        gate = gate_acc[...] * inverse
        hidden = gate * (1.0 / (1.0 + jnp.exp(-gate))) * (up_acc[...] * inverse)
        hidden = hidden.astype(BF16)
        for copy in range(out_ref.shape[0]):
            out_ref[copy] = hidden


def down_kernel(h_ref, w_ref, out_ref):
    part = h_ref.shape[2] // 4
    rows = h_ref.shape[1]
    for ys in range(4):
        total = jnp.zeros((rows, w_ref.shape[1]), F32)
        for xs in range(4):
            at = [(((ys + j) % 4) * 4 + xs) * part for j in range(4)]
            weight = jnp.concatenate([w_ref[a : a + part, :] for a in at], axis=0)
            total = total + dot(h_ref[ys * 4 + xs], weight)
        out_ref[ys * rows : (ys + 1) * rows, :] = total.astype(BF16)


def mix_kernel(
    at_ref, h0_ref, h1_ref, h2_ref, h3_ref, near_ref, a_ref, b_ref, o0_ref, o1_ref, acc, heads
):
    step = pl.program_id(0)
    half = heads.shape[0] // 2
    c, x, y = at_ref[0], at_ref[2], at_ref[3]

    @pl.when(step == 0)
    def _():
        acc[...] = jnp.zeros_like(acc)
        for ky, ref in enumerate((h0_ref, h1_ref, h2_ref, h3_ref)):
            for kx in range(4):
                heads[lax.rem(y + ky, 4) * 4 + lax.rem(x + 4 - kx, 4)] = ref[kx]

    pieces = near_ref.shape[1]
    width = near_ref.shape[2]
    own = jnp.zeros(acc.shape[1:], F32)
    pair = jnp.zeros(acc.shape[1:], F32)
    for i in range(pieces):
        k = step * pieces + i
        rows = slice(i * width, (i + 1) * width)
        own = own + dot(heads[k], near_ref[0, i]) + dot(heads[half + k], near_ref[1, i])
        pair = pair + dot(heads[c * half + k], a_ref[rows, :])
        pair = pair + dot(heads[(1 - c) * half + k], b_ref[rows, :])
    acc[0] += own
    acc[1] += pair

    @pl.when(step == pl.num_programs(0) - 1)
    def _():
        o0_ref[...] = acc[0].astype(BF16)
        o1_ref[...] = acc[1].astype(BF16)


def assemble_kernel(at_ref, own_ref, pair_ref, out_ref):
    block = own_ref.shape[0]
    side = lax.rem(at_ref[2], 2)
    out_ref[pl.ds(pl.multiple_of(side * block, block), block), :] = own_ref[...]
    out_ref[pl.ds(pl.multiple_of((1 - side) * block, block), block), :] = pair_ref[...]


def from_next(x, axis, k):
    n = lax.axis_size(axis)
    return lax.ppermute(x, axis, [((i + k) % n, i) for i in range(n)])


def swapped(x, axis):
    n = lax.axis_size(axis)
    return lax.ppermute(x, axis, [(i ^ 1, i) for i in range(n)])


def exchange(x, axis):
    return lax.all_to_all(x, axis, split_axis=0, concat_axis=0, tiled=True)


def body(
    query_rows,
    key_rows,
    value_rows,
    in_gate,
    forget_gate,
    out_gate,
    head_gain,
    mix_weight,
    expert_input,
    routes,
    route_weight,
    gate_weight,
    up_weight,
    down_weight,
):
    sds = jax.ShapeDtypeStruct
    rows_a, dk = query_rows.shape
    dv = value_rows.shape[1]
    tokens, columns = expert_input.shape
    ep, tp = lax.axis_size(EP), lax.axis_size(TP)
    gate_local, up_local, down_local = gate_weight[0], up_weight[0], down_weight[0]
    width = gate_local.shape[0]
    slots = ep * 32
    at = jnp.stack(
        [lax.axis_index(axis) for axis in ("c", "z", "x", "y")]
    ).astype(jnp.int32)

    table = call(dispatch_kernel, sds((slots, columns), BF16), (routes.T, expert_input))
    arrived = exchange(table.reshape(ep, 32, columns), EP)
    arrived = arrived.reshape(4, 1, slots // 4, columns)

    pair = call(pair_kernel, sds((2 * width, gate_local.shape[1]), BF16), (gate_local, up_local))
    own_half = lax.dynamic_slice_in_dim(
        mix_weight, at[0] * (mix_weight.shape[0] // 2), mix_weight.shape[0] // 2, 0
    )
    far = []
    for k in (1, 2, 3):
        far.append(from_next(pair, "y", k))
    mix_far = swapped(own_half, "x")
    mix_swap = swapped(mix_far, "c")

    mine = call(
        summary_kernel, sds((dk + 8, dv), F32), (key_rows, value_rows, in_gate, forget_gate)
    )
    other = swapped(mine, "c")
    packed = call(chip_kernel, sds((dk + 16, dv // 2), BF16), (at, mine, other))
    chips = lax.all_gather(packed, "z", axis=0)
    prior = call(prior_kernel, sds((dk + 8, dv // 2), F32), (at, chips))
    prior_other = swapped(prior, "c")
    block = rows_a // 2
    heads = call(
        output_kernel,
        sds((2, block, dv), BF16),
        (
            at, query_rows, key_rows, value_rows, in_gate, forget_gate, out_gate,
            head_gain[None, :], prior, prior_other, other,
        ),
    )

    sent = jnp.broadcast_to(arrived, (4, 4, slots // 4, columns)).reshape(tp, slots // 4, columns)
    rows = exchange(sent, TP)
    grid = 2
    per = tp // grid
    weights_spec = lambda r: pl.BlockSpec((r, per * columns), lambda i: (0, i))
    hidden = call(
        hidden_kernel,
        sds((tp, slots // 4, 4 * width), BF16),
        (rows, gate_local, up_local, *far),
        scratch=[pltpu.VMEM((slots // 4, 4 * width), F32)] * 2
        + [pltpu.VMEM((slots // 4, columns), F32)],
        grid=(grid,),
        in_specs=[
            pl.BlockSpec((per, slots // 4, columns), lambda i: (i, 0, 0)),
            weights_spec(width),
            weights_spec(width),
        ]
        + [weights_spec(2 * width)] * 3,
        out_specs=pl.BlockSpec((tp, slots // 4, 4 * width), lambda i: (0, 0, 0)),
    )
    gathered = exchange(hidden, TP)
    results = call(down_kernel, sds((slots, columns), BF16), (gathered, down_local))
    back = exchange(results.reshape(ep, 32, columns), EP).reshape(slots, columns)

    along_x = [heads[0]]
    for k in (1, 2, 3):
        along_x.append(from_next(heads[k % 2], "x", -k))
    along_x = jnp.stack(along_x)
    head_rows = [along_x]
    for k in (1, 2, 3):
        head_rows.append(from_next(along_x, "y", k))
    half = tp // 2
    steps = 2
    pieces = half // steps
    weight_block = pl.BlockSpec((pieces * dv, columns), lambda i: (i, 0))
    projected = call(
        mix_kernel,
        [sds((block, columns), BF16)] * 2,
        (at, *head_rows, mix_weight.reshape(2, half, dv, columns), mix_far, mix_swap),
        scratch=[pltpu.VMEM((2, block, columns), F32), pltpu.VMEM((tp, block, dv), BF16)],
        grid=(steps,),
        in_specs=[pl.BlockSpec(memory_space=pltpu.SMEM)]
        + [pl.BlockSpec((4, block, dv), lambda i: (0, 0, 0))] * 4
        + [pl.BlockSpec((2, pieces, dv, columns), lambda i: (0, i, 0, 0))]
        + [weight_block] * 2,
        out_specs=[pl.BlockSpec((block, columns), lambda i: (0, 0))] * 2,
    )
    from_pair = swapped(projected[1], "x")
    mixer_out = call(assemble_kernel, sds((rows_a, columns), BF16), (at, projected[0], from_pair))

    expert_out = call(collect_kernel, sds((tokens, columns), BF16), (routes, route_weight, back))
    return (mixer_out, expert_out)


def solution(mesh):
    split = Mesh(mesh.devices.reshape(16, 2, 4, 4), (*EP, *TP))
    in_specs = (
        P(EP, TP),
        P(EP, TP),
        P(EP, TP),
        P(TP, EP),
        P(TP, EP),
        P(EP, TP),
        P(TP),
        P(None, TP),
        P(EP, TP),
        P(EP, None),
        P(EP, None),
        P(EP, TP, None),
        P(EP, TP, None),
        P(EP, None, TP),
    )
    out_specs = (P(EP, TP), P(EP, TP))

    return jax.shard_map(body, mesh=split, in_specs=in_specs, out_specs=out_specs, check_vma=False)
```

profile of v0, /device:TPU:1, one launch (start us, length us, event | category | flops | bytes accessed | tf_op | source)
XLA Modules:
  0.0 316.9 jit_solution(7124202853160305544)
XLA Ops:
  3.0 50.3 %all_to_all.20 = bf16[32,32,256]{2,1,0:T(8,128)(2,1)S(1)} all-to-all(bf16[32,32,256]{2,1,0:T(8,128)(2,1)} %bitcast.27), channel_id=1, replica_groups=mesh['z'=16,'c'=2,'y'=4,'x'=4] {'z','c'}, dimensions={0} | all-to-all | bytes 1048576 | tf_op jit(solution)/shard_map/all_to_all | solution.py:369
  54.8 6.8 %all-to-all-start.1 = ((bf16[16,256,256]{2,1,0:T(8,128)(2,1)}), bf16[16,256,256]{2,1,0:T(8,128)(2,1)S(1)}, u32[]{:S(2)}, u32[]{:S(2)}) async-start(bf16[16,256,256]{2,1,0:T(8,128)(2,1)} %bitcast.15), calls=%async_computation.1 | async-start | bytes 4194304 | tf_op jit(solution)/shard_map/all_to_all | solution.py:369
  63.9 4.5 %collective-permute-start.11 = (bf16[128,4096]{1,0:T(8,128)(2,1)}, bf16[128,4096]{1,0:T(8,128)(2,1)S(1)}, u32[]{:S(2)}, u32[]{:S(2)}) collective-permute-start(bf16[128,4096]{1,0:T(8,128)(2,1)} %shard_map.156), channel_id=1, source_target_pairs={{4,0},{8,4},{12,8},{0,12},{5,1},{9,5},{13,9},{1,13},{6,2},{10,6},{... | collective-permute-start | bytes 3145736 | tf_op jit(solution)/shard_map/ppermute | solution.py:360
  70.8 2.5 collective-permute-start.13
  73.3 35.0 %collective-permute-done.11.w1_ref = bf16[128,4096]{1,0:T(8,128)(2,1)S(1)} collective-permute-done((bf16[128,4096]{1,0:T(8,128)(2,1)}, bf16[128,4096]{1,0:T(8,128)(2,1)S(1)}, u32[]{:S(2)}, u32[]{:S(2)}) %collective-permute-start.11) | collective-permute-done | bytes 1048608 | tf_op jit(solution)/shard_map/ppermute | solution.py:360
  111.7 21.7 %collective-permute-done.13.w3_ref = bf16[128,4096]{1,0:T(8,128)(2,1)} collective-permute-done((bf16[128,4096]{1,0:T(8,128)(2,1)}, bf16[128,4096]{1,0:T(8,128)(2,1)}, u32[]{:S(2)}, u32[]{:S(2)}) %collective-permute-start.13) | collective-permute-done | bytes 1048608 | tf_op jit(solution)/shard_map/ppermute | solution.py:360
  134.8 5.3 %shard_map.157 = bf16[16,256,256]{2,1,0:T(8,128)(2,1)} custom-call(bf16[16,256,256]{2,1,0:T(8,128)(2,1)} %copy-done.1, bf16[64,4096]{1,0:T(8,128)(2,1)} %bitcast.29, bf16[64,4096]{1,0:T(8,128)(2,1)} %bitcast.31, bf16[128,4096]{1,0:T(8,128)(2,1)} %copy-done.6, bf16[128,4096]{1,0:T(8,128)(2,1)} %copy-done.7, bf16[128,4096]{1,0:T(8,128)(2,1)} %collective-permute-done.13.w3_ref), custom_call_target="tpu_custom_call" | custom-call | tf_op jit(solution)/shard_map/pallas_call | solution.py:40
  140.0 4.4 %all-to-all-start.2 = ((bf16[16,256,256]{2,1,0:T(8,128)(2,1)}), bf16[16,256,256]{2,1,0:T(8,128)(2,1)S(1)}, u32[]{:S(2)}, u32[]{:S(2)}) async-start(bf16[16,256,256]{2,1,0:T(8,128)(2,1)} %shard_map.157), calls=%async_computation.2 | async-start | bytes 4194304 | tf_op jit(solution)/shard_map/all_to_all | solution.py:369
  146.8 3.2 %collective-permute-start.8 = (bf16[2048,256]{1,0:T(8,128)(2,1)}, bf16[2048,256]{1,0:T(8,128)(2,1)S(1)}, u32[]{:S(2)}, u32[]{:S(2)}) collective-permute-start(bf16[2048,256]{1,0:T(8,128)(2,1)} %constant_dynamic-slice_fusion), channel_id=1, source_target_pairs={{1,0},{0,1},{3,2},{2,3},{5,4},{4,5},{7,6},{6,7},{9,8},{8,9},{11,10... | collective-permute-start | bytes 3145736 | tf_op jit(solution)/shard_map/ppermute | solution.py:365
  150.0 22.2 %all-to-all-done.2.h_ref = bf16[16,256,256]{2,1,0:T(8,128)(2,1)S(1)} async-done(((bf16[16,256,256]{2,1,0:T(8,128)(2,1)}), bf16[16,256,256]{2,1,0:T(8,128)(2,1)S(1)}, u32[]{:S(2)}, u32[]{:S(2)}) %all-to-all-start.2) | async-done | bytes 2097184 | tf_op jit(solution)/shard_map/all_to_all | solution.py:369
  173.6 3.2 %shard_map.158 = bf16[1024,256]{1,0:T(8,128)(2,1)} custom-call(bf16[16,256,256]{2,1,0:T(8,128)(2,1)} %copy-done, bf16[1024,256]{1,0:T(8,128)(2,1)} %bitcast.33), custom_call_target="tpu_custom_call" | custom-call | tf_op jit(solution)/shard_map/pallas_call | solution.py:40
  176.8 10.0 %all-to-all-start.3 = ((bf16[32,32,256]{2,1,0:T(8,128)(2,1)}), bf16[32,32,256]{2,1,0:T(8,128)(2,1)S(1)}, u32[]{:S(2)}, u32[]{:S(2)}) async-start(bf16[32,32,256]{2,1,0:T(8,128)(2,1)} %bitcast.32), calls=%async_computation.3 | async-start | bytes 1048576 | tf_op jit(solution)/shard_map/all_to_all | solution.py:369
  194.7 40.7 %all-gather = bf16[2304,128]{1,0:T(8,128)(2,1)} all-gather(bf16[144,128]{1,0:T(8,128)(2,1)} %shard_map.150), channel_id=2, replica_groups=mesh['z'=16,'c'=2,'y'=4,'x'=4] {'z'}, dimensions={0}, use_global_device_ids=true | all-gather | bytes 626688 | tf_op jit(solution)/shard_map/all_gather | solution.py:419
  237.4 8.5 %collective-permute-start.1 = (f32[136,128]{1,0:T(8,128)}, f32[136,128]{1,0:T(8,128)S(1)}, u32[]{:S(2)}, u32[]{:S(2)}) collective-permute-start(f32[136,128]{1,0:T(8,128)} %shard_map.151.prior_ref), channel_id=1, source_target_pairs={{16,0},{0,16},{17,1},{1,17},{18,2},{2,18},{19,3},{3,19},{20,4},{4,... | collective-permute-start | bytes 208904 | tf_op jit(solution)/shard_map/ppermute | solution.py:365
  248.5 3.4 %shard_map.152 = bf16[2,256,256]{2,1,0:T(8,128)(2,1)} custom-call(s32[4]{0:T(128)} %pad_add_fusion.at_ref, bf16[512,128]{1,0:T(8,128)(2,1)} %q_ref.1, bf16[512,128]{1,0:T(8,128)(2,1)} %k_ref.3, bf16[512,256]{1,0:T(8,128)(2,1)} %v_ref.3, f32[1,512]{1,0:T(1,128)} %in_ref.3, f32[1,512]{1,0:T(1,128)} %forget_ref.3, bf16[512,256]{1,0:T(8,128)(2,1)} %gate_ref.1, ...), custom_call_target="tpu_custom_call" | custom-call | tf_op jit(solution)/shard_map/pallas_call | solution.py:40
  254.8 3.4 %collective-permute-start.2 = (bf16[256,256]{1,0:T(8,128)(2,1)S(1)}, bf16[256,256]{1,0:T(8,128)(2,1)S(1)}, u32[]{:S(2)}, u32[]{:S(2)}) collective-permute-start(bf16[256,256]{1,0:T(8,128)(2,1)S(1)} %get-tuple-element.8), channel_id=1, source_target_pairs={{3,0},{0,1},{1,2},{2,3},{7,4},{4,5},{5,6},{6,7},{11,8},{8,9},{9,10... | collective-permute-start | bytes 393224 | tf_op jit(solution)/shard_map/ppermute | solution.py:360
  262.4 3.0 collective-permute-done.3
  265.5 3.2 %collective-permute-start.5 = (bf16[4,256,256]{2,1,0:T(8,128)(2,1)S(1)}, bf16[4,256,256]{2,1,0:T(8,128)(2,1)S(1)}, u32[]{:S(2)}, u32[]{:S(2)}) collective-permute-start(bf16[4,256,256]{2,1,0:T(8,128)(2,1)S(1)} %pad_maximum_fusion.h0_ref), channel_id=1, source_target_pairs={{4,0},{8,4},{12,8},{0,12},{5,1},{9,5},{13,9},{1,13},{6,2},{10,6},{... | collective-permute-start | bytes 1572872 | tf_op jit(solution)/shard_map/ppermute | solution.py:360
  273.4 5.2 %collective-permute-done.5.h1_ref = bf16[4,256,256]{2,1,0:T(8,128)(2,1)S(1)} collective-permute-done((bf16[4,256,256]{2,1,0:T(8,128)(2,1)S(1)}, bf16[4,256,256]{2,1,0:T(8,128)(2,1)S(1)}, u32[]{:S(2)}, u32[]{:S(2)}) %collective-permute-start.5) | collective-permute-done | bytes 524320 | tf_op jit(solution)/shard_map/ppermute | solution.py:360
  278.6 4.5 %collective-permute-done.6.h2_ref = bf16[4,256,256]{2,1,0:T(8,128)(2,1)S(1)} collective-permute-done((bf16[4,256,256]{2,1,0:T(8,128)(2,1)S(1)}, bf16[4,256,256]{2,1,0:T(8,128)(2,1)S(1)}, u32[]{:S(2)}, u32[]{:S(2)}) %collective-permute-start.6) | collective-permute-done | bytes 524320 | tf_op jit(solution)/shard_map/ppermute | solution.py:360
  283.1 14.0 %collective-permute-done.7.h3_ref = bf16[4,256,256]{2,1,0:T(8,128)(2,1)S(1)} collective-permute-done((bf16[4,256,256]{2,1,0:T(8,128)(2,1)S(1)}, bf16[4,256,256]{2,1,0:T(8,128)(2,1)S(1)}, u32[]{:S(2)}, u32[]{:S(2)}) %collective-permute-start.7) | collective-permute-done | bytes 524320 | tf_op jit(solution)/shard_map/ppermute | solution.py:360
  299.0 4.5 %shard_map.153 = (bf16[256,256]{1,0:T(8,128)(2,1)}, bf16[256,256]{1,0:T(8,128)(2,1)}) custom-call(s32[4]{0:T(128)} %pad_add_fusion.at_ref, bf16[4,256,256]{2,1,0:T(8,128)(2,1)} %copy-done.2, bf16[4,256,256]{2,1,0:T(8,128)(2,1)} %copy-done.9, bf16[4,256,256]{2,1,0:T(8,128)(2,1)} %copy-done.10, bf16[4,256,256]{2,1,0:T(8,128)(2,1)} %copy-done.11, ...), custom_call_target="tpu_custom_call" | custom-call | tf_op jit(solution)/shard_map/pallas_call | solution.py:40
  307.5 2.7 collective-permute-done.10.pair_ref
  313.3 3.6 %shard_map.159 = bf16[256,256]{1,0:T(8,128)(2,1)} custom-call(s32[256,2]{1,0:T(8,128)} %copy.16.routes_ref, f32[256,2]{1,0:T(8,128)} %copy.17.weight_ref, bf16[1024,256]{1,0:T(8,128)(2,1)} %bitcast.26), custom_call_target="tpu_custom_call" | custom-call | tf_op jit(solution)/shard_map/pallas_call | solution.py:40
  (62 shorter events, 50.2 us)
Async XLA Ops:
  54.8 78.6 %all-to-all-start.1 = ((bf16[16,256,256]{2,1,0:T(8,128)(2,1)}), bf16[16,256,256]{2,1,0:T(8,128)(2,1)S(1)}, u32[]{:S(2)}, u32[]{:S(2)}) async-start(bf16[16,256,256]{2,1,0:T(8,128)(2,1)} %bitcast.15), calls=%async_computation.1 | async-start | bytes 4194304 | tf_op jit(solution)/shard_map/all_to_all | solution.py:369
  63.9 44.4 %collective-permute-start.11 = (bf16[128,4096]{1,0:T(8,128)(2,1)}, bf16[128,4096]{1,0:T(8,128)(2,1)S(1)}, u32[]{:S(2)}, u32[]{:S(2)}) collective-permute-start(bf16[128,4096]{1,0:T(8,128)(2,1)} %shard_map.156), channel_id=1, source_target_pairs={{4,0},{8,4},{12,8},{0,12},{5,1},{9,5},{13,9},{1,13},{6,2},{10,6},{... | collective-permute-start | bytes 3145736 | tf_op jit(solution)/shard_map/ppermute | solution.py:360
  68.3 42.4 %collective-permute-start.12 = (bf16[128,4096]{1,0:T(8,128)(2,1)}, bf16[128,4096]{1,0:T(8,128)(2,1)S(1)}, u32[]{:S(2)}, u32[]{:S(2)}) collective-permute-start(bf16[128,4096]{1,0:T(8,128)(2,1)} %shard_map.156), channel_id=1, source_target_pairs={{8,0},{12,4},{0,8},{4,12},{9,1},{13,5},{1,9},{5,13},{10,2},{14,6},... | collective-permute-start | bytes 3145736 | tf_op jit(solution)/shard_map/ppermute | solution.py:360
  70.8 62.6 %collective-permute-start.13 = (bf16[128,4096]{1,0:T(8,128)(2,1)}, bf16[128,4096]{1,0:T(8,128)(2,1)}, u32[]{:S(2)}, u32[]{:S(2)}) collective-permute-start(bf16[128,4096]{1,0:T(8,128)(2,1)} %shard_map.156), channel_id=1, source_target_pairs={{12,0},{0,4},{4,8},{8,12},{13,1},{1,5},{5,9},{9,13},{14,2},{2,6},{... | collective-permute-start | bytes 3145736 | tf_op jit(solution)/shard_map/ppermute | solution.py:360
  108.3 25.1 %copy-start.6 = (bf16[128,4096]{1,0:T(8,128)(2,1)}, bf16[128,4096]{1,0:T(8,128)(2,1)S(1)}, u32[]{:S(2)}) copy-start(bf16[128,4096]{1,0:T(8,128)(2,1)S(1)} %collective-permute-done.11.w1_ref) | copy-start | bytes 3145732
  140.0 32.2 %all-to-all-start.2 = ((bf16[16,256,256]{2,1,0:T(8,128)(2,1)}), bf16[16,256,256]{2,1,0:T(8,128)(2,1)S(1)}, u32[]{:S(2)}, u32[]{:S(2)}) async-start(bf16[16,256,256]{2,1,0:T(8,128)(2,1)} %shard_map.157), calls=%async_computation.2 | async-start | bytes 4194304 | tf_op jit(solution)/shard_map/all_to_all | solution.py:369
  146.8 99.1 %collective-permute-start.8 = (bf16[2048,256]{1,0:T(8,128)(2,1)}, bf16[2048,256]{1,0:T(8,128)(2,1)S(1)}, u32[]{:S(2)}, u32[]{:S(2)}) collective-permute-start(bf16[2048,256]{1,0:T(8,128)(2,1)} %constant_dynamic-slice_fusion), channel_id=1, source_target_pairs={{1,0},{0,1},{3,2},{2,3},{5,4},{4,5},{7,6},{6,7},{9,8},{8,9},{11,10... | collective-permute-start | bytes 3145736 | tf_op jit(solution)/shard_map/ppermute | solution.py:365
  176.8 135.7 %all-to-all-start.3 = ((bf16[32,32,256]{2,1,0:T(8,128)(2,1)}), bf16[32,32,256]{2,1,0:T(8,128)(2,1)S(1)}, u32[]{:S(2)}, u32[]{:S(2)}) async-start(bf16[32,32,256]{2,1,0:T(8,128)(2,1)} %bitcast.32), calls=%async_computation.3 | async-start | bytes 1048576 | tf_op jit(solution)/shard_map/all_to_all | solution.py:369
  189.0 3.5 %collective-permute-start = (f32[136,256]{1,0:T(8,128)}, f32[136,256]{1,0:T(8,128)S(1)}, u32[]{:S(2)}, u32[]{:S(2)}) collective-permute-start(f32[136,256]{1,0:T(8,128)} %shard_map.149.mine_ref), channel_id=1, source_target_pairs={{16,0},{0,16},{17,1},{1,17},{18,2},{2,18},{19,3},{3,19},{20,4},{4,... | collective-permute-start | bytes 417800 | tf_op jit(solution)/shard_map/ppermute | solution.py:365
  237.4 10.5 %collective-permute-start.1 = (f32[136,128]{1,0:T(8,128)}, f32[136,128]{1,0:T(8,128)S(1)}, u32[]{:S(2)}, u32[]{:S(2)}) collective-permute-start(f32[136,128]{1,0:T(8,128)} %shard_map.151.prior_ref), channel_id=1, source_target_pairs={{16,0},{0,16},{17,1},{1,17},{18,2},{2,18},{19,3},{3,19},{20,4},{4,... | collective-permute-start | bytes 208904 | tf_op jit(solution)/shard_map/ppermute | solution.py:365
  245.9 52.1 %copy-start.4 = (bf16[2048,256]{1,0:T(8,128)(2,1)}, bf16[2048,256]{1,0:T(8,128)(2,1)S(1)}, u32[]{:S(2)}) copy-start(bf16[2048,256]{1,0:T(8,128)(2,1)S(1)} %collective-permute-done.8.a_ref) | copy-start | bytes 3145732
  245.9 51.3 %collective-permute-start.9 = (bf16[2048,256]{1,0:T(8,128)(2,1)S(1)}, bf16[2048,256]{1,0:T(8,128)(2,1)S(1)}, u32[]{:S(2)}, u32[]{:S(2)}) collective-permute-start(bf16[2048,256]{1,0:T(8,128)(2,1)S(1)} %collective-permute-done.8.a_ref), channel_id=1, source_target_pairs={{16,0},{0,16},{17,1},{1,17},{18,2},{2,18},{19,3},{3,19},{20,4},{4,... | collective-permute-start | bytes 3145736 | tf_op jit(solution)/shard_map/ppermute | solution.py:365
  252.9 7.2 %collective-permute-start.4 = (bf16[256,256]{1,0:T(8,128)(2,1)S(1)}, bf16[256,256]{1,0:T(8,128)(2,1)S(1)}, u32[]{:S(2)}, u32[]{:S(2)}) collective-permute-start(bf16[256,256]{1,0:T(8,128)(2,1)S(1)} %get-tuple-element.8), channel_id=1, source_target_pairs={{1,0},{2,1},{3,2},{0,3},{5,4},{6,5},{7,6},{4,7},{9,8},{10,9},{11,1... | collective-permute-start | bytes 393224 | tf_op jit(solution)/shard_map/ppermute | solution.py:360
  254.8 7.6 %collective-permute-start.2 = (bf16[256,256]{1,0:T(8,128)(2,1)S(1)}, bf16[256,256]{1,0:T(8,128)(2,1)S(1)}, u32[]{:S(2)}, u32[]{:S(2)}) collective-permute-start(bf16[256,256]{1,0:T(8,128)(2,1)S(1)} %get-tuple-element.8), channel_id=1, source_target_pairs={{3,0},{0,1},{1,2},{2,3},{7,4},{4,5},{5,6},{6,7},{11,8},{8,9},{9,10... | collective-permute-start | bytes 393224 | tf_op jit(solution)/shard_map/ppermute | solution.py:360
  258.2 7.2 %collective-permute-start.3 = (bf16[256,256]{1,0:T(8,128)(2,1)S(1)}, bf16[256,256]{1,0:T(8,128)(2,1)S(1)}, u32[]{:S(2)}, u32[]{:S(2)}) collective-permute-start(bf16[256,256]{1,0:T(8,128)(2,1)S(1)} %get-tuple-element.7), channel_id=1, source_target_pairs={{2,0},{3,1},{0,2},{1,3},{6,4},{7,5},{4,6},{5,7},{10,8},{11,9},{8,1... | collective-permute-start | bytes 393224 | tf_op jit(solution)/shard_map/ppermute | solution.py:360
  265.5 32.5 %copy-start.2 = (bf16[4,256,256]{2,1,0:T(8,128)(2,1)}, bf16[4,256,256]{2,1,0:T(8,128)(2,1)S(1)}, u32[]{:S(2)}) copy-start(bf16[4,256,256]{2,1,0:T(8,128)(2,1)S(1)} %pad_maximum_fusion.h0_ref) | copy-start | bytes 1572868
  265.5 13.2 %collective-permute-start.5 = (bf16[4,256,256]{2,1,0:T(8,128)(2,1)S(1)}, bf16[4,256,256]{2,1,0:T(8,128)(2,1)S(1)}, u32[]{:S(2)}, u32[]{:S(2)}) collective-permute-start(bf16[4,256,256]{2,1,0:T(8,128)(2,1)S(1)} %pad_maximum_fusion.h0_ref), channel_id=1, source_target_pairs={{4,0},{8,4},{12,8},{0,12},{5,1},{9,5},{13,9},{1,13},{6,2},{10,6},{... | collective-permute-start | bytes 1572872 | tf_op jit(solution)/shard_map/ppermute | solution.py:360
  268.7 14.4 %collective-permute-start.6 = (bf16[4,256,256]{2,1,0:T(8,128)(2,1)S(1)}, bf16[4,256,256]{2,1,0:T(8,128)(2,1)S(1)}, u32[]{:S(2)}, u32[]{:S(2)}) collective-permute-start(bf16[4,256,256]{2,1,0:T(8,128)(2,1)S(1)} %pad_maximum_fusion.h0_ref), channel_id=1, source_target_pairs={{8,0},{12,4},{0,8},{4,12},{9,1},{13,5},{1,9},{5,13},{10,2},{14,6},... | collective-permute-start | bytes 1572872 | tf_op jit(solution)/shard_map/ppermute | solution.py:360
  271.2 26.0 %collective-permute-start.7 = (bf16[4,256,256]{2,1,0:T(8,128)(2,1)S(1)}, bf16[4,256,256]{2,1,0:T(8,128)(2,1)S(1)}, u32[]{:S(2)}, u32[]{:S(2)}) collective-permute-start(bf16[4,256,256]{2,1,0:T(8,128)(2,1)S(1)} %pad_maximum_fusion.h0_ref), channel_id=1, source_target_pairs={{12,0},{0,4},{4,8},{8,12},{13,1},{1,5},{5,9},{9,13},{14,2},{2,6},{... | collective-permute-start | bytes 1572872 | tf_op jit(solution)/shard_map/ppermute | solution.py:360
  278.6 18.6 %copy-start.9 = (bf16[4,256,256]{2,1,0:T(8,128)(2,1)}, bf16[4,256,256]{2,1,0:T(8,128)(2,1)S(1)}, u32[]{:S(2)}) copy-start(bf16[4,256,256]{2,1,0:T(8,128)(2,1)S(1)} %collective-permute-done.5.h1_ref) | copy-start | bytes 1572868
  283.1 14.1 %copy-start.10 = (bf16[4,256,256]{2,1,0:T(8,128)(2,1)}, bf16[4,256,256]{2,1,0:T(8,128)(2,1)S(1)}, u32[]{:S(2)}) copy-start(bf16[4,256,256]{2,1,0:T(8,128)(2,1)S(1)} %collective-permute-done.6.h2_ref) | copy-start | bytes 1572868
  299.0 6.9 %copy-start.14 = (s32[256,2]{0,1:T(2,128)S(1)}, s32[256,2]{0,1:T(2,128)}, u32[]{:S(2)}) copy-start(s32[256,2]{0,1:T(2,128)} %param.23) | copy-start | bytes 6148
  299.0 7.7 %copy-start.15 = (f32[256,2]{0,1:T(2,128)S(1)}, f32[256,2]{0,1:T(2,128)}, u32[]{:S(2)}) copy-start(f32[256,2]{0,1:T(2,128)} %param.24) | copy-start | bytes 6148
  303.5 6.7 %collective-permute-start.10 = (bf16[256,256]{1,0:T(8,128)(2,1)}, bf16[256,256]{1,0:T(8,128)(2,1)S(1)}, u32[]{:S(2)}, u32[]{:S(2)}) collective-permute-start(bf16[256,256]{1,0:T(8,128)(2,1)} %get-tuple-element.5), channel_id=1, source_target_pairs={{1,0},{0,1},{3,2},{2,3},{5,4},{4,5},{7,6},{6,7},{9,8},{8,9},{11,10... | collective-permute-start | bytes 393224 | tf_op jit(solution)/shard_map/ppermute | solution.py:365
  (9 other events, 8.2 us)
where the time goes:
time: 318 us; the launch traced here: 317 us
  waiting for transfers between devices  114 us (36%)
  blocking collectives  91 us (29%)
  starting transfers between devices  64 us (20%)
  Pallas kernels  32.1 us (10%)
  local copies, waits for them, and re-layouts  14.6 us (5%)
    ppermute x9, waiting for transfers between devices, from_next(): return lax.ppermute(x, axis, [((i + k) % n, i) for i in range(n)])  88.1 us
    all_to_all x1, blocking collectives, exchange(): return lax.all_to_all(x, axis, split_axis=0, concat_axis=0, tiled=True)  50.3 us
    all_gather x1, blocking collectives, body(): chips = lax.all_gather(packed, 'z', axis=0)  40.7 us
    pallas_call x11, Pallas kernels, call(): pl.pallas_call(kernel, out_shape=out, in_specs=in_specs, out_specs=out_sp...  32.1 us
    ppermute x9, starting transfers between devices, from_next(): return lax.ppermute(x, axis, [((i + k) % n, i) for i in range(n)])  24.6 us
    all_to_all x3, waiting for transfers between devices, exchange(): return lax.all_to_all(x, axis, split_axis=0, concat_axis=0, tiled=True)  22.2 us
    all_to_all x3, starting transfers between devices, exchange(): return lax.all_to_all(x, axis, split_axis=0, concat_axis=0, tiled=True)  21.2 us
    ppermute x5, starting transfers between devices, swapped(): return lax.ppermute(x, axis, [(i ^ 1, i) for i in range(n)])  18.2 us
  transfers between devices with their start and end apart: 17, of which 11 were waited for; matrix products, arithmetic and copies ran while one was open for 2% of the time, Pallas kernels for 7%

commit v1 on v0

--- a/solution.py
+++ b/solution.py
@@ -1,3 +1,5 @@
+import functools
+
 import jax
 import jax.numpy as jnp
 from jax import lax
@@ -29,7 +31,11 @@
     return lax.broadcasted_iota(jnp.int32, shape, dim)
 
 
-def call(kernel, out, args, scratch=(), grid=None, in_specs=None, out_specs=None):
+def call(kernel, out, args, scratch=(), grid=None, in_specs=None, out_specs=None, near=()):
+    args = [
+        pltpu.with_memory_space_constraint(a, pltpu.VMEM) if i in near else a
+        for i, a in enumerate(args)
+    ]
     vmem = pl.BlockSpec(memory_space=pltpu.VMEM)
     smem = pl.BlockSpec(memory_space=pltpu.SMEM)
     if in_specs is None:
@@ -43,6 +49,7 @@
         in_specs=in_specs,
         out_specs=out_specs,
         scratch_shapes=list(scratch),
+        compiler_params=pltpu.CompilerParams(vmem_limit_bytes=57 << 20),
         **kw,
     )(*args)
 
@@ -140,14 +147,6 @@
     )
 
 
-def fold_earlier(all_ref, here, dk):
-    state = before = first_state(dk, all_ref.shape[2])
-    for k in range(all_ref.shape[0]):
-        state = fold(state, unpack(all_ref[k], dk))
-        before = tuple(jnp.where(k < here, new, old) for new, old in zip(state, before))
-    return before, state
-
-
 def store_state(out_ref, state):
     memory, normal, decay, top = state
     dk, width = memory.shape
@@ -157,7 +156,7 @@
     )
 
 
-def chip_kernel(at_ref, mine_ref, other_ref, packed_ref):
+def chip_kernel(at_ref, mine_ref, other_ref, total_ref, packed_ref):
     dk = 128
     south = at_ref[0] == 0
     mine, other = mine_ref[...], other_ref[...]
@@ -165,12 +164,27 @@
     second = parts_of(jnp.where(south, other, mine), dk)
     total = fold(first, second)
     half = mine.shape[1] // 2
-    pack(packed_ref, *[jnp.where(south, v[:, :half], v[:, half:]) for v in total])
-
-
-def prior_kernel(at_ref, all_ref, out_ref):
-    before, _ = fold_earlier(all_ref, at_ref[1], 128)
-    store_state(out_ref, before)
+    total = [jnp.where(south, v[:, :half], v[:, half:]) for v in total]
+    store_state(total_ref, total)
+    pack(packed_ref, *total)
+
+
+def step_kernel(reach, first, last, at_ref, came_ref, *refs):
+    dk = 128
+    valid = at_ref[1] >= reach
+    came = unpack(came_ref[...], dk)
+    if first:
+        before = first_state(dk, came_ref.shape[1])
+    else:
+        before, refs = parts_of(refs[0][...], dk), refs[1:]
+    joined = fold(came, before)
+    if not last:
+        total = parts_of(refs[0][...], dk)
+        more = fold(came, total)
+        total = [jnp.where(valid, new, old) for new, old in zip(more, total)]
+        store_state(refs[1], total)
+        pack(refs[3], *total)
+    store_state(refs[0 if last else 2], [jnp.where(valid, n, o) for n, o in zip(joined, before)])
 
 
 def output_kernel(
@@ -239,9 +253,8 @@
     out_ref[width:, :] = up_ref[...]
 
 
-def collect_kernel(routes_ref, weight_ref, back_ref, out_ref):
-    tokens = out_ref.shape[0]
-    slots = back_ref.shape[0]
+def plan_kernel(routes_ref, weight_ref, high_ref, low_ref):
+    tokens, slots = high_ref.shape
     experts, room = 32, slots // 32
     expert = iota((tokens, experts), 1)
     named = jnp.zeros((tokens, experts), F32)
@@ -257,11 +270,14 @@
     spread = (slot // room == iota((experts, slots), 0)).astype(F32).astype(BF16)
     wanted = (iota((tokens, slots), 1) % room).astype(F32)
     chosen = dot(key, spread) == wanted
-    total = jnp.zeros(out_ref.shape, F32)
-    for part in split3(weight):
-        share = jnp.where(chosen, dot(part, spread), 0.0).astype(BF16)
-        total = total + dot(share, back_ref[...])
-    out_ref[...] = total.astype(BF16)
+    high, low, _ = split3(weight)
+    high_ref[...] = jnp.where(chosen, dot(high, spread), 0.0).astype(BF16)
+    low_ref[...] = jnp.where(chosen, dot(low, spread), 0.0).astype(BF16)
+
+
+def collect_kernel(high_ref, low_ref, back_ref, out_ref):
+    back = back_ref[...]
+    out_ref[...] = (dot(high_ref[...], back) + dot(low_ref[...], back)).astype(BF16)
 
 
 def hidden_kernel(
@@ -270,14 +286,16 @@
     step = pl.program_id(0)
     width = gate_ref.shape[0]
     far = (w1_ref, w2_ref, w3_ref)
-    senders, _, columns = x_ref.shape
-    x = jnp.concatenate([x_ref[i] for i in range(senders)], axis=1)
+    _, _, columns = x_ref.shape
+    senders = gate_ref.shape[1] // columns
+    pieces = [x_ref[step * senders + i] for i in range(senders)]
+    x = jnp.concatenate(pieces, axis=1)
     gate = jnp.concatenate([gate_ref[...]] + [w[0:width] for w in far], axis=0)
     up = jnp.concatenate([up_ref[...]] + [w[width:] for w in far], axis=0)
     gate_part, up_part = dot_t(x, gate), dot_t(x, up)
     square = jnp.zeros(squares.shape, F32)
-    for i in range(senders):
-        wide = x_ref[i].astype(F32)
+    for piece in pieces:
+        wide = piece.astype(F32)
         square = square + wide * wide
 
     @pl.when(step == 0)
@@ -397,7 +415,7 @@
         [lax.axis_index(axis) for axis in ("c", "z", "x", "y")]
     ).astype(jnp.int32)
 
-    table = call(dispatch_kernel, sds((slots, columns), BF16), (routes.T, expert_input))
+    table = call(dispatch_kernel, pltpu.VMEM((slots, columns), BF16), (routes.T, expert_input))
     arrived = exchange(table.reshape(ep, 32, columns), EP)
     arrived = arrived.reshape(4, 1, slots // 4, columns)
 
@@ -415,9 +433,23 @@
         summary_kernel, sds((dk + 8, dv), F32), (key_rows, value_rows, in_gate, forget_gate)
     )
     other = swapped(mine, "c")
-    packed = call(chip_kernel, sds((dk + 16, dv // 2), BF16), (at, mine, other))
-    chips = lax.all_gather(packed, "z", axis=0)
-    prior = call(prior_kernel, sds((dk + 8, dv // 2), F32), (at, chips))
+    state, lines = sds((dk + 8, dv // 2), F32), sds((dk + 16, dv // 2), BF16)
+    total, packed = call(chip_kernel, [state, lines], (at, mine, other), near=(2,))
+    before, reach, chips = (), 1, lax.axis_size("z")
+    while reach < chips:
+        came = lax.ppermute(packed, "z", [(i, i + reach) for i in range(chips - reach)])
+        last = 2 * reach == chips
+        result = call(
+            functools.partial(step_kernel, reach, reach == 1, last),
+            [state] if last else [state, state, lines],
+            (at, came, *before) + (() if last else (total,)),
+            near=(1,),
+        )
+        if last:
+            (prior,) = result
+        else:
+            total, before, packed = result[0], result[1:2], result[2]
+        reach *= 2
     prior_other = swapped(prior, "c")
     block = rows_a // 2
     heads = call(
@@ -427,6 +459,7 @@
             at, query_rows, key_rows, value_rows, in_gate, forget_gate, out_gate,
             head_gain[None, :], prior, prior_other, other,
         ),
+        near=(9, 10),
     )
 
     sent = jnp.broadcast_to(arrived, (4, 4, slots // 4, columns)).reshape(tp, slots // 4, columns)
@@ -442,15 +475,16 @@
         + [pltpu.VMEM((slots // 4, columns), F32)],
         grid=(grid,),
         in_specs=[
-            pl.BlockSpec((per, slots // 4, columns), lambda i: (i, 0, 0)),
+            pl.BlockSpec(memory_space=pltpu.VMEM),
             weights_spec(width),
             weights_spec(width),
         ]
         + [weights_spec(2 * width)] * 3,
-        out_specs=pl.BlockSpec((tp, slots // 4, 4 * width), lambda i: (0, 0, 0)),
+        out_specs=pl.BlockSpec(memory_space=pltpu.VMEM),
+        near=(0,),
     )
     gathered = exchange(hidden, TP)
-    results = call(down_kernel, sds((slots, columns), BF16), (gathered, down_local))
+    results = call(down_kernel, pltpu.VMEM((slots, columns), BF16), (gathered, down_local), near=(0,))
     back = exchange(results.reshape(ep, 32, columns), EP).reshape(slots, columns)
 
     along_x = [heads[0]]
@@ -471,15 +505,20 @@
         scratch=[pltpu.VMEM((2, block, columns), F32), pltpu.VMEM((tp, block, dv), BF16)],
         grid=(steps,),
         in_specs=[pl.BlockSpec(memory_space=pltpu.SMEM)]
-        + [pl.BlockSpec((4, block, dv), lambda i: (0, 0, 0))] * 4
+        + [pl.BlockSpec(memory_space=pltpu.VMEM)] * 4
         + [pl.BlockSpec((2, pieces, dv, columns), lambda i: (0, i, 0, 0))]
         + [weight_block] * 2,
         out_specs=[pl.BlockSpec((block, columns), lambda i: (0, 0))] * 2,
+        near=(1, 2, 3, 4),
     )
     from_pair = swapped(projected[1], "x")
-    mixer_out = call(assemble_kernel, sds((rows_a, columns), BF16), (at, projected[0], from_pair))
-
-    expert_out = call(collect_kernel, sds((tokens, columns), BF16), (routes, route_weight, back))
+    mixer_out = call(
+        assemble_kernel, sds((rows_a, columns), BF16), (at, projected[0], from_pair), near=(2,)
+    )
+
+    share = [pltpu.VMEM((tokens, slots), BF16)] * 2
+    plan = call(plan_kernel, share, (routes, route_weight))
+    expert_out = call(collect_kernel, sds((tokens, columns), BF16), (*plan, back), near=(0, 1, 2))
     return (mixer_out, expert_out)
 
 

time: 318 us -> 312 us (0.981)
  blocking collectives: 91 us -> 50.1 us
  starting transfers between devices: 64 us -> 98.1 us
  local copies, waits for them, and re-layouts: 14.6 us -> 8.36 us
  waiting for transfers between devices: 114 us -> 120 us
    all_gather x1 -> x0, blocking collectives: 40.7 us -> none  [body(): chips = lax.all_gather(packed, 'z', axis=0)]
    ppermute x0 -> x4, starting transfers between devices: none -> 36.5 us  [body(): lax.ppermute(packed, 'z', [(i, i + reach) for i in range(chips - reach)])]
    ppermute x0 -> x4, waiting for transfers between devices: none -> 11.7 us  [body(): lax.ppermute(packed, 'z', [(i, i + reach) for i in range(chips - reach)])]
    unnamed x34 -> x12, local copies, waits for them, and re-layouts: 9.76 us -> 3.54 us
    ppermute x9, waiting for transfers between devices: 88.1 us -> 83.8 us  [from_next(): return lax.ppermute(x, axis, [((i + k) % n, i) for i in range(n)])]
    ppermute x5, starting transfers between devices: 18.2 us -> 14.1 us  [swapped(): return lax.ppermute(x, axis, [(i ^ 1, i) for i in range(n)])]
    pallas_call x11 -> x15, Pallas kernels: 32.1 us -> 33.1 us  [call(): pl.pallas_call(kernel, out_shape=out, in_specs=in_specs, out_specs=out_sp...]
  transfers between devices with their start and end apart: 17 -> 21, of which waited for: 11 -> 14; matrix products, arithmetic and copies ran while one was open for 2% -> 2% of each run, Pallas kernels for 7% -> 8%
where the time goes in v1:
time: 312 us; the launch traced here: 311 us
  waiting for transfers between devices  120 us (38%)
  starting transfers between devices  98.1 us (31%)
  blocking collectives  50.1 us (16%)
  Pallas kernels  33.1 us (11%)
  local copies, waits for them, and re-layouts  8.36 us (3%)
    ppermute x9, waiting for transfers between devices, from_next(): return lax.ppermute(x, axis, [((i + k) % n, i) for i in range(n)])  83.8 us
    all_to_all x1, blocking collectives, exchange(): return lax.all_to_all(x, axis, split_axis=0, concat_axis=0, tiled=True)  50.1 us
    ppermute x4, starting transfers between devices, body(): lax.ppermute(packed, 'z', [(i, i + reach) for i in range(chips - reach)])  36.5 us
    pallas_call x15, Pallas kernels, call(): pl.pallas_call(kernel, out_shape=out, in_specs=in_specs, out_specs=out_sp...  33.1 us
    ppermute x9, starting transfers between devices, from_next(): return lax.ppermute(x, axis, [((i + k) % n, i) for i in range(n)])  26.3 us
    all_to_all x3, waiting for transfers between devices, exchange(): return lax.all_to_all(x, axis, split_axis=0, concat_axis=0, tiled=True)  22.2 us
    all_to_all x3, starting transfers between devices, exchange(): return lax.all_to_all(x, axis, split_axis=0, concat_axis=0, tiled=True)  21.2 us
    ppermute x5, starting transfers between devices, swapped(): return lax.ppermute(x, axis, [(i ^ 1, i) for i in range(n)])  14.1 us
  transfers between devices with their start and end apart: 21, of which 14 were waited for; matrix products, arithmetic and copies ran while one was open for 2% of the time, Pallas kernels for 8%

profile of v1, /device:TPU:1, one launch (start us, length us, event | category | flops | bytes accessed | tf_op | source)
XLA Modules:
  0.0 310.9 jit_solution(430050502832122807)
XLA Ops:
  2.2 50.1 %all_to_all.20 = bf16[32,32,256]{2,1,0:T(8,128)(2,1)S(1)} all-to-all(bf16[32,32,256]{2,1,0:T(8,128)(2,1)S(1)} %bitcast.22), channel_id=1, replica_groups=mesh['z'=16,'c'=2,'y'=4,'x'=4] {'z','c'}, dimensions={0} | all-to-all | bytes 1048576 | tf_op jit(solution)/shard_map/all_to_all | solution.py:387
  53.8 6.8 %all-to-all-start.1 = ((bf16[16,256,256]{2,1,0:T(8,128)(2,1)}), bf16[16,256,256]{2,1,0:T(8,128)(2,1)S(1)}, u32[]{:S(2)}, u32[]{:S(2)}) async-start(bf16[16,256,256]{2,1,0:T(8,128)(2,1)} %bitcast.24), calls=%async_computation.1 | async-start | bytes 4194304 | tf_op jit(solution)/shard_map/all_to_all | solution.py:387
  62.9 4.5 %collective-permute-start.15 = (bf16[128,4096]{1,0:T(8,128)(2,1)}, bf16[128,4096]{1,0:T(8,128)(2,1)S(1)}, u32[]{:S(2)}, u32[]{:S(2)}) collective-permute-start(bf16[128,4096]{1,0:T(8,128)(2,1)} %shard_map.160), channel_id=1, source_target_pairs={{4,0},{8,4},{12,8},{0,12},{5,1},{9,5},{13,9},{1,13},{6,2},{10,6},{... | collective-permute-start | bytes 3145736 | tf_op jit(solution)/shard_map/ppermute | solution.py:378
  72.3 35.0 %collective-permute-done.15.w1_ref = bf16[128,4096]{1,0:T(8,128)(2,1)S(1)} collective-permute-done((bf16[128,4096]{1,0:T(8,128)(2,1)}, bf16[128,4096]{1,0:T(8,128)(2,1)S(1)}, u32[]{:S(2)}, u32[]{:S(2)}) %collective-permute-start.15) | collective-permute-done | bytes 1048608 | tf_op jit(solution)/shard_map/ppermute | solution.py:378
  110.7 21.7 %collective-permute-done.17.w3_ref = bf16[128,4096]{1,0:T(8,128)(2,1)} collective-permute-done((bf16[128,4096]{1,0:T(8,128)(2,1)}, bf16[128,4096]{1,0:T(8,128)(2,1)}, u32[]{:S(2)}, u32[]{:S(2)}) %collective-permute-start.17) | collective-permute-done | bytes 1048608 | tf_op jit(solution)/shard_map/ppermute | solution.py:378
  132.4 4.8 %shard_map.161 = bf16[16,256,256]{2,1,0:T(8,128)(2,1)} custom-call(bf16[16,256,256]{2,1,0:T(8,128)(2,1)S(1)} %all-to-all-done.1.x_ref, bf16[64,4096]{1,0:T(8,128)(2,1)} %bitcast.28, bf16[64,4096]{1,0:T(8,128)(2,1)} %bitcast.30, bf16[128,4096]{1,0:T(8,128)(2,1)} %copy-done.1, bf16[128,4096]{1,0:T(8,128)(2,1)} %copy-done.2, ...), custom_call_target="tpu_custom_call" | custom-call | tf_op jit(solution)/shard_map/pallas_call | solution.py:46
  137.2 4.4 %all-to-all-start.2 = ((bf16[16,256,256]{2,1,0:T(8,128)(2,1)}), bf16[16,256,256]{2,1,0:T(8,128)(2,1)S(1)}, u32[]{:S(2)}, u32[]{:S(2)}) async-start(bf16[16,256,256]{2,1,0:T(8,128)(2,1)} %shard_map.161), calls=%async_computation.2 | async-start | bytes 4194304 | tf_op jit(solution)/shard_map/all_to_all | solution.py:387
  143.9 3.3 %collective-permute-start.12 = (bf16[2048,256]{1,0:T(8,128)(2,1)}, bf16[2048,256]{1,0:T(8,128)(2,1)}, u32[]{:S(2)}, u32[]{:S(2)}) collective-permute-start(bf16[2048,256]{1,0:T(8,128)(2,1)} %constant_dynamic-slice_fusion), channel_id=1, source_target_pairs={{1,0},{0,1},{3,2},{2,3},{5,4},{4,5},{7,6},{6,7},{9,8},{8,9},{11,10... | collective-permute-start | bytes 3145736 | tf_op jit(solution)/shard_map/ppermute | solution.py:383
  147.2 22.2 %all-to-all-done.2.h_ref = bf16[16,256,256]{2,1,0:T(8,128)(2,1)S(1)} async-done(((bf16[16,256,256]{2,1,0:T(8,128)(2,1)}), bf16[16,256,256]{2,1,0:T(8,128)(2,1)S(1)}, u32[]{:S(2)}, u32[]{:S(2)}) %all-to-all-start.2) | async-done | bytes 2097184 | tf_op jit(solution)/shard_map/all_to_all | solution.py:387
  172.0 10.0 %all-to-all-start.3 = ((bf16[32,32,256]{2,1,0:T(8,128)(2,1)}), bf16[32,32,256]{2,1,0:T(8,128)(2,1)S(1)}, u32[]{:S(2)}, u32[]{:S(2)}) async-start(bf16[32,32,256]{2,1,0:T(8,128)(2,1)} %bitcast.18), calls=%async_computation.3 | async-start | bytes 1048576 | tf_op jit(solution)/shard_map/all_to_all | solution.py:387
  189.2 3.3 %collective-permute-start.1 = (bf16[144,128]{1,0:T(8,128)(2,1)}, bf16[144,128]{1,0:T(8,128)(2,1)S(1)}, u32[]{:S(2)}, u32[]{:S(2)}) collective-permute-start(bf16[144,128]{1,0:T(8,128)(2,1)} %get-tuple-element.16), channel_id=1, source_target_pairs={{0,32},{32,64},{64,96},{96,128},{128,160},{160,192},{192,224},{224... | collective-permute-start | bytes 110600 | tf_op jit(solution)/shard_map/ppermute | solution.py:440
  192.5 7.6 %collective-permute-done.1.came_ref = bf16[144,128]{1,0:T(8,128)(2,1)S(1)} collective-permute-done((bf16[144,128]{1,0:T(8,128)(2,1)}, bf16[144,128]{1,0:T(8,128)(2,1)S(1)}, u32[]{:S(2)}, u32[]{:S(2)}) %collective-permute-start.1) | collective-permute-done | bytes 36896 | tf_op jit(solution)/shard_map/ppermute | solution.py:440
  201.7 8.9 %collective-permute-start.2 = (bf16[144,128]{1,0:T(8,128)(2,1)}, bf16[144,128]{1,0:T(8,128)(2,1)S(1)}, u32[]{:S(2)}, u32[]{:S(2)}) collective-permute-start(bf16[144,128]{1,0:T(8,128)(2,1)} %get-tuple-element.18), channel_id=1, source_target_pairs={{0,64},{32,96},{64,128},{96,160},{128,192},{160,224},{192,256},{22... | collective-permute-start | bytes 110600 | tf_op jit(solution)/shard_map/ppermute | solution.py:440
  213.6 10.1 %collective-permute-start.3 = (bf16[144,128]{1,0:T(8,128)(2,1)}, bf16[144,128]{1,0:T(8,128)(2,1)S(1)}, u32[]{:S(2)}, u32[]{:S(2)}) collective-permute-start(bf16[144,128]{1,0:T(8,128)(2,1)} %get-tuple-element.21), channel_id=1, source_target_pairs={{0,128},{32,160},{64,192},{96,224},{128,256},{160,288},{192,320},{... | collective-permute-start | bytes 110600 | tf_op jit(solution)/shard_map/ppermute | solution.py:440
  226.6 14.3 %collective-permute-start.4 = (bf16[144,128]{1,0:T(8,128)(2,1)}, bf16[144,128]{1,0:T(8,128)(2,1)S(1)}, u32[]{:S(2)}, u32[]{:S(2)}) collective-permute-start(bf16[144,128]{1,0:T(8,128)(2,1)} %get-tuple-element.24), channel_id=1, source_target_pairs={{0,256},{32,288},{64,320},{96,352},{128,384},{160,416},{192,448},{... | collective-permute-start | bytes 110600 | tf_op jit(solution)/shard_map/ppermute | solution.py:440
  243.8 4.9 %collective-permute-start.5 = (f32[136,128]{1,0:T(8,128)}, f32[136,128]{1,0:T(8,128)S(1)}, u32[]{:S(2)}, u32[]{:S(2)}) collective-permute-start(f32[136,128]{1,0:T(8,128)} %shard_map.154.prior_ref), channel_id=1, source_target_pairs={{16,0},{0,16},{17,1},{1,17},{18,2},{2,18},{19,3},{3,19},{20,4},{4,... | collective-permute-start | bytes 208904 | tf_op jit(solution)/shard_map/ppermute | solution.py:383
  250.7 3.3 %shard_map.155 = bf16[2,256,256]{2,1,0:T(8,128)(2,1)} custom-call(s32[4]{0:T(128)} %pad_add_fusion.at_ref, bf16[512,128]{1,0:T(8,128)(2,1)} %q_ref.1, bf16[512,128]{1,0:T(8,128)(2,1)} %k_ref.3, bf16[512,256]{1,0:T(8,128)(2,1)} %v_ref.3, f32[1,512]{1,0:T(1,128)} %in_ref.3, f32[1,512]{1,0:T(1,128)} %forget_ref.3, bf16[512,256]{1,0:T(8,128)(2,1)} %gate_ref.1, ...), custom_call_target="tpu_custom_call" | custom-call | tf_op jit(solution)/shard_map/pallas_call | solution.py:46
  256.9 2.9 collective-permute-start.7
  259.8 3.6 %collective-permute-start.8 = (bf16[256,256]{1,0:T(8,128)(2,1)S(1)}, bf16[256,256]{1,0:T(8,128)(2,1)S(1)}, u32[]{:S(2)}, u32[]{:S(2)}) collective-permute-start(bf16[256,256]{1,0:T(8,128)(2,1)S(1)} %get-tuple-element.32), channel_id=1, source_target_pairs={{1,0},{2,1},{3,2},{0,3},{5,4},{6,5},{7,6},{4,7},{9,8},{10,9},{11,1... | collective-permute-start | bytes 393224 | tf_op jit(solution)/shard_map/ppermute | solution.py:378
  264.9 3.1 collective-permute-done.8
  270.1 3.8 %collective-permute-start.11 = (bf16[4,256,256]{2,1,0:T(8,128)(2,1)S(1)}, bf16[4,256,256]{2,1,0:T(8,128)(2,1)S(1)}, u32[]{:S(2)}, u32[]{:S(2)}) collective-permute-start(bf16[4,256,256]{2,1,0:T(8,128)(2,1)S(1)} %pad_maximum_fusion.h0_ref), channel_id=1, source_target_pairs={{12,0},{0,4},{4,8},{8,12},{13,1},{1,5},{5,9},{9,13},{14,2},{2,6},{... | collective-permute-start | bytes 1572872 | tf_op jit(solution)/shard_map/ppermute | solution.py:378
  276.6 7.2 %collective-permute-done.10.h2_ref = bf16[4,256,256]{2,1,0:T(8,128)(2,1)S(1)} collective-permute-done((bf16[4,256,256]{2,1,0:T(8,128)(2,1)S(1)}, bf16[4,256,256]{2,1,0:T(8,128)(2,1)S(1)}, u32[]{:S(2)}, u32[]{:S(2)}) %collective-permute-start.10) | collective-permute-done | bytes 524320 | tf_op jit(solution)/shard_map/ppermute | solution.py:378
  283.8 12.8 %collective-permute-done.11.h3_ref = bf16[4,256,256]{2,1,0:T(8,128)(2,1)S(1)} collective-permute-done((bf16[4,256,256]{2,1,0:T(8,128)(2,1)S(1)}, bf16[4,256,256]{2,1,0:T(8,128)(2,1)S(1)}, u32[]{:S(2)}, u32[]{:S(2)}) %collective-permute-start.11) | collective-permute-done | bytes 524320 | tf_op jit(solution)/shard_map/ppermute | solution.py:378
  297.6 3.9 %shard_map.156 = (bf16[256,256]{1,0:T(8,128)(2,1)}, bf16[256,256]{1,0:T(8,128)(2,1)}) custom-call(s32[4]{0:T(128)} %pad_add_fusion.at_ref, bf16[4,256,256]{2,1,0:T(8,128)(2,1)S(1)} %pad_maximum_fusion.h0_ref, bf16[4,256,256]{2,1,0:T(8,128)(2,1)S(1)} %collective-permute-done.9.h1_ref, bf16[4,256,256]{2,1,0:T(8,128)(2,1)S(1)} %collective-permute-done.10.h2_ref, ...), custom_call_target="tpu_custom_call" | custom-call | tf_op jit(solution)/shard_map/pallas_call | solution.py:46
  (51 shorter events, 57.5 us)
Async XLA Ops:
  53.8 78.6 %all-to-all-start.1 = ((bf16[16,256,256]{2,1,0:T(8,128)(2,1)}), bf16[16,256,256]{2,1,0:T(8,128)(2,1)S(1)}, u32[]{:S(2)}, u32[]{:S(2)}) async-start(bf16[16,256,256]{2,1,0:T(8,128)(2,1)} %bitcast.24), calls=%async_computation.1 | async-start | bytes 4194304 | tf_op jit(solution)/shard_map/all_to_all | solution.py:387
  62.9 44.4 %collective-permute-start.15 = (bf16[128,4096]{1,0:T(8,128)(2,1)}, bf16[128,4096]{1,0:T(8,128)(2,1)S(1)}, u32[]{:S(2)}, u32[]{:S(2)}) collective-permute-start(bf16[128,4096]{1,0:T(8,128)(2,1)} %shard_map.160), channel_id=1, source_target_pairs={{4,0},{8,4},{12,8},{0,12},{5,1},{9,5},{13,9},{1,13},{6,2},{10,6},{... | collective-permute-start | bytes 3145736 | tf_op jit(solution)/shard_map/ppermute | solution.py:378
  67.3 42.4 %collective-permute-start.16 = (bf16[128,4096]{1,0:T(8,128)(2,1)}, bf16[128,4096]{1,0:T(8,128)(2,1)S(1)}, u32[]{:S(2)}, u32[]{:S(2)}) collective-permute-start(bf16[128,4096]{1,0:T(8,128)(2,1)} %shard_map.160), channel_id=1, source_target_pairs={{8,0},{12,4},{0,8},{4,12},{9,1},{13,5},{1,9},{5,13},{10,2},{14,6},... | collective-permute-start | bytes 3145736 | tf_op jit(solution)/shard_map/ppermute | solution.py:378
  69.8 62.6 %collective-permute-start.17 = (bf16[128,4096]{1,0:T(8,128)(2,1)}, bf16[128,4096]{1,0:T(8,128)(2,1)}, u32[]{:S(2)}, u32[]{:S(2)}) collective-permute-start(bf16[128,4096]{1,0:T(8,128)(2,1)} %shard_map.160), channel_id=1, source_target_pairs={{12,0},{0,4},{4,8},{8,12},{13,1},{1,5},{5,9},{9,13},{14,2},{2,6},{... | collective-permute-start | bytes 3145736 | tf_op jit(solution)/shard_map/ppermute | solution.py:378
  107.3 2.4 copy-start.1
  137.2 32.2 %all-to-all-start.2 = ((bf16[16,256,256]{2,1,0:T(8,128)(2,1)}), bf16[16,256,256]{2,1,0:T(8,128)(2,1)S(1)}, u32[]{:S(2)}, u32[]{:S(2)}) async-start(bf16[16,256,256]{2,1,0:T(8,128)(2,1)} %shard_map.161), calls=%async_computation.2 | async-start | bytes 4194304 | tf_op jit(solution)/shard_map/all_to_all | solution.py:387
  143.9 104.8 %collective-permute-start.12 = (bf16[2048,256]{1,0:T(8,128)(2,1)}, bf16[2048,256]{1,0:T(8,128)(2,1)}, u32[]{:S(2)}, u32[]{:S(2)}) collective-permute-start(bf16[2048,256]{1,0:T(8,128)(2,1)} %constant_dynamic-slice_fusion), channel_id=1, source_target_pairs={{1,0},{0,1},{3,2},{2,3},{5,4},{4,5},{7,6},{6,7},{9,8},{8,9},{11,10... | collective-permute-start | bytes 3145736 | tf_op jit(solution)/shard_map/ppermute | solution.py:383
  172.0 137.8 %all-to-all-start.3 = ((bf16[32,32,256]{2,1,0:T(8,128)(2,1)}), bf16[32,32,256]{2,1,0:T(8,128)(2,1)S(1)}, u32[]{:S(2)}, u32[]{:S(2)}) async-start(bf16[32,32,256]{2,1,0:T(8,128)(2,1)} %bitcast.18), calls=%async_computation.3 | async-start | bytes 1048576 | tf_op jit(solution)/shard_map/all_to_all | solution.py:387
  184.1 3.5 %collective-permute-start = (f32[136,256]{1,0:T(8,128)}, f32[136,256]{1,0:T(8,128)S(1)}, u32[]{:S(2)}, u32[]{:S(2)}) collective-permute-start(f32[136,256]{1,0:T(8,128)} %shard_map.149.mine_ref), channel_id=1, source_target_pairs={{16,0},{0,16},{17,1},{1,17},{18,2},{2,18},{19,3},{3,19},{20,4},{4,... | collective-permute-start | bytes 417800 | tf_op jit(solution)/shard_map/ppermute | solution.py:383
  189.2 10.9 %collective-permute-start.1 = (bf16[144,128]{1,0:T(8,128)(2,1)}, bf16[144,128]{1,0:T(8,128)(2,1)S(1)}, u32[]{:S(2)}, u32[]{:S(2)}) collective-permute-start(bf16[144,128]{1,0:T(8,128)(2,1)} %get-tuple-element.16), channel_id=1, source_target_pairs={{0,32},{32,64},{64,96},{96,128},{128,160},{160,192},{192,224},{224... | collective-permute-start | bytes 110600 | tf_op jit(solution)/shard_map/ppermute | solution.py:440
  201.7 10.3 %collective-permute-start.2 = (bf16[144,128]{1,0:T(8,128)(2,1)}, bf16[144,128]{1,0:T(8,128)(2,1)S(1)}, u32[]{:S(2)}, u32[]{:S(2)}) collective-permute-start(bf16[144,128]{1,0:T(8,128)(2,1)} %get-tuple-element.18), channel_id=1, source_target_pairs={{0,64},{32,96},{64,128},{96,160},{128,192},{160,224},{192,256},{22... | collective-permute-start | bytes 110600 | tf_op jit(solution)/shard_map/ppermute | solution.py:440
  213.6 11.4 %collective-permute-start.3 = (bf16[144,128]{1,0:T(8,128)(2,1)}, bf16[144,128]{1,0:T(8,128)(2,1)S(1)}, u32[]{:S(2)}, u32[]{:S(2)}) collective-permute-start(bf16[144,128]{1,0:T(8,128)(2,1)} %get-tuple-element.21), channel_id=1, source_target_pairs={{0,128},{32,160},{64,192},{96,224},{128,256},{160,288},{192,320},{... | collective-permute-start | bytes 110600 | tf_op jit(solution)/shard_map/ppermute | solution.py:440
  226.6 15.6 %collective-permute-start.4 = (bf16[144,128]{1,0:T(8,128)(2,1)}, bf16[144,128]{1,0:T(8,128)(2,1)S(1)}, u32[]{:S(2)}, u32[]{:S(2)}) collective-permute-start(bf16[144,128]{1,0:T(8,128)(2,1)} %get-tuple-element.24), channel_id=1, source_target_pairs={{0,256},{32,288},{64,320},{96,352},{128,384},{160,416},{192,448},{... | collective-permute-start | bytes 110600 | tf_op jit(solution)/shard_map/ppermute | solution.py:440
  243.8 6.9 %collective-permute-start.5 = (f32[136,128]{1,0:T(8,128)}, f32[136,128]{1,0:T(8,128)S(1)}, u32[]{:S(2)}, u32[]{:S(2)}) collective-permute-start(f32[136,128]{1,0:T(8,128)} %shard_map.154.prior_ref), channel_id=1, source_target_pairs={{16,0},{0,16},{17,1},{1,17},{18,2},{2,18},{19,3},{3,19},{20,4},{4,... | collective-permute-start | bytes 208904 | tf_op jit(solution)/shard_map/ppermute | solution.py:383
  248.8 47.8 %collective-permute-start.13 = (bf16[2048,256]{1,0:T(8,128)(2,1)}, bf16[2048,256]{1,0:T(8,128)(2,1)S(1)}, u32[]{:S(2)}, u32[]{:S(2)}) collective-permute-start(bf16[2048,256]{1,0:T(8,128)(2,1)} %collective-permute-done.12.a_ref), channel_id=1, source_target_pairs={{16,0},{0,16},{17,1},{1,17},{18,2},{2,18},{19,3},{3,19},{20,4},{4,... | collective-permute-start | bytes 3145736 | tf_op jit(solution)/shard_map/ppermute | solution.py:383
  255.0 8.4 %collective-permute-start.6 = (bf16[256,256]{1,0:T(8,128)(2,1)S(1)}, bf16[256,256]{1,0:T(8,128)(2,1)S(1)}, u32[]{:S(2)}, u32[]{:S(2)}) collective-permute-start(bf16[256,256]{1,0:T(8,128)(2,1)S(1)} %get-tuple-element.32), channel_id=1, source_target_pairs={{3,0},{0,1},{1,2},{2,3},{7,4},{4,5},{5,6},{6,7},{11,8},{8,9},{9,10... | collective-permute-start | bytes 393224 | tf_op jit(solution)/shard_map/ppermute | solution.py:378
  256.9 8.0 %collective-permute-start.7 = (bf16[256,256]{1,0:T(8,128)(2,1)S(1)}, bf16[256,256]{1,0:T(8,128)(2,1)S(1)}, u32[]{:S(2)}, u32[]{:S(2)}) collective-permute-start(bf16[256,256]{1,0:T(8,128)(2,1)S(1)} %get-tuple-element.31), channel_id=1, source_target_pairs={{2,0},{3,1},{0,2},{1,3},{6,4},{7,5},{4,6},{5,7},{10,8},{11,9},{8,1... | collective-permute-start | bytes 393224 | tf_op jit(solution)/shard_map/ppermute | solution.py:378
  259.8 8.2 %collective-permute-start.8 = (bf16[256,256]{1,0:T(8,128)(2,1)S(1)}, bf16[256,256]{1,0:T(8,128)(2,1)S(1)}, u32[]{:S(2)}, u32[]{:S(2)}) collective-permute-start(bf16[256,256]{1,0:T(8,128)(2,1)S(1)} %get-tuple-element.32), channel_id=1, source_target_pairs={{1,0},{2,1},{3,2},{0,3},{5,4},{6,5},{7,6},{4,7},{9,8},{10,9},{11,1... | collective-permute-start | bytes 393224 | tf_op jit(solution)/shard_map/ppermute | solution.py:378
  268.1 15.6 %collective-permute-start.10 = (bf16[4,256,256]{2,1,0:T(8,128)(2,1)S(1)}, bf16[4,256,256]{2,1,0:T(8,128)(2,1)S(1)}, u32[]{:S(2)}, u32[]{:S(2)}) collective-permute-start(bf16[4,256,256]{2,1,0:T(8,128)(2,1)S(1)} %pad_maximum_fusion.h0_ref), channel_id=1, source_target_pairs={{8,0},{12,4},{0,8},{4,12},{9,1},{13,5},{1,9},{5,13},{10,2},{14,6},... | collective-permute-start | bytes 1572872 | tf_op jit(solution)/shard_map/ppermute | solution.py:378
  270.1 26.6 %collective-permute-start.11 = (bf16[4,256,256]{2,1,0:T(8,128)(2,1)S(1)}, bf16[4,256,256]{2,1,0:T(8,128)(2,1)S(1)}, u32[]{:S(2)}, u32[]{:S(2)}) collective-permute-start(bf16[4,256,256]{2,1,0:T(8,128)(2,1)S(1)} %pad_maximum_fusion.h0_ref), channel_id=1, source_target_pairs={{12,0},{0,4},{4,8},{8,12},{13,1},{1,5},{5,9},{9,13},{14,2},{2,6},{... | collective-permute-start | bytes 1572872 | tf_op jit(solution)/shard_map/ppermute | solution.py:378
  273.9 22.7 %collective-permute-start.9 = (bf16[4,256,256]{2,1,0:T(8,128)(2,1)S(1)}, bf16[4,256,256]{2,1,0:T(8,128)(2,1)S(1)}, u32[]{:S(2)}, u32[]{:S(2)}) collective-permute-start(bf16[4,256,256]{2,1,0:T(8,128)(2,1)S(1)} %pad_maximum_fusion.h0_ref), channel_id=1, source_target_pairs={{4,0},{8,4},{12,8},{0,12},{5,1},{9,5},{13,9},{1,13},{6,2},{10,6},{... | collective-permute-start | bytes 1572872 | tf_op jit(solution)/shard_map/ppermute | solution.py:378
  297.6 5.8 %copy-start.3 = (s32[256,2]{0,1:T(2,128)S(1)}, s32[256,2]{0,1:T(2,128)}, u32[]{:S(2)}) copy-start(s32[256,2]{0,1:T(2,128)} %param.23) | copy-start | bytes 6148
  297.6 6.6 %copy-start.4 = (f32[256,2]{0,1:T(2,128)S(1)}, f32[256,2]{0,1:T(2,128)}, u32[]{:S(2)}) copy-start(f32[256,2]{0,1:T(2,128)} %param.24) | copy-start | bytes 6148
  301.5 6.7 %collective-permute-start.14 = (bf16[256,256]{1,0:T(8,128)(2,1)}, bf16[256,256]{1,0:T(8,128)(2,1)S(1)}, u32[]{:S(2)}, u32[]{:S(2)}) collective-permute-start(bf16[256,256]{1,0:T(8,128)(2,1)} %get-tuple-element.27), channel_id=1, source_target_pairs={{1,0},{0,1},{3,2},{2,3},{5,4},{4,5},{7,6},{6,7},{9,8},{8,9},{11,10... | collective-permute-start | bytes 393224 | tf_op jit(solution)/shard_map/ppermute | solution.py:383
  (2 other events, 2.0 us)

commit v2 on v1

--- a/solution.py
+++ b/solution.py
@@ -247,12 +247,6 @@
     out_ref[...] = dot(chosen, x_ref[...]).astype(BF16)
 
 
-def pair_kernel(gate_ref, up_ref, out_ref):
-    width = gate_ref.shape[0]
-    out_ref[0:width, :] = gate_ref[...]
-    out_ref[width:, :] = up_ref[...]
-
-
 def plan_kernel(routes_ref, weight_ref, high_ref, low_ref):
     tokens, slots = high_ref.shape
     experts, room = 32, slots // 32
@@ -281,17 +275,16 @@
 
 
 def hidden_kernel(
-    x_ref, gate_ref, up_ref, w1_ref, w2_ref, w3_ref, out_ref, gate_acc, up_acc, squares
+    x_ref, g0_ref, g1_ref, g2_ref, g3_ref, u0_ref, u1_ref, u2_ref, u3_ref,
+    out_ref, gate_acc, up_acc, squares,
 ):
     step = pl.program_id(0)
-    width = gate_ref.shape[0]
-    far = (w1_ref, w2_ref, w3_ref)
     _, _, columns = x_ref.shape
-    senders = gate_ref.shape[1] // columns
+    senders = g0_ref.shape[1] // columns
     pieces = [x_ref[step * senders + i] for i in range(senders)]
     x = jnp.concatenate(pieces, axis=1)
-    gate = jnp.concatenate([gate_ref[...]] + [w[0:width] for w in far], axis=0)
-    up = jnp.concatenate([up_ref[...]] + [w[width:] for w in far], axis=0)
+    gate = jnp.concatenate([w[...] for w in (g0_ref, g1_ref, g2_ref, g3_ref)], axis=0)
+    up = jnp.concatenate([w[...] for w in (u0_ref, u1_ref, u2_ref, u3_ref)], axis=0)
     gate_part, up_part = dot_t(x, gate), dot_t(x, up)
     square = jnp.zeros(squares.shape, F32)
     for piece in pieces:
@@ -419,13 +412,15 @@
     arrived = exchange(table.reshape(ep, 32, columns), EP)
     arrived = arrived.reshape(4, 1, slots // 4, columns)
 
-    pair = call(pair_kernel, sds((2 * width, gate_local.shape[1]), BF16), (gate_local, up_local))
     own_half = lax.dynamic_slice_in_dim(
         mix_weight, at[0] * (mix_weight.shape[0] // 2), mix_weight.shape[0] // 2, 0
     )
-    far = []
-    for k in (1, 2, 3):
-        far.append(from_next(pair, "y", k))
+    gate_1 = from_next(gate_local, "y", 1)
+    up_3 = from_next(up_local, "y", 3)
+    gate_3 = from_next(gate_local, "y", 3)
+    up_1 = from_next(up_local, "y", 1)
+    gate_2 = from_next(gate_1, "y", 1)
+    up_2 = from_next(up_3, "y", 3)
     mix_far = swapped(own_half, "x")
     mix_swap = swapped(mix_far, "c")
 
@@ -470,16 +465,14 @@
     hidden = call(
         hidden_kernel,
         sds((tp, slots // 4, 4 * width), BF16),
-        (rows, gate_local, up_local, *far),
+        (rows, gate_local, gate_1, gate_2, gate_3, up_local, up_1, up_2, up_3),
         scratch=[pltpu.VMEM((slots // 4, 4 * width), F32)] * 2
         + [pltpu.VMEM((slots // 4, columns), F32)],
         grid=(grid,),
         in_specs=[
             pl.BlockSpec(memory_space=pltpu.VMEM),
-            weights_spec(width),
-            weights_spec(width),
         ]
-        + [weights_spec(2 * width)] * 3,
+        + [weights_spec(width)] * 8,
         out_specs=pl.BlockSpec(memory_space=pltpu.VMEM),
         near=(0,),
     )

time: 312 us -> 301 us (0.965)
  waiting for transfers between devices: 120 us -> 101 us
  starting transfers between devices: 98.1 us -> 107 us
    ppermute x9 -> x12, waiting for transfers between devices: 83.8 us -> 65.2 us  [from_next(): return lax.ppermute(x, axis, [((i + k) % n, i) for i in range(n)])]
    ppermute x9 -> x12, starting transfers between devices: 26.3 us -> 35.2 us  [from_next(): return lax.ppermute(x, axis, [((i + k) % n, i) for i in range(n)])]
    pallas_call x15 -> x14, Pallas kernels: 33.1 us -> 30.9 us  [call(): pl.pallas_call(kernel, out_shape=out, in_specs=in_specs, out_specs=out_sp...]
  transfers between devices with their start and end apart: 21 -> 24, of which waited for: 14 -> 15; matrix products, arithmetic and copies ran while one was open for 2% -> 2% of each run, Pallas kernels for 8% -> 8%
where the time goes in v2:
time: 301 us; the launch traced here: 299 us
  starting transfers between devices  107 us (36%)
  waiting for transfers between devices  101 us (34%)
  blocking collectives  50.1 us (17%)
  Pallas kernels  30.9 us (10%)
  local copies, waits for them, and re-layouts  8.26 us (3%)
    ppermute x12, waiting for transfers between devices, from_next(): return lax.ppermute(x, axis, [((i + k) % n, i) for i in range(n)])  65.2 us
    all_to_all x1, blocking collectives, exchange(): return lax.all_to_all(x, axis, split_axis=0, concat_axis=0, tiled=True)  50.1 us
    ppermute x4, starting transfers between devices, body(): lax.ppermute(packed, 'z', [(i, i + reach) for i in range(chips - reach)])  36.5 us
    ppermute x12, starting transfers between devices, from_next(): return lax.ppermute(x, axis, [((i + k) % n, i) for i in range(n)])  35.2 us
    pallas_call x14, Pallas kernels, call(): pl.pallas_call(kernel, out_shape=out, in_specs=in_specs, out_specs=out_sp...  30.9 us
    all_to_all x3, waiting for transfers between devices, exchange(): return lax.all_to_all(x, axis, split_axis=0, concat_axis=0, tiled=True)  22.6 us
    all_to_all x3, starting transfers between devices, exchange(): return lax.all_to_all(x, axis, split_axis=0, concat_axis=0, tiled=True)  21.2 us
    ppermute x5, starting transfers between devices, swapped(): return lax.ppermute(x, axis, [(i ^ 1, i) for i in range(n)])  14.1 us
  transfers between devices with their start and end apart: 24, of which 15 were waited for; matrix products, arithmetic and copies ran while one was open for 2% of the time, Pallas kernels for 8%

profile of v2, /device:TPU:1, one launch (start us, length us, event | category | flops | bytes accessed | tf_op | source)
XLA Modules:
  0.0 299.4 jit_solution(18059362208533565952)
XLA Ops:
  2.2 50.1 %all_to_all.20 = bf16[32,32,256]{2,1,0:T(8,128)(2,1)S(1)} all-to-all(bf16[32,32,256]{2,1,0:T(8,128)(2,1)S(1)} %bitcast.22), channel_id=1, replica_groups=mesh['z'=16,'c'=2,'y'=4,'x'=4] {'z','c'}, dimensions={0} | all-to-all | bytes 1048576 | tf_op jit(solution)/shard_map/all_to_all | solution.py:380
  53.8 6.9 %all-to-all-start.1 = ((bf16[16,256,256]{2,1,0:T(8,128)(2,1)}), bf16[16,256,256]{2,1,0:T(8,128)(2,1)S(1)}, u32[]{:S(2)}, u32[]{:S(2)}) async-start(bf16[16,256,256]{2,1,0:T(8,128)(2,1)} %bitcast.24), calls=%async_computation.1 | async-start | bytes 4194304 | tf_op jit(solution)/shard_map/all_to_all | solution.py:380
  60.8 4.5 %collective-permute-start.15 = (bf16[64,4096]{1,0:T(8,128)(2,1)S(1)}, bf16[64,4096]{1,0:T(8,128)(2,1)S(1)}, u32[]{:S(2)}, u32[]{:S(2)}) collective-permute-start(bf16[64,4096]{1,0:T(8,128)(2,1)S(1)} %bitcast.28), channel_id=1, source_target_pairs={{4,0},{8,4},{12,8},{0,12},{5,1},{9,5},{13,9},{1,13},{6,2},{10,6},{... | collective-permute-start | bytes 1572872 | tf_op jit(solution)/shard_map/ppermute | solution.py:371
  69.3 4.3 %collective-permute-start.18 = (bf16[64,4096]{1,0:T(8,128)(2,1)S(1)}, bf16[64,4096]{1,0:T(8,128)(2,1)S(1)}, u32[]{:S(2)}, u32[]{:S(2)}) collective-permute-start(bf16[64,4096]{1,0:T(8,128)(2,1)S(1)} %bitcast.32), channel_id=1, source_target_pairs={{4,0},{8,4},{12,8},{0,12},{5,1},{9,5},{13,9},{1,13},{6,2},{10,6},{... | collective-permute-start | bytes 1572872 | tf_op jit(solution)/shard_map/ppermute | solution.py:371
  73.7 22.4 %collective-permute-done.15.g1_ref = bf16[64,4096]{1,0:T(8,128)(2,1)S(1)} collective-permute-done((bf16[64,4096]{1,0:T(8,128)(2,1)S(1)}, bf16[64,4096]{1,0:T(8,128)(2,1)S(1)}, u32[]{:S(2)}, u32[]{:S(2)}) %collective-permute-start.15) | collective-permute-done | bytes 524320 | tf_op jit(solution)/shard_map/ppermute | solution.py:371
  96.1 3.3 %collective-permute-start.16 = (bf16[64,4096]{1,0:T(8,128)(2,1)S(1)}, bf16[64,4096]{1,0:T(8,128)(2,1)S(1)}, u32[]{:S(2)}, u32[]{:S(2)}) collective-permute-start(bf16[64,4096]{1,0:T(8,128)(2,1)S(1)} %collective-permute-done.15.g1_ref), channel_id=1, source_target_pairs={{4,0},{8,4},{12,8},{0,12},{5,1},{9,5},{13,9},{1,13},{6,2},{10,6},{... | collective-permute-start | bytes 1572872 | tf_op jit(solution)/shard_map/ppermute | solution.py:371
  101.6 7.7 %collective-permute-done.17.g3_ref = bf16[64,4096]{1,0:T(8,128)(2,1)S(1)} collective-permute-done((bf16[64,4096]{1,0:T(8,128)(2,1)S(1)}, bf16[64,4096]{1,0:T(8,128)(2,1)S(1)}, u32[]{:S(2)}, u32[]{:S(2)}) %collective-permute-start.17) | collective-permute-done | bytes 524320 | tf_op jit(solution)/shard_map/ppermute | solution.py:371
  109.3 9.4 %collective-permute-done.16.g2_ref = bf16[64,4096]{1,0:T(8,128)(2,1)S(1)} collective-permute-done((bf16[64,4096]{1,0:T(8,128)(2,1)S(1)}, bf16[64,4096]{1,0:T(8,128)(2,1)S(1)}, u32[]{:S(2)}, u32[]{:S(2)}) %collective-permute-start.16) | collective-permute-done | bytes 524320 | tf_op jit(solution)/shard_map/ppermute | solution.py:371
  120.6 4.8 %shard_map.160 = bf16[16,256,256]{2,1,0:T(8,128)(2,1)} custom-call(bf16[16,256,256]{2,1,0:T(8,128)(2,1)S(1)} %all-to-all-done.1.x_ref, bf16[64,4096]{1,0:T(8,128)(2,1)} %bitcast.27, bf16[64,4096]{1,0:T(8,128)(2,1)} %copy-done.3, bf16[64,4096]{1,0:T(8,128)(2,1)} %copy-done.7, bf16[64,4096]{1,0:T(8,128)(2,1)} %copy-done.5, bf16[64,4096]{1,0:T(8,128)(2,1)} %bitcast.30, ...), custom_call_target="tpu_custom_call" | custom-call | tf_op jit(solution)/shard_map/pallas_call | solution.py:46
  125.5 5.1 %all-to-all-start.2 = ((bf16[16,256,256]{2,1,0:T(8,128)(2,1)}), bf16[16,256,256]{2,1,0:T(8,128)(2,1)S(1)}, u32[]{:S(2)}, u32[]{:S(2)}) async-start(bf16[16,256,256]{2,1,0:T(8,128)(2,1)} %shard_map.160), calls=%async_computation.2 | async-start | bytes 4194304 | tf_op jit(solution)/shard_map/all_to_all | solution.py:380
  136.1 22.6 %all-to-all-done.2.h_ref = bf16[16,256,256]{2,1,0:T(8,128)(2,1)S(1)} async-done(((bf16[16,256,256]{2,1,0:T(8,128)(2,1)}), bf16[16,256,256]{2,1,0:T(8,128)(2,1)S(1)}, u32[]{:S(2)}, u32[]{:S(2)}) %all-to-all-start.2) | async-done | bytes 2097184 | tf_op jit(solution)/shard_map/all_to_all | solution.py:380
  161.3 9.2 %all-to-all-start.3 = ((bf16[32,32,256]{2,1,0:T(8,128)(2,1)}), bf16[32,32,256]{2,1,0:T(8,128)(2,1)S(1)}, u32[]{:S(2)}, u32[]{:S(2)}) async-start(bf16[32,32,256]{2,1,0:T(8,128)(2,1)} %bitcast.18), calls=%async_computation.3 | async-start | bytes 1048576 | tf_op jit(solution)/shard_map/all_to_all | solution.py:380
  177.7 3.3 %collective-permute-start.1 = (bf16[144,128]{1,0:T(8,128)(2,1)}, bf16[144,128]{1,0:T(8,128)(2,1)S(1)}, u32[]{:S(2)}, u32[]{:S(2)}) collective-permute-start(bf16[144,128]{1,0:T(8,128)(2,1)} %get-tuple-element.16), channel_id=1, source_target_pairs={{0,32},{32,64},{64,96},{96,128},{128,160},{160,192},{192,224},{224... | collective-permute-start | bytes 110600 | tf_op jit(solution)/shard_map/ppermute | solution.py:435
  181.0 7.6 %collective-permute-done.1.came_ref = bf16[144,128]{1,0:T(8,128)(2,1)S(1)} collective-permute-done((bf16[144,128]{1,0:T(8,128)(2,1)}, bf16[144,128]{1,0:T(8,128)(2,1)S(1)}, u32[]{:S(2)}, u32[]{:S(2)}) %collective-permute-start.1) | collective-permute-done | bytes 36896 | tf_op jit(solution)/shard_map/ppermute | solution.py:435
  190.2 8.9 %collective-permute-start.2 = (bf16[144,128]{1,0:T(8,128)(2,1)}, bf16[144,128]{1,0:T(8,128)(2,1)S(1)}, u32[]{:S(2)}, u32[]{:S(2)}) collective-permute-start(bf16[144,128]{1,0:T(8,128)(2,1)} %get-tuple-element.18), channel_id=1, source_target_pairs={{0,64},{32,96},{64,128},{96,160},{128,192},{160,224},{192,256},{22... | collective-permute-start | bytes 110600 | tf_op jit(solution)/shard_map/ppermute | solution.py:435
  202.1 10.1 %collective-permute-start.3 = (bf16[144,128]{1,0:T(8,128)(2,1)}, bf16[144,128]{1,0:T(8,128)(2,1)S(1)}, u32[]{:S(2)}, u32[]{:S(2)}) collective-permute-start(bf16[144,128]{1,0:T(8,128)(2,1)} %get-tuple-element.21), channel_id=1, source_target_pairs={{0,128},{32,160},{64,192},{96,224},{128,256},{160,288},{192,320},{... | collective-permute-start | bytes 110600 | tf_op jit(solution)/shard_map/ppermute | solution.py:435
  215.1 14.3 %collective-permute-start.4 = (bf16[144,128]{1,0:T(8,128)(2,1)}, bf16[144,128]{1,0:T(8,128)(2,1)S(1)}, u32[]{:S(2)}, u32[]{:S(2)}) collective-permute-start(bf16[144,128]{1,0:T(8,128)(2,1)} %get-tuple-element.24), channel_id=1, source_target_pairs={{0,256},{32,288},{64,320},{96,352},{128,384},{160,416},{192,448},{... | collective-permute-start | bytes 110600 | tf_op jit(solution)/shard_map/ppermute | solution.py:435
  232.3 4.9 %collective-permute-start.5 = (f32[136,128]{1,0:T(8,128)}, f32[136,128]{1,0:T(8,128)S(1)}, u32[]{:S(2)}, u32[]{:S(2)}) collective-permute-start(f32[136,128]{1,0:T(8,128)} %shard_map.154.prior_ref), channel_id=1, source_target_pairs={{16,0},{0,16},{17,1},{1,17},{18,2},{2,18},{19,3},{3,19},{20,4},{4,... | collective-permute-start | bytes 208904 | tf_op jit(solution)/shard_map/ppermute | solution.py:376
  239.2 3.3 %shard_map.155 = bf16[2,256,256]{2,1,0:T(8,128)(2,1)} custom-call(s32[4]{0:T(128)} %pad_add_fusion.at_ref, bf16[512,128]{1,0:T(8,128)(2,1)} %q_ref.1, bf16[512,128]{1,0:T(8,128)(2,1)} %k_ref.3, bf16[512,256]{1,0:T(8,128)(2,1)} %v_ref.3, f32[1,512]{1,0:T(1,128)} %in_ref.3, f32[1,512]{1,0:T(1,128)} %forget_ref.3, bf16[512,256]{1,0:T(8,128)(2,1)} %gate_ref.1, ...), custom_call_target="tpu_custom_call" | custom-call | tf_op jit(solution)/shard_map/pallas_call | solution.py:46
  248.3 3.6 %collective-permute-start.8 = (bf16[256,256]{1,0:T(8,128)(2,1)S(1)}, bf16[256,256]{1,0:T(8,128)(2,1)S(1)}, u32[]{:S(2)}, u32[]{:S(2)}) collective-permute-start(bf16[256,256]{1,0:T(8,128)(2,1)S(1)} %get-tuple-element.32), channel_id=1, source_target_pairs={{1,0},{2,1},{3,2},{0,3},{5,4},{6,5},{7,6},{4,7},{9,8},{10,9},{11,1... | collective-permute-start | bytes 393224 | tf_op jit(solution)/shard_map/ppermute | solution.py:371
  258.6 3.8 %collective-permute-start.11 = (bf16[4,256,256]{2,1,0:T(8,128)(2,1)S(1)}, bf16[4,256,256]{2,1,0:T(8,128)(2,1)S(1)}, u32[]{:S(2)}, u32[]{:S(2)}) collective-permute-start(bf16[4,256,256]{2,1,0:T(8,128)(2,1)S(1)} %pad_maximum_fusion.h0_ref), channel_id=1, source_target_pairs={{12,0},{0,4},{4,8},{8,12},{13,1},{1,5},{5,9},{9,13},{14,2},{2,6},{... | collective-permute-start | bytes 1572872 | tf_op jit(solution)/shard_map/ppermute | solution.py:371
  265.1 7.2 %collective-permute-done.10.h2_ref = bf16[4,256,256]{2,1,0:T(8,128)(2,1)S(1)} collective-permute-done((bf16[4,256,256]{2,1,0:T(8,128)(2,1)S(1)}, bf16[4,256,256]{2,1,0:T(8,128)(2,1)S(1)}, u32[]{:S(2)}, u32[]{:S(2)}) %collective-permute-start.10) | collective-permute-done | bytes 524320 | tf_op jit(solution)/shard_map/ppermute | solution.py:371
  272.3 12.8 %collective-permute-done.11.h3_ref = bf16[4,256,256]{2,1,0:T(8,128)(2,1)S(1)} collective-permute-done((bf16[4,256,256]{2,1,0:T(8,128)(2,1)S(1)}, bf16[4,256,256]{2,1,0:T(8,128)(2,1)S(1)}, u32[]{:S(2)}, u32[]{:S(2)}) %collective-permute-start.11) | collective-permute-done | bytes 524320 | tf_op jit(solution)/shard_map/ppermute | solution.py:371
  286.1 3.9 %shard_map.156 = (bf16[256,256]{1,0:T(8,128)(2,1)}, bf16[256,256]{1,0:T(8,128)(2,1)}) custom-call(s32[4]{0:T(128)} %pad_add_fusion.at_ref, bf16[4,256,256]{2,1,0:T(8,128)(2,1)S(1)} %pad_maximum_fusion.h0_ref, bf16[4,256,256]{2,1,0:T(8,128)(2,1)S(1)} %collective-permute-done.9.h1_ref, bf16[4,256,256]{2,1,0:T(8,128)(2,1)S(1)} %collective-permute-done.10.h2_ref, ...), custom_call_target="tpu_custom_call" | custom-call | tf_op jit(solution)/shard_map/pallas_call | solution.py:46
  (66 shorter events, 64.4 us)
Async XLA Ops:
  53.8 66.8 %all-to-all-start.1 = ((bf16[16,256,256]{2,1,0:T(8,128)(2,1)}), bf16[16,256,256]{2,1,0:T(8,128)(2,1)S(1)}, u32[]{:S(2)}, u32[]{:S(2)}) async-start(bf16[16,256,256]{2,1,0:T(8,128)(2,1)} %bitcast.24), calls=%async_computation.1 | async-start | bytes 4194304 | tf_op jit(solution)/shard_map/all_to_all | solution.py:380
  60.8 35.4 %collective-permute-start.15 = (bf16[64,4096]{1,0:T(8,128)(2,1)S(1)}, bf16[64,4096]{1,0:T(8,128)(2,1)S(1)}, u32[]{:S(2)}, u32[]{:S(2)}) collective-permute-start(bf16[64,4096]{1,0:T(8,128)(2,1)S(1)} %bitcast.28), channel_id=1, source_target_pairs={{4,0},{8,4},{12,8},{0,12},{5,1},{9,5},{13,9},{1,13},{6,2},{10,6},{... | collective-permute-start | bytes 1572872 | tf_op jit(solution)/shard_map/ppermute | solution.py:371
  65.3 34.2 %collective-permute-start.19 = (bf16[64,4096]{1,0:T(8,128)(2,1)S(1)}, bf16[64,4096]{1,0:T(8,128)(2,1)S(1)}, u32[]{:S(2)}, u32[]{:S(2)}) collective-permute-start(bf16[64,4096]{1,0:T(8,128)(2,1)S(1)} %bitcast.31), channel_id=1, source_target_pairs={{12,0},{0,4},{4,8},{8,12},{13,1},{1,5},{5,9},{9,13},{14,2},{2,6},{... | collective-permute-start | bytes 1572872 | tf_op jit(solution)/shard_map/ppermute | solution.py:371
  67.2 42.1 %collective-permute-start.17 = (bf16[64,4096]{1,0:T(8,128)(2,1)S(1)}, bf16[64,4096]{1,0:T(8,128)(2,1)S(1)}, u32[]{:S(2)}, u32[]{:S(2)}) collective-permute-start(bf16[64,4096]{1,0:T(8,128)(2,1)S(1)} %bitcast.29), channel_id=1, source_target_pairs={{12,0},{0,4},{4,8},{8,12},{13,1},{1,5},{5,9},{9,13},{14,2},{2,6},{... | collective-permute-start | bytes 1572872 | tf_op jit(solution)/shard_map/ppermute | solution.py:371
  69.3 40.0 %collective-permute-start.18 = (bf16[64,4096]{1,0:T(8,128)(2,1)S(1)}, bf16[64,4096]{1,0:T(8,128)(2,1)S(1)}, u32[]{:S(2)}, u32[]{:S(2)}) collective-permute-start(bf16[64,4096]{1,0:T(8,128)(2,1)S(1)} %bitcast.32), channel_id=1, source_target_pairs={{4,0},{8,4},{12,8},{0,12},{5,1},{9,5},{13,9},{1,13},{6,2},{10,6},{... | collective-permute-start | bytes 1572872 | tf_op jit(solution)/shard_map/ppermute | solution.py:371
  96.1 22.6 %collective-permute-start.16 = (bf16[64,4096]{1,0:T(8,128)(2,1)S(1)}, bf16[64,4096]{1,0:T(8,128)(2,1)S(1)}, u32[]{:S(2)}, u32[]{:S(2)}) collective-permute-start(bf16[64,4096]{1,0:T(8,128)(2,1)S(1)} %collective-permute-done.15.g1_ref), channel_id=1, source_target_pairs={{4,0},{8,4},{12,8},{0,12},{5,1},{9,5},{13,9},{1,13},{6,2},{10,6},{... | collective-permute-start | bytes 1572872 | tf_op jit(solution)/shard_map/ppermute | solution.py:371
  99.5 21.2 %collective-permute-start.20 = (bf16[64,4096]{1,0:T(8,128)(2,1)S(1)}, bf16[64,4096]{1,0:T(8,128)(2,1)}, u32[]{:S(2)}, u32[]{:S(2)}) collective-permute-start(bf16[64,4096]{1,0:T(8,128)(2,1)S(1)} %collective-permute-done.19.u3_ref), channel_id=1, source_target_pairs={{12,0},{0,4},{4,8},{8,12},{13,1},{1,5},{5,9},{9,13},{14,2},{2,6},{... | collective-permute-start | bytes 1572872 | tf_op jit(solution)/shard_map/ppermute | solution.py:371
  125.5 33.3 %all-to-all-start.2 = ((bf16[16,256,256]{2,1,0:T(8,128)(2,1)}), bf16[16,256,256]{2,1,0:T(8,128)(2,1)S(1)}, u32[]{:S(2)}, u32[]{:S(2)}) async-start(bf16[16,256,256]{2,1,0:T(8,128)(2,1)} %shard_map.160), calls=%async_computation.2 | async-start | bytes 4194304 | tf_op jit(solution)/shard_map/all_to_all | solution.py:380
  132.8 104.4 %collective-permute-start.12 = (bf16[2048,256]{1,0:T(8,128)(2,1)}, bf16[2048,256]{1,0:T(8,128)(2,1)}, u32[]{:S(2)}, u32[]{:S(2)}) collective-permute-start(bf16[2048,256]{1,0:T(8,128)(2,1)} %constant_dynamic-slice_fusion), channel_id=1, source_target_pairs={{1,0},{0,1},{3,2},{2,3},{5,4},{4,5},{7,6},{6,7},{9,8},{8,9},{11,10... | collective-permute-start | bytes 3145736 | tf_op jit(solution)/shard_map/ppermute | solution.py:376
  161.3 137.0 %all-to-all-start.3 = ((bf16[32,32,256]{2,1,0:T(8,128)(2,1)}), bf16[32,32,256]{2,1,0:T(8,128)(2,1)S(1)}, u32[]{:S(2)}, u32[]{:S(2)}) async-start(bf16[32,32,256]{2,1,0:T(8,128)(2,1)} %bitcast.18), calls=%async_computation.3 | async-start | bytes 1048576 | tf_op jit(solution)/shard_map/all_to_all | solution.py:380
  172.6 3.5 %collective-permute-start = (f32[136,256]{1,0:T(8,128)}, f32[136,256]{1,0:T(8,128)S(1)}, u32[]{:S(2)}, u32[]{:S(2)}) collective-permute-start(f32[136,256]{1,0:T(8,128)} %shard_map.149.mine_ref), channel_id=1, source_target_pairs={{16,0},{0,16},{17,1},{1,17},{18,2},{2,18},{19,3},{3,19},{20,4},{4,... | collective-permute-start | bytes 417800 | tf_op jit(solution)/shard_map/ppermute | solution.py:376
  177.7 10.9 %collective-permute-start.1 = (bf16[144,128]{1,0:T(8,128)(2,1)}, bf16[144,128]{1,0:T(8,128)(2,1)S(1)}, u32[]{:S(2)}, u32[]{:S(2)}) collective-permute-start(bf16[144,128]{1,0:T(8,128)(2,1)} %get-tuple-element.16), channel_id=1, source_target_pairs={{0,32},{32,64},{64,96},{96,128},{128,160},{160,192},{192,224},{224... | collective-permute-start | bytes 110600 | tf_op jit(solution)/shard_map/ppermute | solution.py:435
  190.2 10.3 %collective-permute-start.2 = (bf16[144,128]{1,0:T(8,128)(2,1)}, bf16[144,128]{1,0:T(8,128)(2,1)S(1)}, u32[]{:S(2)}, u32[]{:S(2)}) collective-permute-start(bf16[144,128]{1,0:T(8,128)(2,1)} %get-tuple-element.18), channel_id=1, source_target_pairs={{0,64},{32,96},{64,128},{96,160},{128,192},{160,224},{192,256},{22... | collective-permute-start | bytes 110600 | tf_op jit(solution)/shard_map/ppermute | solution.py:435
  202.1 11.4 %collective-permute-start.3 = (bf16[144,128]{1,0:T(8,128)(2,1)}, bf16[144,128]{1,0:T(8,128)(2,1)S(1)}, u32[]{:S(2)}, u32[]{:S(2)}) collective-permute-start(bf16[144,128]{1,0:T(8,128)(2,1)} %get-tuple-element.21), channel_id=1, source_target_pairs={{0,128},{32,160},{64,192},{96,224},{128,256},{160,288},{192,320},{... | collective-permute-start | bytes 110600 | tf_op jit(solution)/shard_map/ppermute | solution.py:435
  215.1 15.6 %collective-permute-start.4 = (bf16[144,128]{1,0:T(8,128)(2,1)}, bf16[144,128]{1,0:T(8,128)(2,1)S(1)}, u32[]{:S(2)}, u32[]{:S(2)}) collective-permute-start(bf16[144,128]{1,0:T(8,128)(2,1)} %get-tuple-element.24), channel_id=1, source_target_pairs={{0,256},{32,288},{64,320},{96,352},{128,384},{160,416},{192,448},{... | collective-permute-start | bytes 110600 | tf_op jit(solution)/shard_map/ppermute | solution.py:435
  232.3 6.9 %collective-permute-start.5 = (f32[136,128]{1,0:T(8,128)}, f32[136,128]{1,0:T(8,128)S(1)}, u32[]{:S(2)}, u32[]{:S(2)}) collective-permute-start(f32[136,128]{1,0:T(8,128)} %shard_map.154.prior_ref), channel_id=1, source_target_pairs={{16,0},{0,16},{17,1},{1,17},{18,2},{2,18},{19,3},{3,19},{20,4},{4,... | collective-permute-start | bytes 208904 | tf_op jit(solution)/shard_map/ppermute | solution.py:376
  237.3 47.8 %collective-permute-start.13 = (bf16[2048,256]{1,0:T(8,128)(2,1)}, bf16[2048,256]{1,0:T(8,128)(2,1)S(1)}, u32[]{:S(2)}, u32[]{:S(2)}) collective-permute-start(bf16[2048,256]{1,0:T(8,128)(2,1)} %collective-permute-done.12.a_ref), channel_id=1, source_target_pairs={{16,0},{0,16},{17,1},{1,17},{18,2},{2,18},{19,3},{3,19},{20,4},{4,... | collective-permute-start | bytes 3145736 | tf_op jit(solution)/shard_map/ppermute | solution.py:376
  243.5 8.4 %collective-permute-start.6 = (bf16[256,256]{1,0:T(8,128)(2,1)S(1)}, bf16[256,256]{1,0:T(8,128)(2,1)S(1)}, u32[]{:S(2)}, u32[]{:S(2)}) collective-permute-start(bf16[256,256]{1,0:T(8,128)(2,1)S(1)} %get-tuple-element.32), channel_id=1, source_target_pairs={{3,0},{0,1},{1,2},{2,3},{7,4},{4,5},{5,6},{6,7},{11,8},{8,9},{9,10... | collective-permute-start | bytes 393224 | tf_op jit(solution)/shard_map/ppermute | solution.py:371
  245.4 8.0 %collective-permute-start.7 = (bf16[256,256]{1,0:T(8,128)(2,1)S(1)}, bf16[256,256]{1,0:T(8,128)(2,1)S(1)}, u32[]{:S(2)}, u32[]{:S(2)}) collective-permute-start(bf16[256,256]{1,0:T(8,128)(2,1)S(1)} %get-tuple-element.31), channel_id=1, source_target_pairs={{2,0},{3,1},{0,2},{1,3},{6,4},{7,5},{4,6},{5,7},{10,8},{11,9},{8,1... | collective-permute-start | bytes 393224 | tf_op jit(solution)/shard_map/ppermute | solution.py:371
  248.3 8.2 %collective-permute-start.8 = (bf16[256,256]{1,0:T(8,128)(2,1)S(1)}, bf16[256,256]{1,0:T(8,128)(2,1)S(1)}, u32[]{:S(2)}, u32[]{:S(2)}) collective-permute-start(bf16[256,256]{1,0:T(8,128)(2,1)S(1)} %get-tuple-element.32), channel_id=1, source_target_pairs={{1,0},{2,1},{3,2},{0,3},{5,4},{6,5},{7,6},{4,7},{9,8},{10,9},{11,1... | collective-permute-start | bytes 393224 | tf_op jit(solution)/shard_map/ppermute | solution.py:371
  256.6 15.6 %collective-permute-start.10 = (bf16[4,256,256]{2,1,0:T(8,128)(2,1)S(1)}, bf16[4,256,256]{2,1,0:T(8,128)(2,1)S(1)}, u32[]{:S(2)}, u32[]{:S(2)}) collective-permute-start(bf16[4,256,256]{2,1,0:T(8,128)(2,1)S(1)} %pad_maximum_fusion.h0_ref), channel_id=1, source_target_pairs={{8,0},{12,4},{0,8},{4,12},{9,1},{13,5},{1,9},{5,13},{10,2},{14,6},... | collective-permute-start | bytes 1572872 | tf_op jit(solution)/shard_map/ppermute | solution.py:371
  258.6 26.6 %collective-permute-start.11 = (bf16[4,256,256]{2,1,0:T(8,128)(2,1)S(1)}, bf16[4,256,256]{2,1,0:T(8,128)(2,1)S(1)}, u32[]{:S(2)}, u32[]{:S(2)}) collective-permute-start(bf16[4,256,256]{2,1,0:T(8,128)(2,1)S(1)} %pad_maximum_fusion.h0_ref), channel_id=1, source_target_pairs={{12,0},{0,4},{4,8},{8,12},{13,1},{1,5},{5,9},{9,13},{14,2},{2,6},{... | collective-permute-start | bytes 1572872 | tf_op jit(solution)/shard_map/ppermute | solution.py:371
  262.4 22.7 %collective-permute-start.9 = (bf16[4,256,256]{2,1,0:T(8,128)(2,1)S(1)}, bf16[4,256,256]{2,1,0:T(8,128)(2,1)S(1)}, u32[]{:S(2)}, u32[]{:S(2)}) collective-permute-start(bf16[4,256,256]{2,1,0:T(8,128)(2,1)S(1)} %pad_maximum_fusion.h0_ref), channel_id=1, source_target_pairs={{4,0},{8,4},{12,8},{0,12},{5,1},{9,5},{13,9},{1,13},{6,2},{10,6},{... | collective-permute-start | bytes 1572872 | tf_op jit(solution)/shard_map/ppermute | solution.py:371
  290.0 6.7 %collective-permute-start.14 = (bf16[256,256]{1,0:T(8,128)(2,1)}, bf16[256,256]{1,0:T(8,128)(2,1)S(1)}, u32[]{:S(2)}, u32[]{:S(2)}) collective-permute-start(bf16[256,256]{1,0:T(8,128)(2,1)} %get-tuple-element.27), channel_id=1, source_target_pairs={{1,0},{0,1},{3,2},{2,3},{5,4},{4,5},{7,6},{6,7},{9,8},{8,9},{11,10... | collective-permute-start | bytes 393224 | tf_op jit(solution)/shard_map/ppermute | solution.py:376
  (10 other events, 93.2 us)

commit v3 on v2

--- a/solution.py
+++ b/solution.py
@@ -1,5 +1,3 @@
-import functools
-
 import jax
 import jax.numpy as jnp
 from jax import lax
@@ -85,16 +83,14 @@
     )
     normal = jnp.sum(weighted, axis=0, keepdims=True)
     width = out_ref.shape[1]
-    out_ref[0:dk, :] = memory
-    out_ref[dk : dk + 1, 0:dk] = normal
-    out_ref[dk : dk + 1, dk:] = normal
-    out_ref[dk + 1 : dk + 2, :] = jnp.broadcast_to(total, (1, width))
-    out_ref[dk + 2 : dk + 3, :] = jnp.broadcast_to(top, (1, width))
-    out_ref[dk + 3 :, :] = jnp.zeros((out_ref.shape[0] - dk - 3, width), F32)
-
-
-def parts_of(x, dk):
-    return x[0:dk, :], x[dk : dk + 1, :], x[dk + 1 : dk + 2, :], x[dk + 2 : dk + 3, :]
+    normal = jnp.concatenate([normal] * (width // dk), axis=1)
+    pack(
+        out_ref,
+        memory,
+        normal,
+        jnp.broadcast_to(total, (1, width)),
+        jnp.broadcast_to(top, (1, width)),
+    )
 
 
 def fold(first, second):
@@ -147,59 +143,18 @@
     )
 
 
-def store_state(out_ref, state):
-    memory, normal, decay, top = state
-    dk, width = memory.shape
-    out_ref[0:dk, :] = memory
-    out_ref[dk:, :] = jnp.concatenate(
-        [normal, decay, top, jnp.zeros((out_ref.shape[0] - dk - 3, width), F32)], axis=0
-    )
-
-
-def chip_kernel(at_ref, mine_ref, other_ref, total_ref, packed_ref):
-    dk = 128
-    south = at_ref[0] == 0
-    mine, other = mine_ref[...], other_ref[...]
-    first = parts_of(jnp.where(south, mine, other), dk)
-    second = parts_of(jnp.where(south, other, mine), dk)
-    total = fold(first, second)
-    half = mine.shape[1] // 2
-    total = [jnp.where(south, v[:, :half], v[:, half:]) for v in total]
-    store_state(total_ref, total)
-    pack(packed_ref, *total)
-
-
-def step_kernel(reach, first, last, at_ref, came_ref, *refs):
-    dk = 128
-    valid = at_ref[1] >= reach
-    came = unpack(came_ref[...], dk)
-    if first:
-        before = first_state(dk, came_ref.shape[1])
-    else:
-        before, refs = parts_of(refs[0][...], dk), refs[1:]
-    joined = fold(came, before)
-    if not last:
-        total = parts_of(refs[0][...], dk)
-        more = fold(came, total)
-        total = [jnp.where(valid, new, old) for new, old in zip(more, total)]
-        store_state(refs[1], total)
-        pack(refs[3], *total)
-    store_state(refs[0 if last else 2], [jnp.where(valid, n, o) for n, o in zip(joined, before)])
-
-
 def output_kernel(
-    at_ref, q_ref, k_ref, v_ref, in_ref, forget_ref, gate_ref, gain_ref,
-    prior_ref, prior_other_ref, other_ref, out_ref,
+    at_ref, q_ref, k_ref, v_ref, in_ref, forget_ref, gate_ref, gain_ref, all_ref, out_ref
 ):
     n, dk = q_ref.shape
     scale = dk ** (-0.5)
-    south = at_ref[0] == 0
     column, row = cumulative_forms(forget_ref[...])
-    left = jnp.where(south, prior_ref[...], prior_other_ref[...])
-    right = jnp.where(south, prior_other_ref[...], prior_ref[...])
-    before = parts_of(jnp.concatenate([left, right], axis=1), dk)
-    joined = fold(before, parts_of(other_ref[...], dk))
-    memory, normal, _, top_before = [jnp.where(south, b, j) for b, j in zip(before, joined)]
+    memory, normal, _, top_before = lax.fori_loop(
+        0,
+        at_ref[0],
+        lambda k, state: fold(state, unpack(all_ref[k], dk)),
+        first_state(dk, all_ref.shape[2]),
+    )
     normal = normal[:, :dk]
     top_before = top_before[:, 0:1]
     log_in = in_ref[...]
@@ -225,8 +180,7 @@
         values = values * lax.rsqrt(jnp.mean(values * values, axis=1, keepdims=True) + EPSILON)
         gate = gate_ref[rows, :].astype(F32)
         values = values * gain_ref[...] * (1.0 / (1.0 + jnp.exp(-gate)))
-        side, inner = divmod(start, n // 2)
-        out_ref[lax.rem(at_ref[2] + side, 2), inner : inner + step, :] = values.astype(BF16)
+        out_ref[rows, :] = values.astype(BF16)
 
 
 def dispatch_kernel(routes_ref, x_ref, out_ref):
@@ -326,54 +280,29 @@
         out_ref[ys * rows : (ys + 1) * rows, :] = total.astype(BF16)
 
 
-def mix_kernel(
-    at_ref, h0_ref, h1_ref, h2_ref, h3_ref, near_ref, a_ref, b_ref, o0_ref, o1_ref, acc, heads
-):
+def mix_kernel(h_ref, w_ref, out_ref, acc):
     step = pl.program_id(0)
-    half = heads.shape[0] // 2
-    c, x, y = at_ref[0], at_ref[2], at_ref[3]
+    width = h_ref.shape[2]
+    total = jnp.zeros(acc.shape, F32)
+    for i in range(h_ref.shape[0]):
+        total = total + dot(h_ref[i], w_ref[i * width : (i + 1) * width, :])
 
     @pl.when(step == 0)
     def _():
-        acc[...] = jnp.zeros_like(acc)
-        for ky, ref in enumerate((h0_ref, h1_ref, h2_ref, h3_ref)):
-            for kx in range(4):
-                heads[lax.rem(y + ky, 4) * 4 + lax.rem(x + 4 - kx, 4)] = ref[kx]
-
-    pieces = near_ref.shape[1]
-    width = near_ref.shape[2]
-    own = jnp.zeros(acc.shape[1:], F32)
-    pair = jnp.zeros(acc.shape[1:], F32)
-    for i in range(pieces):
-        k = step * pieces + i
-        rows = slice(i * width, (i + 1) * width)
-        own = own + dot(heads[k], near_ref[0, i]) + dot(heads[half + k], near_ref[1, i])
-        pair = pair + dot(heads[c * half + k], a_ref[rows, :])
-        pair = pair + dot(heads[(1 - c) * half + k], b_ref[rows, :])
-    acc[0] += own
-    acc[1] += pair
+        acc[...] = total
+
+    @pl.when(step > 0)
+    def _():
+        acc[...] += total
 
     @pl.when(step == pl.num_programs(0) - 1)
     def _():
-        o0_ref[...] = acc[0].astype(BF16)
-        o1_ref[...] = acc[1].astype(BF16)
-
-
-def assemble_kernel(at_ref, own_ref, pair_ref, out_ref):
-    block = own_ref.shape[0]
-    side = lax.rem(at_ref[2], 2)
-    out_ref[pl.ds(pl.multiple_of(side * block, block), block), :] = own_ref[...]
-    out_ref[pl.ds(pl.multiple_of((1 - side) * block, block), block), :] = pair_ref[...]
+        out_ref[...] = acc[...].astype(BF16)
 
 
 def from_next(x, axis, k):
     n = lax.axis_size(axis)
     return lax.ppermute(x, axis, [((i + k) % n, i) for i in range(n)])
-
-
-def swapped(x, axis):
-    n = lax.axis_size(axis)
-    return lax.ppermute(x, axis, [(i ^ 1, i) for i in range(n)])
 
 
 def exchange(x, axis):
@@ -404,57 +333,29 @@
     gate_local, up_local, down_local = gate_weight[0], up_weight[0], down_weight[0]
     width = gate_local.shape[0]
     slots = ep * 32
-    at = jnp.stack(
-        [lax.axis_index(axis) for axis in ("c", "z", "x", "y")]
-    ).astype(jnp.int32)
+    at = lax.axis_index(EP).astype(jnp.int32)[None]
 
     table = call(dispatch_kernel, pltpu.VMEM((slots, columns), BF16), (routes.T, expert_input))
     arrived = exchange(table.reshape(ep, 32, columns), EP)
     arrived = arrived.reshape(4, 1, slots // 4, columns)
 
-    own_half = lax.dynamic_slice_in_dim(
-        mix_weight, at[0] * (mix_weight.shape[0] // 2), mix_weight.shape[0] // 2, 0
-    )
     gate_1 = from_next(gate_local, "y", 1)
     up_3 = from_next(up_local, "y", 3)
     gate_3 = from_next(gate_local, "y", 3)
     up_1 = from_next(up_local, "y", 1)
     gate_2 = from_next(gate_1, "y", 1)
     up_2 = from_next(up_3, "y", 3)
-    mix_far = swapped(own_half, "x")
-    mix_swap = swapped(mix_far, "c")
-
     mine = call(
-        summary_kernel, sds((dk + 8, dv), F32), (key_rows, value_rows, in_gate, forget_gate)
-    )
-    other = swapped(mine, "c")
-    state, lines = sds((dk + 8, dv // 2), F32), sds((dk + 16, dv // 2), BF16)
-    total, packed = call(chip_kernel, [state, lines], (at, mine, other), near=(2,))
-    before, reach, chips = (), 1, lax.axis_size("z")
-    while reach < chips:
-        came = lax.ppermute(packed, "z", [(i, i + reach) for i in range(chips - reach)])
-        last = 2 * reach == chips
-        result = call(
-            functools.partial(step_kernel, reach, reach == 1, last),
-            [state] if last else [state, state, lines],
-            (at, came, *before) + (() if last else (total,)),
-            near=(1,),
-        )
-        if last:
-            (prior,) = result
-        else:
-            total, before, packed = result[0], result[1:2], result[2]
-        reach *= 2
-    prior_other = swapped(prior, "c")
-    block = rows_a // 2
+        summary_kernel, sds((dk + 16, dv), BF16), (key_rows, value_rows, in_gate, forget_gate)
+    )
+    states = lax.all_gather(mine, EP, axis=0)
     heads = call(
         output_kernel,
-        sds((2, block, dv), BF16),
+        sds((rows_a, dv), BF16),
         (
             at, query_rows, key_rows, value_rows, in_gate, forget_gate, out_gate,
-            head_gain[None, :], prior, prior_other, other,
+            head_gain[None, :], states,
         ),
-        near=(9, 10),
     )
 
     sent = jnp.broadcast_to(arrived, (4, 4, slots // 4, columns)).reshape(tp, slots // 4, columns)
@@ -480,33 +381,19 @@
     results = call(down_kernel, pltpu.VMEM((slots, columns), BF16), (gathered, down_local), near=(0,))
     back = exchange(results.reshape(ep, 32, columns), EP).reshape(slots, columns)
 
-    along_x = [heads[0]]
-    for k in (1, 2, 3):
-        along_x.append(from_next(heads[k % 2], "x", -k))
-    along_x = jnp.stack(along_x)
-    head_rows = [along_x]
-    for k in (1, 2, 3):
-        head_rows.append(from_next(along_x, "y", k))
-    half = tp // 2
+    all_heads = lax.all_gather(heads, TP, axis=0)
     steps = 2
-    pieces = half // steps
-    weight_block = pl.BlockSpec((pieces * dv, columns), lambda i: (i, 0))
-    projected = call(
+    mixer_out = call(
         mix_kernel,
-        [sds((block, columns), BF16)] * 2,
-        (at, *head_rows, mix_weight.reshape(2, half, dv, columns), mix_far, mix_swap),
-        scratch=[pltpu.VMEM((2, block, columns), F32), pltpu.VMEM((tp, block, dv), BF16)],
+        sds((rows_a, columns), BF16),
+        (all_heads, mix_weight),
+        scratch=[pltpu.VMEM((rows_a, columns), F32)],
         grid=(steps,),
-        in_specs=[pl.BlockSpec(memory_space=pltpu.SMEM)]
-        + [pl.BlockSpec(memory_space=pltpu.VMEM)] * 4
-        + [pl.BlockSpec((2, pieces, dv, columns), lambda i: (0, i, 0, 0))]
-        + [weight_block] * 2,
-        out_specs=[pl.BlockSpec((block, columns), lambda i: (0, 0))] * 2,
-        near=(1, 2, 3, 4),
-    )
-    from_pair = swapped(projected[1], "x")
-    mixer_out = call(
-        assemble_kernel, sds((rows_a, columns), BF16), (at, projected[0], from_pair), near=(2,)
+        in_specs=[
+            pl.BlockSpec((tp // steps, rows_a, dv), lambda i: (i, 0, 0)),
+            pl.BlockSpec((tp * dv // steps, columns), lambda i: (i, 0)),
+        ],
+        out_specs=pl.BlockSpec((rows_a, columns), lambda i: (0, 0)),
     )
 
     share = [pltpu.VMEM((tokens, slots), BF16)] * 2

time: 301 us -> 276 us (0.917)
  starting transfers between devices: 107 us -> 50.2 us
  waiting for transfers between devices: 101 us -> 154 us
  blocking collectives: 50.1 us -> 30 us
  between operations: 0.96 us -> 14.2 us
  Pallas kernels: 30.9 us -> 23.2 us
  local copies, waits for them, and re-layouts: 8.26 us -> 3.98 us
    all_gather x0 -> x2, waiting for transfers between devices: none -> 67 us  [the longest x1 67 us: body(): states = lax.all_gather(mine, EP, axis=0)]
    ppermute x9 -> x0, starting transfers between devices: 50.7 us -> none  [the longest x4 36.5 us: body(): lax.ppermute(packed, 'z', [(i, i + reach) for i in range(chips - reach)])]
    all_to_all x1, blocking collectives: 50.1 us -> 30 us  [exchange(): return lax.all_to_all(x, axis, split_axis=0, concat_axis=0, tiled=True)]
    ppermute x12 -> x6, starting transfers between devices: 35.2 us -> 18.2 us  [from_next(): return lax.ppermute(x, axis, [((i + k) % n, i) for i in range(n)])]
    ppermute x9 -> x0, waiting for transfers between devices: 13.6 us -> none  [the longest x4 11.7 us: body(): lax.ppermute(packed, 'z', [(i, i + reach) for i in range(chips - reach)])]
    all_to_all x3, starting transfers between devices: 21.2 us -> 31.9 us  [exchange(): return lax.all_to_all(x, axis, split_axis=0, concat_axis=0, tiled=True)]
    ppermute x12 -> x6, waiting for transfers between devices: 65.2 us -> 57.1 us  [from_next(): return lax.ppermute(x, axis, [((i + k) % n, i) for i in range(n)])]
    pallas_call x14 -> x8, Pallas kernels: 30.9 us -> 23.2 us  [call(): pl.pallas_call(kernel, out_shape=out, in_specs=in_specs, out_specs=out_sp...]
  transfers between devices with their start and end apart: 24 -> 11, of which waited for: 15 -> 6; matrix products, arithmetic and copies ran while one was open for 2% -> 1% of each run, Pallas kernels for 8% -> 6%
where the time goes in v3:
time: 276 us
  waiting for transfers between devices  154 us (56%)
  starting transfers between devices  50.2 us (18%)
  blocking collectives  30 us (11%)
  Pallas kernels  23.2 us (8%)
  between operations  14.2 us (5%)
  local copies, waits for them, and re-layouts  3.98 us (1%)
    all_gather x1, waiting for transfers between devices, body(): states = lax.all_gather(mine, EP, axis=0)  67 us
    ppermute x6, waiting for transfers between devices, from_next(): return lax.ppermute(x, axis, [((i + k) % n, i) for i in range(n)])  57.1 us
    all_to_all x3, starting transfers between devices, exchange(): return lax.all_to_all(x, axis, split_axis=0, concat_axis=0, tiled=True)  31.9 us
    all_to_all x3, waiting for transfers between devices, exchange(): return lax.all_to_all(x, axis, split_axis=0, concat_axis=0, tiled=True)  30 us
    all_to_all x1, blocking collectives, exchange(): return lax.all_to_all(x, axis, split_axis=0, concat_axis=0, tiled=True)  30 us
    pallas_call x8, Pallas kernels, call(): pl.pallas_call(kernel, out_shape=out, in_specs=in_specs, out_specs=out_sp...  23.2 us
    ppermute x6, starting transfers between devices, from_next(): return lax.ppermute(x, axis, [((i + k) % n, i) for i in range(n)])  18.2 us
  transfers between devices with their start and end apart: 11, of which 6 were waited for; matrix products, arithmetic and copies ran while one was open for 1% of the time, Pallas kernels for 6%

profile of v3, /device:TPU:1, one launch (start us, length us, event | category | flops | bytes accessed | tf_op | source)
XLA Modules:
  0.0 275.7 jit_solution(914187488474759927)
XLA Ops:
  7.2 2.1 shard_map.149
  9.3 2.4 shard_map.153
  11.7 16.7 %all-to-all-start = ((bf16[32,32,256]{2,1,0:T(8,128)(2,1)}), bf16[32,32,256]{2,1,0:T(8,128)(2,1)S(1)}, u32[]{:S(2)}, u32[]{:S(2)}) async-start(bf16[32,32,256]{2,1,0:T(8,128)(2,1)} %bitcast.5), calls=%async_computation | async-start | bytes 1048576 | tf_op jit(solution)/shard_map/all_to_all | solution.py:309
  28.5 67.0 %all-gather.5.cloned.1.call-done = bf16[4608,256]{1,0:T(8,128)(2,1)} async-done(((bf16[144,256]{1,0:T(8,128)(2,1)}), bf16[4608,256]{1,0:T(8,128)(2,1)}) %all-gather.5.cloned.1.call-update) | async-done | bytes 2359312 | tf_op jit(solution)/shard_map/all_gather | solution.py:351
  95.5 4.1 %shard_map.150 = bf16[512,256]{1,0:T(8,128)(2,1)} custom-call(s32[1]{0:T(128)} %bitcast.at_ref, bf16[512,128]{1,0:T(8,128)(2,1)} %q_ref.1, bf16[512,128]{1,0:T(8,128)(2,1)} %k_ref.3, bf16[512,256]{1,0:T(8,128)(2,1)} %v_ref.3, f32[1,512]{1,0:T(1,128)} %in_ref.3, f32[1,512]{1,0:T(1,128)} %forget_ref.3, bf16[512,256]{1,0:T(8,128)(2,1)} %gate_ref.1, ...), custom_call_target="tpu_custom_call" | custom-call | tf_op jit(solution)/shard_map/pallas_call | solution.py:44
  99.6 1.6 broadcast_in_dim.16
  101.2 6.8 %all-to-all-start.1 = ((bf16[16,256,256]{2,1,0:T(8,128)(2,1)}), bf16[16,256,256]{2,1,0:T(8,128)(2,1)S(1)}, u32[]{:S(2)}, u32[]{:S(2)}) async-start(bf16[16,256,256]{2,1,0:T(8,128)(2,1)} %bitcast.14), calls=%async_computation.1 | async-start | bytes 4194304 | tf_op jit(solution)/shard_map/all_to_all | solution.py:309
  108.0 4.5 %collective-permute-start = (bf16[64,4096]{1,0:T(8,128)(2,1)S(1)}, bf16[64,4096]{1,0:T(8,128)(2,1)S(1)}, u32[]{:S(2)}, u32[]{:S(2)}) collective-permute-start(bf16[64,4096]{1,0:T(8,128)(2,1)S(1)} %bitcast.19), channel_id=1, source_target_pairs={{4,0},{8,4},{12,8},{0,12},{5,1},{9,5},{13,9},{1,13},{6,2},{10,6},{... | collective-permute-start | bytes 1572872 | tf_op jit(solution)/shard_map/ppermute | solution.py:305
  112.5 1.9 collective-permute-start.4
  114.4 2.1 collective-permute-start.2
  116.6 4.3 %collective-permute-start.3 = (bf16[64,4096]{1,0:T(8,128)(2,1)S(1)}, bf16[64,4096]{1,0:T(8,128)(2,1)S(1)}, u32[]{:S(2)}, u32[]{:S(2)}) collective-permute-start(bf16[64,4096]{1,0:T(8,128)(2,1)S(1)} %bitcast.23), channel_id=1, source_target_pairs={{4,0},{8,4},{12,8},{0,12},{5,1},{9,5},{13,9},{1,13},{6,2},{10,6},{... | collective-permute-start | bytes 1572872 | tf_op jit(solution)/shard_map/ppermute | solution.py:305
  120.9 26.9 %collective-permute-done.g1_ref = bf16[64,4096]{1,0:T(8,128)(2,1)S(1)} collective-permute-done((bf16[64,4096]{1,0:T(8,128)(2,1)S(1)}, bf16[64,4096]{1,0:T(8,128)(2,1)S(1)}, u32[]{:S(2)}, u32[]{:S(2)}) %collective-permute-start) | collective-permute-done | bytes 524320 | tf_op jit(solution)/shard_map/ppermute | solution.py:305
  147.8 3.3 %collective-permute-start.1 = (bf16[64,4096]{1,0:T(8,128)(2,1)S(1)}, bf16[64,4096]{1,0:T(8,128)(2,1)S(1)}, u32[]{:S(2)}, u32[]{:S(2)}) collective-permute-start(bf16[64,4096]{1,0:T(8,128)(2,1)S(1)} %collective-permute-done.g1_ref), channel_id=1, source_target_pairs={{4,0},{8,4},{12,8},{0,12},{5,1},{9,5},{13,9},{1,13},{6,2},{10,6},{... | collective-permute-start | bytes 1572872 | tf_op jit(solution)/shard_map/ppermute | solution.py:305
  151.2 1.9 collective-permute-start.5
  153.1 8.6 %collective-permute-done.2.g3_ref = bf16[64,4096]{1,0:T(8,128)(2,1)S(1)} collective-permute-done((bf16[64,4096]{1,0:T(8,128)(2,1)S(1)}, bf16[64,4096]{1,0:T(8,128)(2,1)S(1)}, u32[]{:S(2)}, u32[]{:S(2)}) %collective-permute-start.2) | collective-permute-done | bytes 524320 | tf_op jit(solution)/shard_map/ppermute | solution.py:305
  161.7 20.0 %collective-permute-done.1.g2_ref = bf16[64,4096]{1,0:T(8,128)(2,1)S(1)} collective-permute-done((bf16[64,4096]{1,0:T(8,128)(2,1)S(1)}, bf16[64,4096]{1,0:T(8,128)(2,1)S(1)}, u32[]{:S(2)}, u32[]{:S(2)}) %collective-permute-start.1) | collective-permute-done | bytes 524320 | tf_op jit(solution)/shard_map/ppermute | solution.py:305
  182.5 1.6 collective-permute-done.5.u2_ref
  184.2 4.8 %shard_map.154 = bf16[16,256,256]{2,1,0:T(8,128)(2,1)} custom-call(bf16[16,256,256]{2,1,0:T(8,128)(2,1)S(1)} %all-to-all-done.1.x_ref, bf16[64,4096]{1,0:T(8,128)(2,1)} %bitcast.18, bf16[64,4096]{1,0:T(8,128)(2,1)} %copy-done.2, bf16[64,4096]{1,0:T(8,128)(2,1)} %copy-done.6, bf16[64,4096]{1,0:T(8,128)(2,1)} %copy-done.4, bf16[64,4096]{1,0:T(8,128)(2,1)} %bitcast.21, ...), custom_call_target="tpu_custom_call" | custom-call | tf_op jit(solution)/shard_map/pallas_call | solution.py:44
  189.0 30.0 %all_to_all.20.h_ref = bf16[16,256,256]{2,1,0:T(8,128)(2,1)S(1)} all-to-all(bf16[16,256,256]{2,1,0:T(8,128)(2,1)} %shard_map.154), channel_id=1, replica_groups=mesh['z'=16,'c'=2,'y'=4,'x'=4] {'y','x'}, dimensions={0} | all-to-all | bytes 4194304 | tf_op jit(solution)/shard_map/all_to_all | solution.py:309
  219.0 2.6 shard_map.155
  221.6 8.4 %all-to-all-start.3 = ((bf16[32,32,256]{2,1,0:T(8,128)(2,1)}), bf16[32,32,256]{2,1,0:T(8,128)(2,1)S(1)}, u32[]{:S(2)}, u32[]{:S(2)}) async-start(bf16[32,32,256]{2,1,0:T(8,128)(2,1)} %bitcast.11), calls=%async_computation.3 | async-start | bytes 1048576 | tf_op jit(solution)/shard_map/all_to_all | solution.py:309
  231.6 1.9 shard_map.152
  233.4 30.0 %all-to-all-done.3 = bf16[32,32,256]{2,1,0:T(8,128)(2,1)S(1)} async-done(((bf16[32,32,256]{2,1,0:T(8,128)(2,1)}), bf16[32,32,256]{2,1,0:T(8,128)(2,1)S(1)}, u32[]{:S(2)}, u32[]{:S(2)}) %all-to-all-start.3) | async-done | bytes 524320 | tf_op jit(solution)/shard_map/all_to_all | solution.py:309
  264.6 4.3 %shard_map.151 = bf16[512,256]{1,0:T(8,128)(2,1)} custom-call(bf16[16,512,256]{2,1,0:T(8,128)(2,1)} %bitcast.15, bf16[4096,256]{1,0:T(8,128)(2,1)} %w_ref.1), custom_call_target="tpu_custom_call" | custom-call | tf_op jit(solution)/shard_map/pallas_call | solution.py:44
  (30 shorter events, 3.6 us)
Async XLA Ops:
  7.2 88.3 %all-gather.5.cloned.1.call-start = ((), (), s32[]{:S(2)}) async-start(), calls=%async_computation.4 | async-start | bytes 2433024 | tf_op jit(solution)/shard_map/all_gather | solution.py:351
  11.7 87.8 %all-to-all-start = ((bf16[32,32,256]{2,1,0:T(8,128)(2,1)}), bf16[32,32,256]{2,1,0:T(8,128)(2,1)S(1)}, u32[]{:S(2)}, u32[]{:S(2)}) async-start(bf16[32,32,256]{2,1,0:T(8,128)(2,1)} %bitcast.5), calls=%async_computation | async-start | bytes 1048576 | tf_op jit(solution)/shard_map/all_to_all | solution.py:309
  28.5 236.1 %all-gather.7.cloned.1.call-start = ((), (), s32[]{:S(2)}) async-start(), calls=%async_computation.5 | async-start | bytes 4456448 | tf_op jit(solution)/shard_map/all_gather | solution.py:384
  101.2 6.8 %copy-start = (bf16[1,64,4096]{2,1,0:T(8,128)(2,1)S(1)}, bf16[1,64,4096]{2,1,0:T(8,128)(2,1)}, u32[]{:S(2)}) copy-start(bf16[1,64,4096]{2,1,0:T(8,128)(2,1)} %param.25) | copy-start | bytes 1572868
  101.2 11.3 %copy-start.1 = (bf16[1,64,4096]{2,1,0:T(8,128)(2,1)S(1)}, bf16[1,64,4096]{2,1,0:T(8,128)(2,1)}, u32[]{:S(2)}) copy-start(bf16[1,64,4096]{2,1,0:T(8,128)(2,1)} %param.26) | copy-start | bytes 1572868
  101.2 83.0 %all-to-all-start.1 = ((bf16[16,256,256]{2,1,0:T(8,128)(2,1)}), bf16[16,256,256]{2,1,0:T(8,128)(2,1)S(1)}, u32[]{:S(2)}, u32[]{:S(2)}) async-start(bf16[16,256,256]{2,1,0:T(8,128)(2,1)} %bitcast.14), calls=%async_computation.1 | async-start | bytes 4194304 | tf_op jit(solution)/shard_map/all_to_all | solution.py:309
  108.0 39.8 %collective-permute-start = (bf16[64,4096]{1,0:T(8,128)(2,1)S(1)}, bf16[64,4096]{1,0:T(8,128)(2,1)S(1)}, u32[]{:S(2)}, u32[]{:S(2)}) collective-permute-start(bf16[64,4096]{1,0:T(8,128)(2,1)S(1)} %bitcast.19), channel_id=1, source_target_pairs={{4,0},{8,4},{12,8},{0,12},{5,1},{9,5},{13,9},{1,13},{6,2},{10,6},{... | collective-permute-start | bytes 1572872 | tf_op jit(solution)/shard_map/ppermute | solution.py:305
  112.5 38.7 %collective-permute-start.4 = (bf16[64,4096]{1,0:T(8,128)(2,1)S(1)}, bf16[64,4096]{1,0:T(8,128)(2,1)S(1)}, u32[]{:S(2)}, u32[]{:S(2)}) collective-permute-start(bf16[64,4096]{1,0:T(8,128)(2,1)S(1)} %bitcast.22), channel_id=1, source_target_pairs={{12,0},{0,4},{4,8},{8,12},{13,1},{1,5},{5,9},{9,13},{14,2},{2,6},{... | collective-permute-start | bytes 1572872 | tf_op jit(solution)/shard_map/ppermute | solution.py:305
  114.4 47.3 %collective-permute-start.2 = (bf16[64,4096]{1,0:T(8,128)(2,1)S(1)}, bf16[64,4096]{1,0:T(8,128)(2,1)S(1)}, u32[]{:S(2)}, u32[]{:S(2)}) collective-permute-start(bf16[64,4096]{1,0:T(8,128)(2,1)S(1)} %bitcast.20), channel_id=1, source_target_pairs={{12,0},{0,4},{4,8},{8,12},{13,1},{1,5},{5,9},{9,13},{14,2},{2,6},{... | collective-permute-start | bytes 1572872 | tf_op jit(solution)/shard_map/ppermute | solution.py:305
  116.6 45.1 %collective-permute-start.3 = (bf16[64,4096]{1,0:T(8,128)(2,1)S(1)}, bf16[64,4096]{1,0:T(8,128)(2,1)S(1)}, u32[]{:S(2)}, u32[]{:S(2)}) collective-permute-start(bf16[64,4096]{1,0:T(8,128)(2,1)S(1)} %bitcast.23), channel_id=1, source_target_pairs={{4,0},{8,4},{12,8},{0,12},{5,1},{9,5},{13,9},{1,13},{6,2},{10,6},{... | collective-permute-start | bytes 1572872 | tf_op jit(solution)/shard_map/ppermute | solution.py:305
  147.8 33.9 %copy-start.2 = (bf16[64,4096]{1,0:T(8,128)(2,1)}, bf16[64,4096]{1,0:T(8,128)(2,1)S(1)}, u32[]{:S(2)}) copy-start(bf16[64,4096]{1,0:T(8,128)(2,1)S(1)} %collective-permute-done.g1_ref) | copy-start | bytes 1572868
  147.8 33.9 %collective-permute-start.1 = (bf16[64,4096]{1,0:T(8,128)(2,1)S(1)}, bf16[64,4096]{1,0:T(8,128)(2,1)S(1)}, u32[]{:S(2)}, u32[]{:S(2)}) collective-permute-start(bf16[64,4096]{1,0:T(8,128)(2,1)S(1)} %collective-permute-done.g1_ref), channel_id=1, source_target_pairs={{4,0},{8,4},{12,8},{0,12},{5,1},{9,5},{13,9},{1,13},{6,2},{10,6},{... | collective-permute-start | bytes 1572872 | tf_op jit(solution)/shard_map/ppermute | solution.py:305
  151.2 30.6 %copy-start.3 = (bf16[64,4096]{1,0:T(8,128)(2,1)}, bf16[64,4096]{1,0:T(8,128)(2,1)S(1)}, u32[]{:S(2)}) copy-start(bf16[64,4096]{1,0:T(8,128)(2,1)S(1)} %collective-permute-done.4.u3_ref) | copy-start | bytes 1572868
  151.2 33.0 %collective-permute-start.5 = (bf16[64,4096]{1,0:T(8,128)(2,1)S(1)}, bf16[64,4096]{1,0:T(8,128)(2,1)}, u32[]{:S(2)}, u32[]{:S(2)}) collective-permute-start(bf16[64,4096]{1,0:T(8,128)(2,1)S(1)} %collective-permute-done.4.u3_ref), channel_id=1, source_target_pairs={{12,0},{0,4},{4,8},{8,12},{13,1},{1,5},{5,9},{9,13},{14,2},{2,6},{... | collective-permute-start | bytes 1572872 | tf_op jit(solution)/shard_map/ppermute | solution.py:305
  161.7 20.0 %copy-start.4 = (bf16[64,4096]{1,0:T(8,128)(2,1)}, bf16[64,4096]{1,0:T(8,128)(2,1)S(1)}, u32[]{:S(2)}) copy-start(bf16[64,4096]{1,0:T(8,128)(2,1)S(1)} %collective-permute-done.2.g3_ref) | copy-start | bytes 1572868
  161.7 20.0 %copy-start.5 = (bf16[64,4096]{1,0:T(8,128)(2,1)}, bf16[64,4096]{1,0:T(8,128)(2,1)S(1)}, u32[]{:S(2)}) copy-start(bf16[64,4096]{1,0:T(8,128)(2,1)S(1)} %collective-permute-done.3.u1_ref) | copy-start | bytes 1572868
  181.8 0.8 copy-start.6
  219.0 11.0 %copy-start.7 = (s32[256,2]{0,1:T(2,128)S(1)}, s32[256,2]{0,1:T(2,128)}, u32[]{:S(2)}) copy-start(s32[256,2]{0,1:T(2,128)} %param.23) | copy-start | bytes 6148
  219.0 11.8 %copy-start.8 = (f32[256,2]{0,1:T(2,128)S(1)}, f32[256,2]{0,1:T(2,128)}, u32[]{:S(2)}) copy-start(f32[256,2]{0,1:T(2,128)} %param.24) | copy-start | bytes 6148
  221.6 41.9 %all-to-all-start.3 = ((bf16[32,32,256]{2,1,0:T(8,128)(2,1)}), bf16[32,32,256]{2,1,0:T(8,128)(2,1)S(1)}, u32[]{:S(2)}, u32[]{:S(2)}) async-start(bf16[32,32,256]{2,1,0:T(8,128)(2,1)} %bitcast.11), calls=%async_computation.3 | async-start | bytes 1048576 | tf_op jit(solution)/shard_map/all_to_all | solution.py:309
Sparse Core Ops, SparseCore 0:
  10.7 84.7 all-gather.4
  99.7 89.8 all-gather.6

commit v4 on v3

--- a/solution.py
+++ b/solution.py
@@ -83,14 +83,18 @@
     )
     normal = jnp.sum(weighted, axis=0, keepdims=True)
     width = out_ref.shape[1]
-    normal = jnp.concatenate([normal] * (width // dk), axis=1)
-    pack(
-        out_ref,
-        memory,
-        normal,
+    out_ref[0:dk, :] = memory
+    rows = [
+        jnp.concatenate([normal] * (width // dk), axis=1),
         jnp.broadcast_to(total, (1, width)),
         jnp.broadcast_to(top, (1, width)),
-    )
+        jnp.zeros((out_ref.shape[0] - dk - 3, width), F32),
+    ]
+    out_ref[dk:, :] = jnp.concatenate(rows, axis=0)
+
+
+def parts_of(x, dk):
+    return x[0:dk, :], x[dk : dk + 1, :], x[dk + 1 : dk + 2, :], x[dk + 2 : dk + 3, :]
 
 
 def fold(first, second):
@@ -143,18 +147,31 @@
     )
 
 
+def chip_kernel(at_ref, mine_ref, other_ref, out_ref):
+    first_here = at_ref[1] == 0
+    mine, other = mine_ref[...], other_ref[...]
+    first = parts_of(jnp.where(first_here, mine, other), 128)
+    second = parts_of(jnp.where(first_here, other, mine), 128)
+    pack(out_ref, *fold(first, second))
+
+
 def output_kernel(
-    at_ref, q_ref, k_ref, v_ref, in_ref, forget_ref, gate_ref, gain_ref, all_ref, out_ref
+    at_ref, q_ref, k_ref, v_ref, in_ref, forget_ref, gate_ref, gain_ref, all_ref, other_ref,
+    out_ref,
 ):
     n, dk = q_ref.shape
     scale = dk ** (-0.5)
     column, row = cumulative_forms(forget_ref[...])
-    memory, normal, _, top_before = lax.fori_loop(
+    before = lax.fori_loop(
         0,
         at_ref[0],
         lambda k, state: fold(state, unpack(all_ref[k], dk)),
         first_state(dk, all_ref.shape[2]),
     )
+    joined = fold(before, parts_of(other_ref[...], dk))
+    memory, normal, _, top_before = [
+        jnp.where(at_ref[1] == 0, alone, both) for alone, both in zip(before, joined)
+    ]
     normal = normal[:, :dk]
     top_before = top_before[:, 0:1]
     log_in = in_ref[...]
@@ -260,7 +277,7 @@
     @pl.when(step == pl.num_programs(0) - 1)
     def _():
         total = jnp.sum(squares[...], axis=1, keepdims=True)
-        inverse = lax.rsqrt(total * (1.0 / (columns * out_ref.shape[0])) + EPSILON)
+        inverse = lax.rsqrt(total * (1.0 / (columns * x_ref.shape[0])) + EPSILON)
         gate = gate_acc[...] * inverse
         hidden = gate * (1.0 / (1.0 + jnp.exp(-gate))) * (up_acc[...] * inverse)
         hidden = hidden.astype(BF16)
@@ -268,16 +285,17 @@
             out_ref[copy] = hidden
 
 
-def down_kernel(h_ref, w_ref, out_ref):
+def down_kernel(at_ref, h_ref, w0_ref, w1_ref, w2_ref, w3_ref, out_ref):
     part = h_ref.shape[2] // 4
-    rows = h_ref.shape[1]
-    for ys in range(4):
-        total = jnp.zeros((rows, w_ref.shape[1]), F32)
+    y = at_ref[2]
+    hidden = jnp.concatenate([h_ref[xs] for xs in range(4)], axis=1)
+    for k, w_ref in enumerate((w0_ref, w1_ref, w2_ref, w3_ref)):
+        weight = []
         for xs in range(4):
-            at = [(((ys + j) % 4) * 4 + xs) * part for j in range(4)]
-            weight = jnp.concatenate([w_ref[a : a + part, :] for a in at], axis=0)
-            total = total + dot(h_ref[ys * 4 + xs], weight)
-        out_ref[ys * rows : (ys + 1) * rows, :] = total.astype(BF16)
+            for j in range(4):
+                start = (lax.rem(y + j, 4) * 4 + xs) * part
+                weight.append(w_ref[pl.ds(pl.multiple_of(start, part), part), :])
+        out_ref[lax.rem(y + k, 4)] = dot(hidden, jnp.concatenate(weight, axis=0)).astype(BF16)
 
 
 def mix_kernel(h_ref, w_ref, out_ref, acc):
@@ -333,7 +351,7 @@
     gate_local, up_local, down_local = gate_weight[0], up_weight[0], down_weight[0]
     width = gate_local.shape[0]
     slots = ep * 32
-    at = lax.axis_index(EP).astype(jnp.int32)[None]
+    at = jnp.stack([lax.axis_index(axis) for axis in ("z", "c", "y")]).astype(jnp.int32)
 
     table = call(dispatch_kernel, pltpu.VMEM((slots, columns), BF16), (routes.T, expert_input))
     arrived = exchange(table.reshape(ep, 32, columns), EP)
@@ -345,17 +363,25 @@
     up_1 = from_next(up_local, "y", 1)
     gate_2 = from_next(gate_1, "y", 1)
     up_2 = from_next(up_3, "y", 3)
+    down_far = []
+    for k in (1, 3, 2):
+        down_far.append(from_next(down_local, "y", k))
+    down_1, down_3, down_2 = down_far
+
     mine = call(
-        summary_kernel, sds((dk + 16, dv), BF16), (key_rows, value_rows, in_gate, forget_gate)
-    )
-    states = lax.all_gather(mine, EP, axis=0)
+        summary_kernel, sds((dk + 8, dv), F32), (key_rows, value_rows, in_gate, forget_gate)
+    )
+    other = lax.ppermute(mine, "c", [(0, 1), (1, 0)])
+    chip = call(chip_kernel, sds((dk + 16, dv), BF16), (at, mine, other), near=(2,))
+    states = lax.all_gather(chip, "z", axis=0)
     heads = call(
         output_kernel,
         sds((rows_a, dv), BF16),
         (
             at, query_rows, key_rows, value_rows, in_gate, forget_gate, out_gate,
-            head_gain[None, :], states,
+            head_gain[None, :], states, other,
         ),
+        near=(9,),
     )
 
     sent = jnp.broadcast_to(arrived, (4, 4, slots // 4, columns)).reshape(tp, slots // 4, columns)
@@ -365,7 +391,7 @@
     weights_spec = lambda r: pl.BlockSpec((r, per * columns), lambda i: (0, i))
     hidden = call(
         hidden_kernel,
-        sds((tp, slots // 4, 4 * width), BF16),
+        sds((4, slots // 4, 4 * width), BF16),
         (rows, gate_local, gate_1, gate_2, gate_3, up_local, up_1, up_2, up_3),
         scratch=[pltpu.VMEM((slots // 4, 4 * width), F32)] * 2
         + [pltpu.VMEM((slots // 4, columns), F32)],
@@ -377,8 +403,14 @@
         out_specs=pl.BlockSpec(memory_space=pltpu.VMEM),
         near=(0,),
     )
-    gathered = exchange(hidden, TP)
-    results = call(down_kernel, pltpu.VMEM((slots, columns), BF16), (gathered, down_local), near=(0,))
+    gathered = exchange(hidden, "x")
+    results = call(
+        down_kernel,
+        pltpu.VMEM((4, slots // 4, columns), BF16),
+        (at, gathered, down_local, down_1, down_2, down_3),
+        near=(1,),
+    )
+    results = exchange(results, "y")
     back = exchange(results.reshape(ep, 32, columns), EP).reshape(slots, columns)
 
     all_heads = lax.all_gather(heads, TP, axis=0)

time: 276 us -> 313 us (1.13)
  blocking collectives: 30 us -> 62.6 us
  starting transfers between devices: 50.2 us -> 65.2 us
  waiting for transfers between devices: 154 us -> 143 us
    all_to_all x1 -> x2, blocking collectives: 30 us -> 62.6 us  [exchange(): return lax.all_to_all(x, axis, split_axis=0, concat_axis=0, tiled=True)]
    ppermute x6 -> x9, starting transfers between devices: 18.2 us -> 27.8 us  [from_next(): return lax.ppermute(x, axis, [((i + k) % n, i) for i in range(n)])]
    ppermute x0 -> x1, starting transfers between devices: none -> 8.73 us  [body(): other = lax.ppermute(mine, 'c', [(0, 1), (1, 0)])]
    all_gather x1, waiting for transfers between devices: 67 us -> 59.5 us  [body(): states = lax.all_gather(chip, 'z', axis=0)]
    ppermute x6 -> x9, waiting for transfers between devices: 57.1 us -> 53.1 us  [from_next(): return lax.ppermute(x, axis, [((i + k) % n, i) for i in range(n)])]
    all_to_all x3, starting transfers between devices: 31.9 us -> 28.6 us  [exchange(): return lax.all_to_all(x, axis, split_axis=0, concat_axis=0, tiled=True)]
    pallas_call x8 -> x9, Pallas kernels: 23.2 us -> 22.6 us  [call(): pl.pallas_call(kernel, out_shape=out, in_specs=in_specs, out_specs=out_sp...]
  transfers between devices with their start and end apart: 11 -> 15, of which waited for: 6 -> 10; matrix products, arithmetic and copies ran while one was open for 1% -> 1% of each run, Pallas kernels for 6% -> 4%
where the time goes in v4:
time: 313 us
  waiting for transfers between devices  143 us (46%)
  starting transfers between devices  65.2 us (21%)
  blocking collectives  62.6 us (20%)
  Pallas kernels  22.6 us (7%)
  between operations  14.2 us (5%)
  local copies, waits for them, and re-layouts  4.01 us (1%)
    all_to_all x2, blocking collectives, exchange(): return lax.all_to_all(x, axis, split_axis=0, concat_axis=0, tiled=True)  62.6 us
    all_gather x1, waiting for transfers between devices, body(): states = lax.all_gather(chip, 'z', axis=0)  59.5 us
    ppermute x9, waiting for transfers between devices, from_next(): return lax.ppermute(x, axis, [((i + k) % n, i) for i in range(n)])  53.1 us
    all_to_all x3, waiting for transfers between devices, exchange(): return lax.all_to_all(x, axis, split_axis=0, concat_axis=0, tiled=True)  30.1 us
    all_to_all x3, starting transfers between devices, exchange(): return lax.all_to_all(x, axis, split_axis=0, concat_axis=0, tiled=True)  28.6 us
    ppermute x9, starting transfers between devices, from_next(): return lax.ppermute(x, axis, [((i + k) % n, i) for i in range(n)])  27.8 us
    pallas_call x9, Pallas kernels, call(): pl.pallas_call(kernel, out_shape=out, in_specs=in_specs, out_specs=out_sp...  22.6 us
    ppermute x1, starting transfers between devices, body(): other = lax.ppermute(mine, 'c', [(0, 1), (1, 0)])  8.73 us
  transfers between devices with their start and end apart: 15, of which 10 were waited for; matrix products, arithmetic and copies ran while one was open for 1% of the time, Pallas kernels for 4%

profile of v4, /device:TPU:1, one launch (start us, length us, event | category | flops | bytes accessed | tf_op | source)
XLA Modules:
  0.0 312.5 jit_solution(4478882319986115614)
XLA Ops:
  7.2 2.1 shard_map.149.mine_ref
  9.3 8.7 %collective-permute-start = (f32[136,256]{1,0:T(8,128)}, f32[136,256]{1,0:T(8,128)S(1)}, u32[]{:S(2)}, u32[]{:S(2)}) collective-permute-start(f32[136,256]{1,0:T(8,128)} %shard_map.149.mine_ref), channel_id=1, source_target_pairs={{0,16},{16,0},{1,17},{17,1},{2,18},{18,2},{3,19},{19,3},{4,20},{20... | collective-permute-start | bytes 417800 | tf_op jit(solution)/shard_map/ppermute | solution.py:374
  21.0 59.5 %all-gather.5.cloned.1.call-done = bf16[2304,256]{1,0:T(8,128)(2,1)} async-done(((bf16[144,256]{1,0:T(8,128)(2,1)}), bf16[2304,256]{1,0:T(8,128)(2,1)}) %all-gather.5.cloned.1.call-update) | async-done | bytes 1179664 | tf_op jit(solution)/shard_map/all_gather | solution.py:376
  80.5 3.6 %shard_map.151 = bf16[512,256]{1,0:T(8,128)(2,1)} custom-call(s32[3]{0:T(128)} %pad_add_fusion.at_ref, bf16[512,128]{1,0:T(8,128)(2,1)} %q_ref.1, bf16[512,128]{1,0:T(8,128)(2,1)} %k_ref.3, bf16[512,256]{1,0:T(8,128)(2,1)} %v_ref.3, f32[1,512]{1,0:T(1,128)} %in_ref.3, f32[1,512]{1,0:T(1,128)} %forget_ref.3, bf16[512,256]{1,0:T(8,128)(2,1)} %gate_ref.1, ...), custom_call_target="tpu_custom_call" | custom-call | tf_op jit(solution)/shard_map/pallas_call | solution.py:44
  85.7 52.5 %all_to_all.25 = bf16[32,32,256]{2,1,0:T(8,128)(2,1)S(1)} all-to-all(bf16[32,32,256]{2,1,0:T(8,128)(2,1)S(1)} %bitcast.15), channel_id=1, replica_groups=mesh['z'=16,'c'=2,'y'=4,'x'=4] {'z','c'}, dimensions={0} | all-to-all | bytes 1048576 | tf_op jit(solution)/shard_map/all_to_all | solution.py:327
  139.8 6.7 %all-to-all-start.1 = ((bf16[16,256,256]{2,1,0:T(8,128)(2,1)}), bf16[16,256,256]{2,1,0:T(8,128)(2,1)S(1)}, u32[]{:S(2)}, u32[]{:S(2)}) async-start(bf16[16,256,256]{2,1,0:T(8,128)(2,1)} %bitcast.17), calls=%async_computation.1 | async-start | bytes 4194304 | tf_op jit(solution)/shard_map/all_to_all | solution.py:327
  146.5 4.5 %collective-permute-start.1 = (bf16[64,4096]{1,0:T(8,128)(2,1)}, bf16[64,4096]{1,0:T(8,128)(2,1)S(1)}, u32[]{:S(2)}, u32[]{:S(2)}) collective-permute-start(bf16[64,4096]{1,0:T(8,128)(2,1)} %bitcast.10.g0_ref), channel_id=1, source_target_pairs={{4,0},{8,4},{12,8},{0,12},{5,1},{9,5},{13,9},{1,13},{6,2},{10,6},{... | collective-permute-start | bytes 1572872 | tf_op jit(solution)/shard_map/ppermute | solution.py:323
  152.9 2.1 collective-permute-start.3
  155.1 4.3 %collective-permute-start.4 = (bf16[64,4096]{1,0:T(8,128)(2,1)}, bf16[64,4096]{1,0:T(8,128)(2,1)S(1)}, u32[]{:S(2)}, u32[]{:S(2)}) collective-permute-start(bf16[64,4096]{1,0:T(8,128)(2,1)} %bitcast.11.u0_ref), channel_id=1, source_target_pairs={{4,0},{8,4},{12,8},{0,12},{5,1},{9,5},{13,9},{1,13},{6,2},{10,6},{... | collective-permute-start | bytes 1572872 | tf_op jit(solution)/shard_map/ppermute | solution.py:323
  159.4 30.9 %collective-permute-done.1.g1_ref = bf16[64,4096]{1,0:T(8,128)(2,1)S(1)} collective-permute-done((bf16[64,4096]{1,0:T(8,128)(2,1)}, bf16[64,4096]{1,0:T(8,128)(2,1)S(1)}, u32[]{:S(2)}, u32[]{:S(2)}) %collective-permute-start.1) | collective-permute-done | bytes 524320 | tf_op jit(solution)/shard_map/ppermute | solution.py:323
  190.4 3.5 %collective-permute-start.2 = (bf16[64,4096]{1,0:T(8,128)(2,1)S(1)}, bf16[64,4096]{1,0:T(8,128)(2,1)S(1)}, u32[]{:S(2)}, u32[]{:S(2)}) collective-permute-start(bf16[64,4096]{1,0:T(8,128)(2,1)S(1)} %collective-permute-done.1.g1_ref), channel_id=1, source_target_pairs={{4,0},{8,4},{12,8},{0,12},{5,1},{9,5},{13,9},{1,13},{6,2},{10,6},{... | collective-permute-start | bytes 1572872 | tf_op jit(solution)/shard_map/ppermute | solution.py:323
  195.8 4.6 %collective-permute-start.7 = (bf16[1024,256]{1,0:T(8,128)(2,1)S(1)}, bf16[1024,256]{1,0:T(8,128)(2,1)S(1)}, u32[]{:S(2)}, u32[]{:S(2)}) collective-permute-start(bf16[1024,256]{1,0:T(8,128)(2,1)S(1)} %bitcast.22), channel_id=1, source_target_pairs={{4,0},{8,4},{12,8},{0,12},{5,1},{9,5},{13,9},{1,13},{6,2},{10,6},{... | collective-permute-start | bytes 1572872 | tf_op jit(solution)/shard_map/ppermute | solution.py:323
  200.4 2.5 collective-permute-done.3.g3_ref
  202.8 2.4 collective-permute-start.8
  205.3 2.5 collective-permute-start.9
  207.8 5.1 %collective-permute-done.2.g2_ref = bf16[64,4096]{1,0:T(8,128)(2,1)S(1)} collective-permute-done((bf16[64,4096]{1,0:T(8,128)(2,1)S(1)}, bf16[64,4096]{1,0:T(8,128)(2,1)S(1)}, u32[]{:S(2)}, u32[]{:S(2)}) %collective-permute-start.2) | collective-permute-done | bytes 524320 | tf_op jit(solution)/shard_map/ppermute | solution.py:323
  214.2 4.2 %shard_map.155 = bf16[4,256,256]{2,1,0:T(8,128)(2,1)} custom-call(bf16[16,256,256]{2,1,0:T(8,128)(2,1)S(1)} %all-to-all-done.1.x_ref, bf16[64,4096]{1,0:T(8,128)(2,1)} %bitcast.10.g0_ref, bf16[64,4096]{1,0:T(8,128)(2,1)} %copy-done.2, bf16[64,4096]{1,0:T(8,128)(2,1)} %copy-done.6, bf16[64,4096]{1,0:T(8,128)(2,1)} %copy-done.4, ...), custom_call_target="tpu_custom_call" | custom-call | tf_op jit(solution)/shard_map/pallas_call | solution.py:44
  218.4 4.1 %all-to-all-start.2 = ((bf16[4,256,256]{2,1,0:T(8,128)(2,1)}), bf16[4,256,256]{2,1,0:T(8,128)(2,1)S(1)}, u32[]{:S(2)}, u32[]{:S(2)}) async-start(bf16[4,256,256]{2,1,0:T(8,128)(2,1)} %shard_map.155), calls=%async_computation.2 | async-start | bytes 1048576 | tf_op jit(solution)/shard_map/all_to_all | solution.py:327
  225.7 10.9 %collective-permute-done.9.w3_ref = bf16[1024,256]{1,0:T(8,128)(2,1)} collective-permute-done((bf16[1024,256]{1,0:T(8,128)(2,1)S(1)}, bf16[1024,256]{1,0:T(8,128)(2,1)}, u32[]{:S(2)}, u32[]{:S(2)}) %collective-permute-start.9) | collective-permute-done | bytes 524320 | tf_op jit(solution)/shard_map/ppermute | solution.py:323
  236.7 2.2 shard_map.156
  238.9 10.0 %all_to_all.26 = bf16[4,256,256]{2,1,0:T(8,128)(2,1)} all-to-all(bf16[4,256,256]{2,1,0:T(8,128)(2,1)S(1)} %shard_map.156), channel_id=1, replica_groups=mesh['z'=16,'c'=2,'y'=4,'x'=4] {'y'}, dimensions={0} | all-to-all | bytes 1048576 | tf_op jit(solution)/shard_map/all_to_all | solution.py:327
  248.9 17.8 %all-to-all-start.4 = ((bf16[32,32,256]{2,1,0:T(8,128)(2,1)}), bf16[32,32,256]{2,1,0:T(8,128)(2,1)S(1)}, u32[]{:S(2)}, u32[]{:S(2)}) async-start(bf16[32,32,256]{2,1,0:T(8,128)(2,1)} %bitcast.13), calls=%async_computation.4 | async-start | bytes 1048576 | tf_op jit(solution)/shard_map/all_to_all | solution.py:327
  270.2 30.0 %all-to-all-done.4 = bf16[32,32,256]{2,1,0:T(8,128)(2,1)S(1)} async-done(((bf16[32,32,256]{2,1,0:T(8,128)(2,1)}), bf16[32,32,256]{2,1,0:T(8,128)(2,1)S(1)}, u32[]{:S(2)}, u32[]{:S(2)}) %all-to-all-start.4) | async-done | bytes 524320 | tf_op jit(solution)/shard_map/all_to_all | solution.py:327
  301.4 4.3 %shard_map.152 = bf16[512,256]{1,0:T(8,128)(2,1)} custom-call(bf16[16,512,256]{2,1,0:T(8,128)(2,1)} %bitcast.18, bf16[4096,256]{1,0:T(8,128)(2,1)} %w_ref.1), custom_call_target="tpu_custom_call" | custom-call | tf_op jit(solution)/shard_map/pallas_call | solution.py:44
  (41 shorter events, 19.0 us)
Async XLA Ops:
  7.2 73.3 %all-gather.5.cloned.1.call-start = ((), (), s32[]{:S(2)}) async-start(), calls=%async_computation.5 | async-start | bytes 1253376 | tf_op jit(solution)/shard_map/all_gather | solution.py:376
  9.3 9.9 %collective-permute-start = (f32[136,256]{1,0:T(8,128)}, f32[136,256]{1,0:T(8,128)S(1)}, u32[]{:S(2)}, u32[]{:S(2)}) collective-permute-start(f32[136,256]{1,0:T(8,128)} %shard_map.149.mine_ref), channel_id=1, source_target_pairs={{0,16},{16,0},{1,17},{17,1},{2,18},{18,2},{3,19},{19,3},{4,20},{20... | collective-permute-start | bytes 417800 | tf_op jit(solution)/shard_map/ppermute | solution.py:374
  20.9 280.5 %all-gather.7.cloned.1.call-start = ((), (), s32[]{:S(2)}) async-start(), calls=%async_computation.6 | async-start | bytes 4456448 | tf_op jit(solution)/shard_map/all_gather | solution.py:416
  139.8 55.9 %copy-start = (bf16[1,1024,256]{2,1,0:T(8,128)(2,1)S(1)}, bf16[1,1024,256]{2,1,0:T(8,128)(2,1)}, u32[]{:S(2)}) copy-start(bf16[1,1024,256]{2,1,0:T(8,128)(2,1)} %param.27) | copy-start | bytes 1572868
  139.8 74.3 %all-to-all-start.1 = ((bf16[16,256,256]{2,1,0:T(8,128)(2,1)}), bf16[16,256,256]{2,1,0:T(8,128)(2,1)S(1)}, u32[]{:S(2)}, u32[]{:S(2)}) async-start(bf16[16,256,256]{2,1,0:T(8,128)(2,1)} %bitcast.17), calls=%async_computation.1 | async-start | bytes 4194304 | tf_op jit(solution)/shard_map/all_to_all | solution.py:327
  146.5 43.8 %collective-permute-start.1 = (bf16[64,4096]{1,0:T(8,128)(2,1)}, bf16[64,4096]{1,0:T(8,128)(2,1)S(1)}, u32[]{:S(2)}, u32[]{:S(2)}) collective-permute-start(bf16[64,4096]{1,0:T(8,128)(2,1)} %bitcast.10.g0_ref), channel_id=1, source_target_pairs={{4,0},{8,4},{12,8},{0,12},{5,1},{9,5},{13,9},{1,13},{6,2},{10,6},{... | collective-permute-start | bytes 1572872 | tf_op jit(solution)/shard_map/ppermute | solution.py:323
  151.0 42.8 %collective-permute-start.5 = (bf16[64,4096]{1,0:T(8,128)(2,1)}, bf16[64,4096]{1,0:T(8,128)(2,1)S(1)}, u32[]{:S(2)}, u32[]{:S(2)}) collective-permute-start(bf16[64,4096]{1,0:T(8,128)(2,1)} %bitcast.11.u0_ref), channel_id=1, source_target_pairs={{12,0},{0,4},{4,8},{8,12},{13,1},{1,5},{5,9},{9,13},{14,2},{2,6},{... | collective-permute-start | bytes 1572872 | tf_op jit(solution)/shard_map/ppermute | solution.py:323
  152.9 49.9 %collective-permute-start.3 = (bf16[64,4096]{1,0:T(8,128)(2,1)}, bf16[64,4096]{1,0:T(8,128)(2,1)S(1)}, u32[]{:S(2)}, u32[]{:S(2)}) collective-permute-start(bf16[64,4096]{1,0:T(8,128)(2,1)} %bitcast.10.g0_ref), channel_id=1, source_target_pairs={{12,0},{0,4},{4,8},{8,12},{13,1},{1,5},{5,9},{9,13},{14,2},{2,6},{... | collective-permute-start | bytes 1572872 | tf_op jit(solution)/shard_map/ppermute | solution.py:323
  155.1 50.2 %collective-permute-start.4 = (bf16[64,4096]{1,0:T(8,128)(2,1)}, bf16[64,4096]{1,0:T(8,128)(2,1)S(1)}, u32[]{:S(2)}, u32[]{:S(2)}) collective-permute-start(bf16[64,4096]{1,0:T(8,128)(2,1)} %bitcast.11.u0_ref), channel_id=1, source_target_pairs={{4,0},{8,4},{12,8},{0,12},{5,1},{9,5},{13,9},{1,13},{6,2},{10,6},{... | collective-permute-start | bytes 1572872 | tf_op jit(solution)/shard_map/ppermute | solution.py:323
  190.4 22.6 %copy-start.2 = (bf16[64,4096]{1,0:T(8,128)(2,1)}, bf16[64,4096]{1,0:T(8,128)(2,1)S(1)}, u32[]{:S(2)}) copy-start(bf16[64,4096]{1,0:T(8,128)(2,1)S(1)} %collective-permute-done.1.g1_ref) | copy-start | bytes 1572868
  190.4 22.6 %collective-permute-start.2 = (bf16[64,4096]{1,0:T(8,128)(2,1)S(1)}, bf16[64,4096]{1,0:T(8,128)(2,1)S(1)}, u32[]{:S(2)}, u32[]{:S(2)}) collective-permute-start(bf16[64,4096]{1,0:T(8,128)(2,1)S(1)} %collective-permute-done.1.g1_ref), channel_id=1, source_target_pairs={{4,0},{8,4},{12,8},{0,12},{5,1},{9,5},{13,9},{1,13},{6,2},{10,6},{... | collective-permute-start | bytes 1572872 | tf_op jit(solution)/shard_map/ppermute | solution.py:323
  193.8 19.1 %copy-start.3 = (bf16[64,4096]{1,0:T(8,128)(2,1)}, bf16[64,4096]{1,0:T(8,128)(2,1)S(1)}, u32[]{:S(2)}) copy-start(bf16[64,4096]{1,0:T(8,128)(2,1)S(1)} %collective-permute-done.5.u3_ref) | copy-start | bytes 1572868
  193.9 20.3 %collective-permute-start.6 = (bf16[64,4096]{1,0:T(8,128)(2,1)S(1)}, bf16[64,4096]{1,0:T(8,128)(2,1)}, u32[]{:S(2)}, u32[]{:S(2)}) collective-permute-start(bf16[64,4096]{1,0:T(8,128)(2,1)S(1)} %collective-permute-done.5.u3_ref), channel_id=1, source_target_pairs={{12,0},{0,4},{4,8},{8,12},{13,1},{1,5},{5,9},{9,13},{14,2},{2,6},{... | collective-permute-start | bytes 1572872 | tf_op jit(solution)/shard_map/ppermute | solution.py:323
  195.8 28.4 %collective-permute-start.7 = (bf16[1024,256]{1,0:T(8,128)(2,1)S(1)}, bf16[1024,256]{1,0:T(8,128)(2,1)S(1)}, u32[]{:S(2)}, u32[]{:S(2)}) collective-permute-start(bf16[1024,256]{1,0:T(8,128)(2,1)S(1)} %bitcast.22), channel_id=1, source_target_pairs={{4,0},{8,4},{12,8},{0,12},{5,1},{9,5},{13,9},{1,13},{6,2},{10,6},{... | collective-permute-start | bytes 1572872 | tf_op jit(solution)/shard_map/ppermute | solution.py:323
  202.8 10.1 %copy-start.4 = (bf16[64,4096]{1,0:T(8,128)(2,1)}, bf16[64,4096]{1,0:T(8,128)(2,1)S(1)}, u32[]{:S(2)}) copy-start(bf16[64,4096]{1,0:T(8,128)(2,1)S(1)} %collective-permute-done.3.g3_ref) | copy-start | bytes 1572868
  202.8 22.9 %collective-permute-start.8 = (bf16[1024,256]{1,0:T(8,128)(2,1)S(1)}, bf16[1024,256]{1,0:T(8,128)(2,1)}, u32[]{:S(2)}, u32[]{:S(2)}) collective-permute-start(bf16[1024,256]{1,0:T(8,128)(2,1)S(1)} %bitcast.23), channel_id=1, source_target_pairs={{8,0},{12,4},{0,8},{4,12},{9,1},{13,5},{1,9},{5,13},{10,2},{14,6},... | collective-permute-start | bytes 1572872 | tf_op jit(solution)/shard_map/ppermute | solution.py:323
  205.3 7.7 %copy-start.5 = (bf16[64,4096]{1,0:T(8,128)(2,1)}, bf16[64,4096]{1,0:T(8,128)(2,1)S(1)}, u32[]{:S(2)}) copy-start(bf16[64,4096]{1,0:T(8,128)(2,1)S(1)} %collective-permute-done.4.u1_ref) | copy-start | bytes 1572868
  205.3 31.4 %collective-permute-start.9 = (bf16[1024,256]{1,0:T(8,128)(2,1)S(1)}, bf16[1024,256]{1,0:T(8,128)(2,1)}, u32[]{:S(2)}, u32[]{:S(2)}) collective-permute-start(bf16[1024,256]{1,0:T(8,128)(2,1)S(1)} %bitcast.24), channel_id=1, source_target_pairs={{12,0},{0,4},{4,8},{8,12},{13,1},{1,5},{5,9},{9,13},{14,2},{2,6},{... | collective-permute-start | bytes 1572872 | tf_op jit(solution)/shard_map/ppermute | solution.py:323
  213.0 0.8 copy-start.6
  218.4 18.3 %all-to-all-start.2 = ((bf16[4,256,256]{2,1,0:T(8,128)(2,1)}), bf16[4,256,256]{2,1,0:T(8,128)(2,1)S(1)}, u32[]{:S(2)}, u32[]{:S(2)}) async-start(bf16[4,256,256]{2,1,0:T(8,128)(2,1)} %shard_map.155), calls=%async_computation.2 | async-start | bytes 1048576 | tf_op jit(solution)/shard_map/all_to_all | solution.py:327
  222.5 44.3 %copy-start.7 = (s32[256,2]{0,1:T(2,128)S(1)}, s32[256,2]{0,1:T(2,128)}, u32[]{:S(2)}) copy-start(s32[256,2]{0,1:T(2,128)} %param.23) | copy-start | bytes 6148
  222.5 45.1 %copy-start.8 = (f32[256,2]{0,1:T(2,128)S(1)}, f32[256,2]{0,1:T(2,128)}, u32[]{:S(2)}) copy-start(f32[256,2]{0,1:T(2,128)} %param.24) | copy-start | bytes 6148
  224.2 12.5 %copy-start.1 = (bf16[1024,256]{1,0:T(8,128)(2,1)}, bf16[1024,256]{1,0:T(8,128)(2,1)S(1)}, u32[]{:S(2)}) copy-start(bf16[1024,256]{1,0:T(8,128)(2,1)S(1)} %collective-permute-done.7.w1_ref) | copy-start | bytes 1572868
  248.9 51.4 %all-to-all-start.4 = ((bf16[32,32,256]{2,1,0:T(8,128)(2,1)}), bf16[32,32,256]{2,1,0:T(8,128)(2,1)S(1)}, u32[]{:S(2)}, u32[]{:S(2)}) async-start(bf16[32,32,256]{2,1,0:T(8,128)(2,1)} %bitcast.13), calls=%async_computation.4 | async-start | bytes 1048576 | tf_op jit(solution)/shard_map/all_to_all | solution.py:327
Sparse Core Ops, SparseCore 0:
  21.0 59.4 all-gather.4
  84.3 97.7 all-gather.6

commit v5 on v3

--- a/solution.py
+++ b/solution.py
@@ -260,7 +260,7 @@
     @pl.when(step == pl.num_programs(0) - 1)
     def _():
         total = jnp.sum(squares[...], axis=1, keepdims=True)
-        inverse = lax.rsqrt(total * (1.0 / (columns * out_ref.shape[0])) + EPSILON)
+        inverse = lax.rsqrt(total * (1.0 / (columns * x_ref.shape[0])) + EPSILON)
         gate = gate_acc[...] * inverse
         hidden = gate * (1.0 / (1.0 + jnp.exp(-gate))) * (up_acc[...] * inverse)
         hidden = hidden.astype(BF16)
@@ -268,16 +268,17 @@
             out_ref[copy] = hidden
 
 
-def down_kernel(h_ref, w_ref, out_ref):
+def down_kernel(at_ref, h_ref, w0_ref, w1_ref, w2_ref, w3_ref, out_ref):
     part = h_ref.shape[2] // 4
-    rows = h_ref.shape[1]
-    for ys in range(4):
-        total = jnp.zeros((rows, w_ref.shape[1]), F32)
+    y = at_ref[1]
+    hidden = jnp.concatenate([h_ref[xs] for xs in range(4)], axis=1)
+    for k, w_ref in enumerate((w0_ref, w1_ref, w2_ref, w3_ref)):
+        weight = []
         for xs in range(4):
-            at = [(((ys + j) % 4) * 4 + xs) * part for j in range(4)]
-            weight = jnp.concatenate([w_ref[a : a + part, :] for a in at], axis=0)
-            total = total + dot(h_ref[ys * 4 + xs], weight)
-        out_ref[ys * rows : (ys + 1) * rows, :] = total.astype(BF16)
+            for j in range(4):
+                start = (lax.rem(y + j, 4) * 4 + xs) * part
+                weight.append(w_ref[pl.ds(pl.multiple_of(start, part), part), :])
+        out_ref[lax.rem(y + k, 4)] = dot(hidden, jnp.concatenate(weight, axis=0)).astype(BF16)
 
 
 def mix_kernel(h_ref, w_ref, out_ref, acc):
@@ -333,8 +334,12 @@
     gate_local, up_local, down_local = gate_weight[0], up_weight[0], down_weight[0]
     width = gate_local.shape[0]
     slots = ep * 32
-    at = lax.axis_index(EP).astype(jnp.int32)[None]
-
+    at = jnp.stack([lax.axis_index(EP), lax.axis_index("y")]).astype(jnp.int32)
+
+    mine = call(
+        summary_kernel, sds((dk + 16, dv), BF16), (key_rows, value_rows, in_gate, forget_gate)
+    )
+    states = lax.all_gather(mine, EP, axis=0)
     table = call(dispatch_kernel, pltpu.VMEM((slots, columns), BF16), (routes.T, expert_input))
     arrived = exchange(table.reshape(ep, 32, columns), EP)
     arrived = arrived.reshape(4, 1, slots // 4, columns)
@@ -345,10 +350,11 @@
     up_1 = from_next(up_local, "y", 1)
     gate_2 = from_next(gate_1, "y", 1)
     up_2 = from_next(up_3, "y", 3)
-    mine = call(
-        summary_kernel, sds((dk + 16, dv), BF16), (key_rows, value_rows, in_gate, forget_gate)
-    )
-    states = lax.all_gather(mine, EP, axis=0)
+    down_far = []
+    for k in (1, 3, 2):
+        down_far.append(from_next(down_local, "y", k))
+    down_1, down_3, down_2 = down_far
+
     heads = call(
         output_kernel,
         sds((rows_a, dv), BF16),
@@ -365,7 +371,7 @@
     weights_spec = lambda r: pl.BlockSpec((r, per * columns), lambda i: (0, i))
     hidden = call(
         hidden_kernel,
-        sds((tp, slots // 4, 4 * width), BF16),
+        sds((4, slots // 4, 4 * width), BF16),
         (rows, gate_local, gate_1, gate_2, gate_3, up_local, up_1, up_2, up_3),
         scratch=[pltpu.VMEM((slots // 4, 4 * width), F32)] * 2
         + [pltpu.VMEM((slots // 4, columns), F32)],
@@ -377,8 +383,14 @@
         out_specs=pl.BlockSpec(memory_space=pltpu.VMEM),
         near=(0,),
     )
-    gathered = exchange(hidden, TP)
-    results = call(down_kernel, pltpu.VMEM((slots, columns), BF16), (gathered, down_local), near=(0,))
+    gathered = exchange(hidden, "x")
+    results = call(
+        down_kernel,
+        pltpu.VMEM((4, slots // 4, columns), BF16),
+        (at, gathered, down_local, down_1, down_2, down_3),
+        near=(1,),
+    )
+    results = exchange(results, "y")
     back = exchange(results.reshape(ep, 32, columns), EP).reshape(slots, columns)
 
     all_heads = lax.all_gather(heads, TP, axis=0)

time: 276 us -> 311 us (1.13)
  blocking collectives: 30 us -> 52.5 us
  waiting for transfers between devices: 154 us -> 161 us
  starting transfers between devices: 50.2 us -> 56.5 us
    all_to_all x1 -> x2, blocking collectives: 30 us -> 52.5 us  [exchange(): return lax.all_to_all(x, axis, split_axis=0, concat_axis=0, tiled=True)]
    all_gather x1, waiting for transfers between devices: 67 us -> 78.1 us  [body(): states = lax.all_gather(mine, EP, axis=0)]
    ppermute x6 -> x9, starting transfers between devices: 18.2 us -> 27.8 us  [from_next(): return lax.ppermute(x, axis, [((i + k) % n, i) for i in range(n)])]
    ppermute x6 -> x9, waiting for transfers between devices: 57.1 us -> 53.1 us  [from_next(): return lax.ppermute(x, axis, [((i + k) % n, i) for i in range(n)])]
    all_to_all x3, starting transfers between devices: 31.9 us -> 28.6 us  [exchange(): return lax.all_to_all(x, axis, split_axis=0, concat_axis=0, tiled=True)]
  transfers between devices with their start and end apart: 11 -> 14, of which waited for: 6 -> 9; matrix products, arithmetic and copies ran while one was open for 1% -> 1% of each run, Pallas kernels for 6% -> 4%
where the time goes in v5:
time: 311 us; the launch traced here: 310 us
  waiting for transfers between devices  161 us (52%)
  starting transfers between devices  56.5 us (18%)
  blocking collectives  52.5 us (17%)
  Pallas kernels  21.4 us (7%)
  between operations  14.2 us (5%)
  local copies, waits for them, and re-layouts  4.02 us (1%)
    all_gather x1, waiting for transfers between devices, body(): states = lax.all_gather(mine, EP, axis=0)  78.1 us
    ppermute x9, waiting for transfers between devices, from_next(): return lax.ppermute(x, axis, [((i + k) % n, i) for i in range(n)])  53.1 us
    all_to_all x2, blocking collectives, exchange(): return lax.all_to_all(x, axis, split_axis=0, concat_axis=0, tiled=True)  52.5 us
    all_to_all x3, waiting for transfers between devices, exchange(): return lax.all_to_all(x, axis, split_axis=0, concat_axis=0, tiled=True)  30 us
    all_to_all x3, starting transfers between devices, exchange(): return lax.all_to_all(x, axis, split_axis=0, concat_axis=0, tiled=True)  28.6 us
    ppermute x9, starting transfers between devices, from_next(): return lax.ppermute(x, axis, [((i + k) % n, i) for i in range(n)])  27.8 us
    pallas_call x8, Pallas kernels, call(): pl.pallas_call(kernel, out_shape=out, in_specs=in_specs, out_specs=out_sp...  21.4 us
  transfers between devices with their start and end apart: 14, of which 9 were waited for; matrix products, arithmetic and copies ran while one was open for 1% of the time, Pallas kernels for 4%

profile of v5, /device:TPU:1, one launch (start us, length us, event | category | flops | bytes accessed | tf_op | source)
XLA Modules:
  0.0 310.5 jit_solution(2303062449296784781)
XLA Ops:
  7.2 2.1 shard_map.149
  10.0 78.1 %all-gather.5.cloned.1.call-done = bf16[4608,256]{1,0:T(8,128)(2,1)} async-done(((bf16[144,256]{1,0:T(8,128)(2,1)}), bf16[4608,256]{1,0:T(8,128)(2,1)}) %all-gather.5.cloned.1.call-update) | async-done | bytes 2359312 | tf_op jit(solution)/shard_map/all_gather | solution.py:342
  88.1 4.1 %shard_map.150 = bf16[512,256]{1,0:T(8,128)(2,1)} custom-call(s32[2]{0:T(128)} %pad_add_fusion.at_ref, bf16[512,128]{1,0:T(8,128)(2,1)} %q_ref.1, bf16[512,128]{1,0:T(8,128)(2,1)} %k_ref.3, bf16[512,256]{1,0:T(8,128)(2,1)} %v_ref.3, f32[1,512]{1,0:T(1,128)} %in_ref.3, f32[1,512]{1,0:T(1,128)} %forget_ref.3, bf16[512,256]{1,0:T(8,128)(2,1)} %gate_ref.1, ...), custom_call_target="tpu_custom_call" | custom-call | tf_op jit(solution)/shard_map/pallas_call | solution.py:44
  93.8 42.4 %all_to_all.25 = bf16[32,32,256]{2,1,0:T(8,128)(2,1)S(1)} all-to-all(bf16[32,32,256]{2,1,0:T(8,128)(2,1)S(1)} %bitcast.14), channel_id=1, replica_groups=mesh['z'=16,'c'=2,'y'=4,'x'=4] {'z','c'}, dimensions={0} | all-to-all | bytes 1048576 | tf_op jit(solution)/shard_map/all_to_all | solution.py:310
  137.8 6.7 %all-to-all-start.1 = ((bf16[16,256,256]{2,1,0:T(8,128)(2,1)}), bf16[16,256,256]{2,1,0:T(8,128)(2,1)S(1)}, u32[]{:S(2)}, u32[]{:S(2)}) async-start(bf16[16,256,256]{2,1,0:T(8,128)(2,1)} %bitcast.16), calls=%async_computation.1 | async-start | bytes 4194304 | tf_op jit(solution)/shard_map/all_to_all | solution.py:310
  144.5 4.5 %collective-permute-start = (bf16[64,4096]{1,0:T(8,128)(2,1)}, bf16[64,4096]{1,0:T(8,128)(2,1)S(1)}, u32[]{:S(2)}, u32[]{:S(2)}) collective-permute-start(bf16[64,4096]{1,0:T(8,128)(2,1)} %bitcast.9.g0_ref), channel_id=1, source_target_pairs={{4,0},{8,4},{12,8},{0,12},{5,1},{9,5},{13,9},{1,13},{6,2},{10,6},{... | collective-permute-start | bytes 1572872 | tf_op jit(solution)/shard_map/ppermute | solution.py:306
  148.9 1.9 collective-permute-start.4
  150.9 2.1 collective-permute-start.2
  153.0 4.3 %collective-permute-start.3 = (bf16[64,4096]{1,0:T(8,128)(2,1)}, bf16[64,4096]{1,0:T(8,128)(2,1)S(1)}, u32[]{:S(2)}, u32[]{:S(2)}) collective-permute-start(bf16[64,4096]{1,0:T(8,128)(2,1)} %bitcast.10.u0_ref), channel_id=1, source_target_pairs={{4,0},{8,4},{12,8},{0,12},{5,1},{9,5},{13,9},{1,13},{6,2},{10,6},{... | collective-permute-start | bytes 1572872 | tf_op jit(solution)/shard_map/ppermute | solution.py:306
  157.4 30.9 %collective-permute-done.g1_ref = bf16[64,4096]{1,0:T(8,128)(2,1)S(1)} collective-permute-done((bf16[64,4096]{1,0:T(8,128)(2,1)}, bf16[64,4096]{1,0:T(8,128)(2,1)S(1)}, u32[]{:S(2)}, u32[]{:S(2)}) %collective-permute-start) | collective-permute-done | bytes 524320 | tf_op jit(solution)/shard_map/ppermute | solution.py:306
  188.3 3.5 %collective-permute-start.1 = (bf16[64,4096]{1,0:T(8,128)(2,1)S(1)}, bf16[64,4096]{1,0:T(8,128)(2,1)S(1)}, u32[]{:S(2)}, u32[]{:S(2)}) collective-permute-start(bf16[64,4096]{1,0:T(8,128)(2,1)S(1)} %collective-permute-done.g1_ref), channel_id=1, source_target_pairs={{4,0},{8,4},{12,8},{0,12},{5,1},{9,5},{13,9},{1,13},{6,2},{10,6},{... | collective-permute-start | bytes 1572872 | tf_op jit(solution)/shard_map/ppermute | solution.py:306
  193.8 4.6 %collective-permute-start.6 = (bf16[1024,256]{1,0:T(8,128)(2,1)S(1)}, bf16[1024,256]{1,0:T(8,128)(2,1)S(1)}, u32[]{:S(2)}, u32[]{:S(2)}) collective-permute-start(bf16[1024,256]{1,0:T(8,128)(2,1)S(1)} %bitcast.21), channel_id=1, source_target_pairs={{4,0},{8,4},{12,8},{0,12},{5,1},{9,5},{13,9},{1,13},{6,2},{10,6},{... | collective-permute-start | bytes 1572872 | tf_op jit(solution)/shard_map/ppermute | solution.py:306
  198.3 2.5 collective-permute-done.2.g3_ref
  200.8 2.4 collective-permute-start.7
  203.3 2.5 collective-permute-start.8
  205.8 5.1 %collective-permute-done.1.g2_ref = bf16[64,4096]{1,0:T(8,128)(2,1)S(1)} collective-permute-done((bf16[64,4096]{1,0:T(8,128)(2,1)S(1)}, bf16[64,4096]{1,0:T(8,128)(2,1)S(1)}, u32[]{:S(2)}, u32[]{:S(2)}) %collective-permute-start.1) | collective-permute-done | bytes 524320 | tf_op jit(solution)/shard_map/ppermute | solution.py:306
  212.1 4.2 %shard_map.154 = bf16[4,256,256]{2,1,0:T(8,128)(2,1)} custom-call(bf16[16,256,256]{2,1,0:T(8,128)(2,1)S(1)} %all-to-all-done.1.x_ref, bf16[64,4096]{1,0:T(8,128)(2,1)} %bitcast.9.g0_ref, bf16[64,4096]{1,0:T(8,128)(2,1)} %copy-done.2, bf16[64,4096]{1,0:T(8,128)(2,1)} %copy-done.6, bf16[64,4096]{1,0:T(8,128)(2,1)} %copy-done.4, ...), custom_call_target="tpu_custom_call" | custom-call | tf_op jit(solution)/shard_map/pallas_call | solution.py:44
  216.3 4.1 %all-to-all-start.2 = ((bf16[4,256,256]{2,1,0:T(8,128)(2,1)}), bf16[4,256,256]{2,1,0:T(8,128)(2,1)S(1)}, u32[]{:S(2)}, u32[]{:S(2)}) async-start(bf16[4,256,256]{2,1,0:T(8,128)(2,1)} %shard_map.154), calls=%async_computation.2 | async-start | bytes 1048576 | tf_op jit(solution)/shard_map/all_to_all | solution.py:310
  223.7 10.9 %collective-permute-done.8.w3_ref = bf16[1024,256]{1,0:T(8,128)(2,1)} collective-permute-done((bf16[1024,256]{1,0:T(8,128)(2,1)S(1)}, bf16[1024,256]{1,0:T(8,128)(2,1)}, u32[]{:S(2)}, u32[]{:S(2)}) %collective-permute-start.8) | collective-permute-done | bytes 524320 | tf_op jit(solution)/shard_map/ppermute | solution.py:306
  234.6 2.2 shard_map.155
  236.9 10.0 %all_to_all.26 = bf16[4,256,256]{2,1,0:T(8,128)(2,1)} all-to-all(bf16[4,256,256]{2,1,0:T(8,128)(2,1)S(1)} %shard_map.155), channel_id=1, replica_groups=mesh['z'=16,'c'=2,'y'=4,'x'=4] {'y'}, dimensions={0} | all-to-all | bytes 1048576 | tf_op jit(solution)/shard_map/all_to_all | solution.py:310
  246.9 17.8 %all-to-all-start.4 = ((bf16[32,32,256]{2,1,0:T(8,128)(2,1)}), bf16[32,32,256]{2,1,0:T(8,128)(2,1)S(1)}, u32[]{:S(2)}, u32[]{:S(2)}) async-start(bf16[32,32,256]{2,1,0:T(8,128)(2,1)} %bitcast.12), calls=%async_computation.4 | async-start | bytes 1048576 | tf_op jit(solution)/shard_map/all_to_all | solution.py:310
  268.2 30.0 %all-to-all-done.4 = bf16[32,32,256]{2,1,0:T(8,128)(2,1)S(1)} async-done(((bf16[32,32,256]{2,1,0:T(8,128)(2,1)}), bf16[32,32,256]{2,1,0:T(8,128)(2,1)S(1)}, u32[]{:S(2)}, u32[]{:S(2)}) %all-to-all-start.4) | async-done | bytes 524320 | tf_op jit(solution)/shard_map/all_to_all | solution.py:310
  299.3 4.3 %shard_map.151 = bf16[512,256]{1,0:T(8,128)(2,1)} custom-call(bf16[16,512,256]{2,1,0:T(8,128)(2,1)} %bitcast.17, bf16[4096,256]{1,0:T(8,128)(2,1)} %w_ref.1), custom_call_target="tpu_custom_call" | custom-call | tf_op jit(solution)/shard_map/pallas_call | solution.py:44
  (38 shorter events, 14.9 us)
Async XLA Ops:
  7.2 81.0 %all-gather.5.cloned.1.call-start = ((), (), s32[]{:S(2)}) async-start(), calls=%async_computation.5 | async-start | bytes 2433024 | tf_op jit(solution)/shard_map/all_gather | solution.py:342
  9.3 290.0 %all-gather.7.cloned.1.call-start = ((), (), s32[]{:S(2)}) async-start(), calls=%async_computation.6 | async-start | bytes 4456448 | tf_op jit(solution)/shard_map/all_gather | solution.py:396
  137.8 56.0 %copy-start = (bf16[1,1024,256]{2,1,0:T(8,128)(2,1)S(1)}, bf16[1,1024,256]{2,1,0:T(8,128)(2,1)}, u32[]{:S(2)}) copy-start(bf16[1,1024,256]{2,1,0:T(8,128)(2,1)} %param.27) | copy-start | bytes 1572868
  137.8 74.4 %all-to-all-start.1 = ((bf16[16,256,256]{2,1,0:T(8,128)(2,1)}), bf16[16,256,256]{2,1,0:T(8,128)(2,1)S(1)}, u32[]{:S(2)}, u32[]{:S(2)}) async-start(bf16[16,256,256]{2,1,0:T(8,128)(2,1)} %bitcast.16), calls=%async_computation.1 | async-start | bytes 4194304 | tf_op jit(solution)/shard_map/all_to_all | solution.py:310
  144.5 43.9 %collective-permute-start = (bf16[64,4096]{1,0:T(8,128)(2,1)}, bf16[64,4096]{1,0:T(8,128)(2,1)S(1)}, u32[]{:S(2)}, u32[]{:S(2)}) collective-permute-start(bf16[64,4096]{1,0:T(8,128)(2,1)} %bitcast.9.g0_ref), channel_id=1, source_target_pairs={{4,0},{8,4},{12,8},{0,12},{5,1},{9,5},{13,9},{1,13},{6,2},{10,6},{... | collective-permute-start | bytes 1572872 | tf_op jit(solution)/shard_map/ppermute | solution.py:306
  148.9 42.9 %collective-permute-start.4 = (bf16[64,4096]{1,0:T(8,128)(2,1)}, bf16[64,4096]{1,0:T(8,128)(2,1)S(1)}, u32[]{:S(2)}, u32[]{:S(2)}) collective-permute-start(bf16[64,4096]{1,0:T(8,128)(2,1)} %bitcast.10.u0_ref), channel_id=1, source_target_pairs={{12,0},{0,4},{4,8},{8,12},{13,1},{1,5},{5,9},{9,13},{14,2},{2,6},{... | collective-permute-start | bytes 1572872 | tf_op jit(solution)/shard_map/ppermute | solution.py:306
  150.9 49.9 %collective-permute-start.2 = (bf16[64,4096]{1,0:T(8,128)(2,1)}, bf16[64,4096]{1,0:T(8,128)(2,1)S(1)}, u32[]{:S(2)}, u32[]{:S(2)}) collective-permute-start(bf16[64,4096]{1,0:T(8,128)(2,1)} %bitcast.9.g0_ref), channel_id=1, source_target_pairs={{12,0},{0,4},{4,8},{8,12},{13,1},{1,5},{5,9},{9,13},{14,2},{2,6},{... | collective-permute-start | bytes 1572872 | tf_op jit(solution)/shard_map/ppermute | solution.py:306
  153.0 50.2 %collective-permute-start.3 = (bf16[64,4096]{1,0:T(8,128)(2,1)}, bf16[64,4096]{1,0:T(8,128)(2,1)S(1)}, u32[]{:S(2)}, u32[]{:S(2)}) collective-permute-start(bf16[64,4096]{1,0:T(8,128)(2,1)} %bitcast.10.u0_ref), channel_id=1, source_target_pairs={{4,0},{8,4},{12,8},{0,12},{5,1},{9,5},{13,9},{1,13},{6,2},{10,6},{... | collective-permute-start | bytes 1572872 | tf_op jit(solution)/shard_map/ppermute | solution.py:306
  188.3 22.6 %copy-start.2 = (bf16[64,4096]{1,0:T(8,128)(2,1)}, bf16[64,4096]{1,0:T(8,128)(2,1)S(1)}, u32[]{:S(2)}) copy-start(bf16[64,4096]{1,0:T(8,128)(2,1)S(1)} %collective-permute-done.g1_ref) | copy-start | bytes 1572868
  188.3 22.6 %collective-permute-start.1 = (bf16[64,4096]{1,0:T(8,128)(2,1)S(1)}, bf16[64,4096]{1,0:T(8,128)(2,1)S(1)}, u32[]{:S(2)}, u32[]{:S(2)}) collective-permute-start(bf16[64,4096]{1,0:T(8,128)(2,1)S(1)} %collective-permute-done.g1_ref), channel_id=1, source_target_pairs={{4,0},{8,4},{12,8},{0,12},{5,1},{9,5},{13,9},{1,13},{6,2},{10,6},{... | collective-permute-start | bytes 1572872 | tf_op jit(solution)/shard_map/ppermute | solution.py:306
  191.8 19.1 %copy-start.3 = (bf16[64,4096]{1,0:T(8,128)(2,1)}, bf16[64,4096]{1,0:T(8,128)(2,1)S(1)}, u32[]{:S(2)}) copy-start(bf16[64,4096]{1,0:T(8,128)(2,1)S(1)} %collective-permute-done.4.u3_ref) | copy-start | bytes 1572868
  191.8 20.3 %collective-permute-start.5 = (bf16[64,4096]{1,0:T(8,128)(2,1)S(1)}, bf16[64,4096]{1,0:T(8,128)(2,1)}, u32[]{:S(2)}, u32[]{:S(2)}) collective-permute-start(bf16[64,4096]{1,0:T(8,128)(2,1)S(1)} %collective-permute-done.4.u3_ref), channel_id=1, source_target_pairs={{12,0},{0,4},{4,8},{8,12},{13,1},{1,5},{5,9},{9,13},{14,2},{2,6},{... | collective-permute-start | bytes 1572872 | tf_op jit(solution)/shard_map/ppermute | solution.py:306
  193.8 28.4 %collective-permute-start.6 = (bf16[1024,256]{1,0:T(8,128)(2,1)S(1)}, bf16[1024,256]{1,0:T(8,128)(2,1)S(1)}, u32[]{:S(2)}, u32[]{:S(2)}) collective-permute-start(bf16[1024,256]{1,0:T(8,128)(2,1)S(1)} %bitcast.21), channel_id=1, source_target_pairs={{4,0},{8,4},{12,8},{0,12},{5,1},{9,5},{13,9},{1,13},{6,2},{10,6},{... | collective-permute-start | bytes 1572872 | tf_op jit(solution)/shard_map/ppermute | solution.py:306
  200.8 10.1 %copy-start.4 = (bf16[64,4096]{1,0:T(8,128)(2,1)}, bf16[64,4096]{1,0:T(8,128)(2,1)S(1)}, u32[]{:S(2)}) copy-start(bf16[64,4096]{1,0:T(8,128)(2,1)S(1)} %collective-permute-done.2.g3_ref) | copy-start | bytes 1572868
  200.8 22.9 %collective-permute-start.7 = (bf16[1024,256]{1,0:T(8,128)(2,1)S(1)}, bf16[1024,256]{1,0:T(8,128)(2,1)}, u32[]{:S(2)}, u32[]{:S(2)}) collective-permute-start(bf16[1024,256]{1,0:T(8,128)(2,1)S(1)} %bitcast.22), channel_id=1, source_target_pairs={{8,0},{12,4},{0,8},{4,12},{9,1},{13,5},{1,9},{5,13},{10,2},{14,6},... | collective-permute-start | bytes 1572872 | tf_op jit(solution)/shard_map/ppermute | solution.py:306
  203.2 7.7 %copy-start.5 = (bf16[64,4096]{1,0:T(8,128)(2,1)}, bf16[64,4096]{1,0:T(8,128)(2,1)S(1)}, u32[]{:S(2)}) copy-start(bf16[64,4096]{1,0:T(8,128)(2,1)S(1)} %collective-permute-done.3.u1_ref) | copy-start | bytes 1572868
  203.3 31.4 %collective-permute-start.8 = (bf16[1024,256]{1,0:T(8,128)(2,1)S(1)}, bf16[1024,256]{1,0:T(8,128)(2,1)}, u32[]{:S(2)}, u32[]{:S(2)}) collective-permute-start(bf16[1024,256]{1,0:T(8,128)(2,1)S(1)} %bitcast.23), channel_id=1, source_target_pairs={{12,0},{0,4},{4,8},{8,12},{13,1},{1,5},{5,9},{9,13},{14,2},{2,6},{... | collective-permute-start | bytes 1572872 | tf_op jit(solution)/shard_map/ppermute | solution.py:306
  210.9 0.8 copy-start.6
  216.3 18.3 %all-to-all-start.2 = ((bf16[4,256,256]{2,1,0:T(8,128)(2,1)}), bf16[4,256,256]{2,1,0:T(8,128)(2,1)S(1)}, u32[]{:S(2)}, u32[]{:S(2)}) async-start(bf16[4,256,256]{2,1,0:T(8,128)(2,1)} %shard_map.154), calls=%async_computation.2 | async-start | bytes 1048576 | tf_op jit(solution)/shard_map/all_to_all | solution.py:310
  220.4 44.3 %copy-start.7 = (s32[256,2]{0,1:T(2,128)S(1)}, s32[256,2]{0,1:T(2,128)}, u32[]{:S(2)}) copy-start(s32[256,2]{0,1:T(2,128)} %param.23) | copy-start | bytes 6148
  220.4 45.1 %copy-start.8 = (f32[256,2]{0,1:T(2,128)S(1)}, f32[256,2]{0,1:T(2,128)}, u32[]{:S(2)}) copy-start(f32[256,2]{0,1:T(2,128)} %param.24) | copy-start | bytes 6148
  222.1 12.5 %copy-start.1 = (bf16[1024,256]{1,0:T(8,128)(2,1)}, bf16[1024,256]{1,0:T(8,128)(2,1)S(1)}, u32[]{:S(2)}) copy-start(bf16[1024,256]{1,0:T(8,128)(2,1)S(1)} %collective-permute-done.6.w1_ref) | copy-start | bytes 1572868
  246.9 51.4 %all-to-all-start.4 = ((bf16[32,32,256]{2,1,0:T(8,128)(2,1)}), bf16[32,32,256]{2,1,0:T(8,128)(2,1)S(1)}, u32[]{:S(2)}, u32[]{:S(2)}) async-start(bf16[32,32,256]{2,1,0:T(8,128)(2,1)} %bitcast.12), calls=%async_computation.4 | async-start | bytes 1048576 | tf_op jit(solution)/shard_map/all_to_all | solution.py:310
Sparse Core Ops, SparseCore 0:
  10.7 77.4 all-gather.4
  92.3 87.6 all-gather.6

commit v6 on v5

--- a/solution.py
+++ b/solution.py
@@ -235,7 +235,8 @@
     step = pl.program_id(0)
     _, _, columns = x_ref.shape
     senders = g0_ref.shape[1] // columns
-    pieces = [x_ref[step * senders + i] for i in range(senders)]
+    order = [step * senders + i for i in range(senders)]
+    pieces = [x_ref[lax.rem(t, 4) * 4 + t // 4] for t in order]
     x = jnp.concatenate(pieces, axis=1)
     gate = jnp.concatenate([w[...] for w in (g0_ref, g1_ref, g2_ref, g3_ref)], axis=0)
     up = jnp.concatenate([w[...] for w in (u0_ref, u1_ref, u2_ref, u3_ref)], axis=0)
@@ -341,8 +342,8 @@
     )
     states = lax.all_gather(mine, EP, axis=0)
     table = call(dispatch_kernel, pltpu.VMEM((slots, columns), BF16), (routes.T, expert_input))
-    arrived = exchange(table.reshape(ep, 32, columns), EP)
-    arrived = arrived.reshape(4, 1, slots // 4, columns)
+    arrived = exchange(table.reshape(4 * ep, 8, columns), (*EP, "y"))
+    arrived = arrived.reshape(ep, 4, 8, columns).transpose(1, 0, 2, 3)
 
     gate_1 = from_next(gate_local, "y", 1)
     up_3 = from_next(up_local, "y", 3)
@@ -364,8 +365,8 @@
         ),
     )
 
-    sent = jnp.broadcast_to(arrived, (4, 4, slots // 4, columns)).reshape(tp, slots // 4, columns)
-    rows = exchange(sent, TP)
+    sent = jnp.broadcast_to(arrived.reshape(1, slots, columns), (4, slots, columns))
+    rows = exchange(sent, "x").reshape(tp, slots // 4, columns)
     grid = 2
     per = tp // grid
     weights_spec = lambda r: pl.BlockSpec((r, per * columns), lambda i: (0, i))
@@ -390,8 +391,8 @@
         (at, gathered, down_local, down_1, down_2, down_3),
         near=(1,),
     )
-    results = exchange(results, "y")
-    back = exchange(results.reshape(ep, 32, columns), EP).reshape(slots, columns)
+    results = results.reshape(4, ep, 8, columns).transpose(1, 0, 2, 3)
+    back = exchange(results.reshape(4 * ep, 8, columns), (*EP, "y")).reshape(slots, columns)
 
     all_heads = lax.all_gather(heads, TP, axis=0)
     steps = 2

time: 311 us -> 283 us (0.910)
  waiting for transfers between devices: 161 us -> 140 us
  blocking collectives: 52.5 us -> 46.2 us
    ppermute x9, waiting for transfers between devices: 53.1 us -> 31.2 us  [from_next(): return lax.ppermute(x, axis, [((i + k) % n, i) for i in range(n)])]
    all_to_all x2 -> x1, blocking collectives: 52.5 us -> 46.2 us  [exchange(): return lax.all_to_all(x, axis, split_axis=0, concat_axis=0, tiled=True)]
  transfers between devices with their start and end apart: 14 -> 14, of which waited for: 9 -> 8; matrix products, arithmetic and copies ran while one was open for 1% -> 2% of each run, Pallas kernels for 4% -> 4%
where the time goes in v6:
time: 283 us
  waiting for transfers between devices  140 us (49%)
  starting transfers between devices  55.9 us (20%)
  blocking collectives  46.2 us (16%)
  Pallas kernels  21.4 us (8%)
  between operations  14.2 us (5%)
  local copies, waits for them, and re-layouts  4.88 us (2%)
    all_gather x1, waiting for transfers between devices, body(): states = lax.all_gather(mine, EP, axis=0)  78.1 us
    all_to_all x1, blocking collectives, exchange(): return lax.all_to_all(x, axis, split_axis=0, concat_axis=0, tiled=True)  46.2 us
    ppermute x9, waiting for transfers between devices, from_next(): return lax.ppermute(x, axis, [((i + k) % n, i) for i in range(n)])  31.2 us
    all_to_all x3, waiting for transfers between devices, exchange(): return lax.all_to_all(x, axis, split_axis=0, concat_axis=0, tiled=True)  30.2 us
    all_to_all x3, starting transfers between devices, exchange(): return lax.all_to_all(x, axis, split_axis=0, concat_axis=0, tiled=True)  29.3 us
    ppermute x9, starting transfers between devices, from_next(): return lax.ppermute(x, axis, [((i + k) % n, i) for i in range(n)])  26.5 us
    pallas_call x8, Pallas kernels, call(): pl.pallas_call(kernel, out_shape=out, in_specs=in_specs, out_specs=out_sp...  21.4 us
  transfers between devices with their start and end apart: 14, of which 8 were waited for; matrix products, arithmetic and copies ran while one was open for 2% of the time, Pallas kernels for 4%

profile of v6, /device:TPU:1, one launch (start us, length us, event | category | flops | bytes accessed | tf_op | source)
XLA Modules:
  0.0 282.7 jit_solution(12939135370379951201)
XLA Ops:
  7.2 2.1 shard_map.149
  10.0 78.1 %all-gather.5.cloned.1.call-done = bf16[4608,256]{1,0:T(8,128)(2,1)} async-done(((bf16[144,256]{1,0:T(8,128)(2,1)}), bf16[4608,256]{1,0:T(8,128)(2,1)}) %all-gather.5.cloned.1.call-update) | async-done | bytes 2359312 | tf_op jit(solution)/shard_map/all_gather | solution.py:343
  88.1 4.1 %shard_map.150 = bf16[512,256]{1,0:T(8,128)(2,1)} custom-call(s32[2]{0:T(128)} %pad_add_fusion.at_ref, bf16[512,128]{1,0:T(8,128)(2,1)} %q_ref.1, bf16[512,128]{1,0:T(8,128)(2,1)} %k_ref.3, bf16[512,256]{1,0:T(8,128)(2,1)} %v_ref.3, f32[1,512]{1,0:T(1,128)} %in_ref.3, f32[1,512]{1,0:T(1,128)} %forget_ref.3, bf16[512,256]{1,0:T(8,128)(2,1)} %gate_ref.1, ...), custom_call_target="tpu_custom_call" | custom-call | tf_op jit(solution)/shard_map/pallas_call | solution.py:44
  93.8 46.2 %all_to_all.20 = bf16[128,8,256]{2,1,0:T(8,128)(2,1)S(1)} all-to-all(bf16[128,8,256]{2,1,0:T(8,128)(2,1)S(1)} %bitcast.21), channel_id=1, replica_groups=mesh['z'=16,'c'=2,'y'=4,'x'=4] {'z','c','y'}, dimensions={0} | all-to-all | bytes 1048576 | tf_op jit(solution)/shard_map/all_to_all | solution.py:311
  141.5 4.1 %all-to-all-start.1 = ((bf16[4,1024,256]{2,1,0:T(8,128)(2,1)}), bf16[4,1024,256]{2,1,0:T(8,128)(2,1)S(1)}, u32[]{:S(2)}, u32[]{:S(2)}) async-start(bf16[4,1024,256]{2,1,0:T(8,128)(2,1)} %broadcast_in_dim.12), calls=%async_computation.1 | async-start | bytes 4194304 | tf_op jit(solution)/shard_map/all_to_all | solution.py:311
  147.7 3.2 %collective-permute-start.4 = (bf16[64,4096]{1,0:T(8,128)(2,1)}, bf16[64,4096]{1,0:T(8,128)(2,1)S(1)}, u32[]{:S(2)}, u32[]{:S(2)}) collective-permute-start(bf16[64,4096]{1,0:T(8,128)(2,1)} %bitcast.12.u0_ref), channel_id=1, source_target_pairs={{12,0},{0,4},{4,8},{8,12},{13,1},{1,5},{5,9},{9,13},{14,2},{2,6},{... | collective-permute-start | bytes 1572872 | tf_op jit(solution)/shard_map/ppermute | solution.py:307
  150.9 3.1 %collective-permute-start.2 = (bf16[64,4096]{1,0:T(8,128)(2,1)}, bf16[64,4096]{1,0:T(8,128)(2,1)S(1)}, u32[]{:S(2)}, u32[]{:S(2)}) collective-permute-start(bf16[64,4096]{1,0:T(8,128)(2,1)} %bitcast.11.g0_ref), channel_id=1, source_target_pairs={{12,0},{0,4},{4,8},{8,12},{13,1},{1,5},{5,9},{9,13},{14,2},{2,6},{... | collective-permute-start | bytes 1572872 | tf_op jit(solution)/shard_map/ppermute | solution.py:307
  154.0 3.4 %collective-permute-start.3 = (bf16[64,4096]{1,0:T(8,128)(2,1)}, bf16[64,4096]{1,0:T(8,128)(2,1)S(1)}, u32[]{:S(2)}, u32[]{:S(2)}) collective-permute-start(bf16[64,4096]{1,0:T(8,128)(2,1)} %bitcast.12.u0_ref), channel_id=1, source_target_pairs={{4,0},{8,4},{12,8},{0,12},{5,1},{9,5},{13,9},{1,13},{6,2},{10,6},{... | collective-permute-start | bytes 1572872 | tf_op jit(solution)/shard_map/ppermute | solution.py:307
  157.4 9.7 %collective-permute-done.g1_ref = bf16[64,4096]{1,0:T(8,128)(2,1)S(1)} collective-permute-done((bf16[64,4096]{1,0:T(8,128)(2,1)}, bf16[64,4096]{1,0:T(8,128)(2,1)S(1)}, u32[]{:S(2)}, u32[]{:S(2)}) %collective-permute-start) | collective-permute-done | bytes 524320 | tf_op jit(solution)/shard_map/ppermute | solution.py:307
  167.2 2.4 collective-permute-start.1
  169.7 2.9 %collective-permute-start.5 = (bf16[64,4096]{1,0:T(8,128)(2,1)S(1)}, bf16[64,4096]{1,0:T(8,128)(2,1)}, u32[]{:S(2)}, u32[]{:S(2)}) collective-permute-start(bf16[64,4096]{1,0:T(8,128)(2,1)S(1)} %collective-permute-done.4.u3_ref), channel_id=1, source_target_pairs={{12,0},{0,4},{4,8},{8,12},{13,1},{1,5},{5,9},{9,13},{14,2},{2,6},{... | collective-permute-start | bytes 1572872 | tf_op jit(solution)/shard_map/ppermute | solution.py:307
  172.5 3.6 %collective-permute-start.6 = (bf16[1024,256]{1,0:T(8,128)(2,1)S(1)}, bf16[1024,256]{1,0:T(8,128)(2,1)S(1)}, u32[]{:S(2)}, u32[]{:S(2)}) collective-permute-start(bf16[1024,256]{1,0:T(8,128)(2,1)S(1)} %bitcast.29), channel_id=1, source_target_pairs={{4,0},{8,4},{12,8},{0,12},{5,1},{9,5},{13,9},{1,13},{6,2},{10,6},{... | collective-permute-start | bytes 1572872 | tf_op jit(solution)/shard_map/ppermute | solution.py:307
  176.2 2.4 collective-permute-done.2.g3_ref
  178.6 3.7 %collective-permute-start.7 = (bf16[1024,256]{1,0:T(8,128)(2,1)S(1)}, bf16[1024,256]{1,0:T(8,128)(2,1)}, u32[]{:S(2)}, u32[]{:S(2)}) collective-permute-start(bf16[1024,256]{1,0:T(8,128)(2,1)S(1)} %bitcast.30), channel_id=1, source_target_pairs={{8,0},{12,4},{0,8},{4,12},{9,1},{13,5},{1,9},{5,13},{10,2},{14,6},... | collective-permute-start | bytes 1572872 | tf_op jit(solution)/shard_map/ppermute | solution.py:307
  182.4 2.1 collective-permute-start.8
  184.4 5.3 %collective-permute-done.1.g2_ref = bf16[64,4096]{1,0:T(8,128)(2,1)S(1)} collective-permute-done((bf16[64,4096]{1,0:T(8,128)(2,1)S(1)}, bf16[64,4096]{1,0:T(8,128)(2,1)S(1)}, u32[]{:S(2)}, u32[]{:S(2)}) %collective-permute-start.1) | collective-permute-done | bytes 524320 | tf_op jit(solution)/shard_map/ppermute | solution.py:307
  190.6 4.2 %shard_map.154 = bf16[4,256,256]{2,1,0:T(8,128)(2,1)} custom-call(bf16[16,256,256]{2,1,0:T(8,128)(2,1)S(1)} %bitcast.20, bf16[64,4096]{1,0:T(8,128)(2,1)} %bitcast.11.g0_ref, bf16[64,4096]{1,0:T(8,128)(2,1)} %copy-done.2, bf16[64,4096]{1,0:T(8,128)(2,1)} %copy-done.6, bf16[64,4096]{1,0:T(8,128)(2,1)} %copy-done.4, bf16[64,4096]{1,0:T(8,128)(2,1)} %bitcast.12.u0_ref, ...), custom_call_target="tpu_custom_call" | custom-call | tf_op jit(solution)/shard_map/pallas_call | solution.py:44
  194.8 3.9 %all-to-all-start.2 = ((bf16[4,256,256]{2,1,0:T(8,128)(2,1)}), bf16[4,256,256]{2,1,0:T(8,128)(2,1)S(1)}, u32[]{:S(2)}, u32[]{:S(2)}) async-start(bf16[4,256,256]{2,1,0:T(8,128)(2,1)} %shard_map.154), calls=%async_computation.2 | async-start | bytes 1048576 | tf_op jit(solution)/shard_map/all_to_all | solution.py:311
  198.7 2.3 collective-permute-done.6.w1_ref
  202.3 10.1 %collective-permute-done.8.w3_ref = bf16[1024,256]{1,0:T(8,128)(2,1)} collective-permute-done((bf16[1024,256]{1,0:T(8,128)(2,1)S(1)}, bf16[1024,256]{1,0:T(8,128)(2,1)}, u32[]{:S(2)}, u32[]{:S(2)}) %collective-permute-start.8) | collective-permute-done | bytes 524320 | tf_op jit(solution)/shard_map/ppermute | solution.py:307
  212.4 2.2 shard_map.155
  215.5 21.3 %all-to-all-start.3 = ((bf16[128,8,256]{2,1,0:T(8,128)(2,1)}), bf16[128,8,256]{2,1,0:T(8,128)(2,1)S(1)}, u32[]{:S(2)}, u32[]{:S(2)}) async-start(bf16[128,8,256]{2,1,0:T(8,128)(2,1)} %bitcast.16), calls=%async_computation.3 | async-start | bytes 1048576 | tf_op jit(solution)/shard_map/all_to_all | solution.py:311
  240.3 30.2 %all-to-all-done.3 = bf16[128,8,256]{2,1,0:T(8,128)(2,1)S(1)} async-done(((bf16[128,8,256]{2,1,0:T(8,128)(2,1)}), bf16[128,8,256]{2,1,0:T(8,128)(2,1)S(1)}, u32[]{:S(2)}, u32[]{:S(2)}) %all-to-all-start.3) | async-done | bytes 524320 | tf_op jit(solution)/shard_map/all_to_all | solution.py:311
  271.6 4.3 %shard_map.151 = bf16[512,256]{1,0:T(8,128)(2,1)} custom-call(bf16[16,512,256]{2,1,0:T(8,128)(2,1)} %bitcast.24, bf16[4096,256]{1,0:T(8,128)(2,1)} %w_ref.1), custom_call_target="tpu_custom_call" | custom-call | tf_op jit(solution)/shard_map/pallas_call | solution.py:44
  (39 shorter events, 13.5 us)
Async XLA Ops:
  7.2 81.0 %all-gather.5.cloned.1.call-start = ((), (), s32[]{:S(2)}) async-start(), calls=%async_computation.4 | async-start | bytes 2433024 | tf_op jit(solution)/shard_map/all_gather | solution.py:343
  9.3 262.2 %all-gather.7.cloned.1.call-start = ((), (), s32[]{:S(2)}) async-start(), calls=%async_computation.5 | async-start | bytes 4456448 | tf_op jit(solution)/shard_map/all_gather | solution.py:397
  141.5 31.0 %copy-start = (bf16[1,1024,256]{2,1,0:T(8,128)(2,1)S(1)}, bf16[1,1024,256]{2,1,0:T(8,128)(2,1)}, u32[]{:S(2)}) copy-start(bf16[1,1024,256]{2,1,0:T(8,128)(2,1)} %param.27) | copy-start | bytes 1572868
  141.5 49.1 %all-to-all-start.1 = ((bf16[4,1024,256]{2,1,0:T(8,128)(2,1)}), bf16[4,1024,256]{2,1,0:T(8,128)(2,1)S(1)}, u32[]{:S(2)}, u32[]{:S(2)}) async-start(bf16[4,1024,256]{2,1,0:T(8,128)(2,1)} %broadcast_in_dim.12), calls=%async_computation.1 | async-start | bytes 4194304 | tf_op jit(solution)/shard_map/all_to_all | solution.py:311
  145.6 21.6 %collective-permute-start = (bf16[64,4096]{1,0:T(8,128)(2,1)}, bf16[64,4096]{1,0:T(8,128)(2,1)S(1)}, u32[]{:S(2)}, u32[]{:S(2)}) collective-permute-start(bf16[64,4096]{1,0:T(8,128)(2,1)} %bitcast.11.g0_ref), channel_id=1, source_target_pairs={{4,0},{8,4},{12,8},{0,12},{5,1},{9,5},{13,9},{1,13},{6,2},{10,6},{... | collective-permute-start | bytes 1572872 | tf_op jit(solution)/shard_map/ppermute | solution.py:307
  147.7 21.9 %collective-permute-start.4 = (bf16[64,4096]{1,0:T(8,128)(2,1)}, bf16[64,4096]{1,0:T(8,128)(2,1)S(1)}, u32[]{:S(2)}, u32[]{:S(2)}) collective-permute-start(bf16[64,4096]{1,0:T(8,128)(2,1)} %bitcast.12.u0_ref), channel_id=1, source_target_pairs={{12,0},{0,4},{4,8},{8,12},{13,1},{1,5},{5,9},{9,13},{14,2},{2,6},{... | collective-permute-start | bytes 1572872 | tf_op jit(solution)/shard_map/ppermute | solution.py:307
  150.9 27.7 %collective-permute-start.2 = (bf16[64,4096]{1,0:T(8,128)(2,1)}, bf16[64,4096]{1,0:T(8,128)(2,1)S(1)}, u32[]{:S(2)}, u32[]{:S(2)}) collective-permute-start(bf16[64,4096]{1,0:T(8,128)(2,1)} %bitcast.11.g0_ref), channel_id=1, source_target_pairs={{12,0},{0,4},{4,8},{8,12},{13,1},{1,5},{5,9},{9,13},{14,2},{2,6},{... | collective-permute-start | bytes 1572872 | tf_op jit(solution)/shard_map/ppermute | solution.py:307
  154.0 28.3 %collective-permute-start.3 = (bf16[64,4096]{1,0:T(8,128)(2,1)}, bf16[64,4096]{1,0:T(8,128)(2,1)S(1)}, u32[]{:S(2)}, u32[]{:S(2)}) collective-permute-start(bf16[64,4096]{1,0:T(8,128)(2,1)} %bitcast.12.u0_ref), channel_id=1, source_target_pairs={{4,0},{8,4},{12,8},{0,12},{5,1},{9,5},{13,9},{1,13},{6,2},{10,6},{... | collective-permute-start | bytes 1572872 | tf_op jit(solution)/shard_map/ppermute | solution.py:307
  167.2 22.6 %copy-start.2 = (bf16[64,4096]{1,0:T(8,128)(2,1)}, bf16[64,4096]{1,0:T(8,128)(2,1)S(1)}, u32[]{:S(2)}) copy-start(bf16[64,4096]{1,0:T(8,128)(2,1)S(1)} %collective-permute-done.g1_ref) | copy-start | bytes 1572868
  167.2 22.6 %collective-permute-start.1 = (bf16[64,4096]{1,0:T(8,128)(2,1)S(1)}, bf16[64,4096]{1,0:T(8,128)(2,1)S(1)}, u32[]{:S(2)}, u32[]{:S(2)}) collective-permute-start(bf16[64,4096]{1,0:T(8,128)(2,1)S(1)} %collective-permute-done.g1_ref), channel_id=1, source_target_pairs={{4,0},{8,4},{12,8},{0,12},{5,1},{9,5},{13,9},{1,13},{6,2},{10,6},{... | collective-permute-start | bytes 1572872 | tf_op jit(solution)/shard_map/ppermute | solution.py:307
  169.6 20.1 %copy-start.3 = (bf16[64,4096]{1,0:T(8,128)(2,1)}, bf16[64,4096]{1,0:T(8,128)(2,1)S(1)}, u32[]{:S(2)}) copy-start(bf16[64,4096]{1,0:T(8,128)(2,1)S(1)} %collective-permute-done.4.u3_ref) | copy-start | bytes 1572868
  169.7 21.0 %collective-permute-start.5 = (bf16[64,4096]{1,0:T(8,128)(2,1)S(1)}, bf16[64,4096]{1,0:T(8,128)(2,1)}, u32[]{:S(2)}, u32[]{:S(2)}) collective-permute-start(bf16[64,4096]{1,0:T(8,128)(2,1)S(1)} %collective-permute-done.4.u3_ref), channel_id=1, source_target_pairs={{12,0},{0,4},{4,8},{8,12},{13,1},{1,5},{5,9},{9,13},{14,2},{2,6},{... | collective-permute-start | bytes 1572872 | tf_op jit(solution)/shard_map/ppermute | solution.py:307
  172.5 28.5 %collective-permute-start.6 = (bf16[1024,256]{1,0:T(8,128)(2,1)S(1)}, bf16[1024,256]{1,0:T(8,128)(2,1)S(1)}, u32[]{:S(2)}, u32[]{:S(2)}) collective-permute-start(bf16[1024,256]{1,0:T(8,128)(2,1)S(1)} %bitcast.29), channel_id=1, source_target_pairs={{4,0},{8,4},{12,8},{0,12},{5,1},{9,5},{13,9},{1,13},{6,2},{10,6},{... | collective-permute-start | bytes 1572872 | tf_op jit(solution)/shard_map/ppermute | solution.py:307
  178.6 11.2 %copy-start.4 = (bf16[64,4096]{1,0:T(8,128)(2,1)}, bf16[64,4096]{1,0:T(8,128)(2,1)S(1)}, u32[]{:S(2)}) copy-start(bf16[64,4096]{1,0:T(8,128)(2,1)S(1)} %collective-permute-done.2.g3_ref) | copy-start | bytes 1572868
  178.6 23.7 %collective-permute-start.7 = (bf16[1024,256]{1,0:T(8,128)(2,1)S(1)}, bf16[1024,256]{1,0:T(8,128)(2,1)}, u32[]{:S(2)}, u32[]{:S(2)}) collective-permute-start(bf16[1024,256]{1,0:T(8,128)(2,1)S(1)} %bitcast.30), channel_id=1, source_target_pairs={{8,0},{12,4},{0,8},{4,12},{9,1},{13,5},{1,9},{5,13},{10,2},{14,6},... | collective-permute-start | bytes 1572872 | tf_op jit(solution)/shard_map/ppermute | solution.py:307
  182.3 7.4 %copy-start.5 = (bf16[64,4096]{1,0:T(8,128)(2,1)}, bf16[64,4096]{1,0:T(8,128)(2,1)S(1)}, u32[]{:S(2)}) copy-start(bf16[64,4096]{1,0:T(8,128)(2,1)S(1)} %collective-permute-done.3.u1_ref) | copy-start | bytes 1572868
  182.4 30.0 %collective-permute-start.8 = (bf16[1024,256]{1,0:T(8,128)(2,1)S(1)}, bf16[1024,256]{1,0:T(8,128)(2,1)}, u32[]{:S(2)}, u32[]{:S(2)}) collective-permute-start(bf16[1024,256]{1,0:T(8,128)(2,1)S(1)} %bitcast.31), channel_id=1, source_target_pairs={{12,0},{0,4},{4,8},{8,12},{13,1},{1,5},{5,9},{9,13},{14,2},{2,6},{... | collective-permute-start | bytes 1572872 | tf_op jit(solution)/shard_map/ppermute | solution.py:307
  189.8 0.8 copy-start.6
  194.8 17.6 %all-to-all-start.2 = ((bf16[4,256,256]{2,1,0:T(8,128)(2,1)}), bf16[4,256,256]{2,1,0:T(8,128)(2,1)S(1)}, u32[]{:S(2)}, u32[]{:S(2)}) async-start(bf16[4,256,256]{2,1,0:T(8,128)(2,1)} %shard_map.154), calls=%async_computation.2 | async-start | bytes 1048576 | tf_op jit(solution)/shard_map/all_to_all | solution.py:311
  198.7 38.1 %copy-start.7 = (s32[256,2]{0,1:T(2,128)S(1)}, s32[256,2]{0,1:T(2,128)}, u32[]{:S(2)}) copy-start(s32[256,2]{0,1:T(2,128)} %param.23) | copy-start | bytes 6148
  198.7 39.0 %copy-start.8 = (f32[256,2]{0,1:T(2,128)S(1)}, f32[256,2]{0,1:T(2,128)}, u32[]{:S(2)}) copy-start(f32[256,2]{0,1:T(2,128)} %param.24) | copy-start | bytes 6148
  201.0 11.4 %copy-start.1 = (bf16[1024,256]{1,0:T(8,128)(2,1)}, bf16[1024,256]{1,0:T(8,128)(2,1)S(1)}, u32[]{:S(2)}) copy-start(bf16[1024,256]{1,0:T(8,128)(2,1)S(1)} %collective-permute-done.6.w1_ref) | copy-start | bytes 1572868
  215.5 55.0 %all-to-all-start.3 = ((bf16[128,8,256]{2,1,0:T(8,128)(2,1)}), bf16[128,8,256]{2,1,0:T(8,128)(2,1)S(1)}, u32[]{:S(2)}, u32[]{:S(2)}) async-start(bf16[128,8,256]{2,1,0:T(8,128)(2,1)} %bitcast.16), calls=%async_computation.3 | async-start | bytes 1048576 | tf_op jit(solution)/shard_map/all_to_all | solution.py:311
Sparse Core Ops, SparseCore 0:
  10.7 77.4 all-gather.4
  92.3 71.3 all-gather.6

commit v7 on v6

--- a/solution.py
+++ b/solution.py
@@ -56,24 +56,39 @@
     return jnp.minimum(f, 0.0) - jnp.log1p(jnp.exp(-jnp.abs(f)))
 
 
+def as_column(row, keep):
+    n = row.shape[1]
+    chosen = keep(iota((n, n), 1), iota((n, n), 0))
+    return jnp.sum(jnp.where(chosen, jnp.broadcast_to(row, (n, n)), 0.0), axis=1, keepdims=True)
+
+
+def column_of(row):
+    pieces = [row[:, i : i + 128] for i in range(0, row.shape[1], 128)]
+    return jnp.concatenate([as_column(p, lambda lane, at: lane == at) for p in pieces], axis=0)
+
+
 def cumulative_forms(forget_row):
-    n = forget_row.shape[1]
-    logs = jnp.broadcast_to(log_sigmoid(forget_row), (n, n))
-    at_row, at_col = iota((n, n), 0), iota((n, n), 1)
-    column = jnp.sum(jnp.where(at_col <= at_row, logs, 0.0), axis=1, keepdims=True)
-    own = jnp.sum(jnp.where(at_col == at_row, logs, 0.0), axis=1, keepdims=True)
-    row = jnp.sum(jnp.where(at_row <= at_col, own, 0.0), axis=0, keepdims=True)
-    return column, row
+    logs = log_sigmoid(forget_row)
+    before = jnp.zeros((1, 1), F32)
+    columns, rows = [], []
+    for start in range(0, forget_row.shape[1], 128):
+        piece = logs[:, start : start + 128]
+        n = piece.shape[1]
+        column = as_column(piece, lambda lane, at: lane <= at)
+        own = as_column(piece, lambda lane, at: lane == at)
+        earlier = iota((n, n), 0) <= iota((n, n), 1)
+        row = jnp.sum(jnp.where(earlier, own, 0.0), axis=0, keepdims=True)
+        columns.append(column + before)
+        rows.append(row + before)
+        before = before + column[n - 1 :, :]
+    return jnp.concatenate(columns, axis=0), jnp.concatenate(rows, axis=1)
 
 
 def summary_kernel(k_ref, v_ref, in_ref, forget_ref, out_ref):
     n = k_ref.shape[0]
     dk = k_ref.shape[1]
     column, _ = cumulative_forms(forget_ref[...])
-    diagonal = iota((n, n), 0) == iota((n, n), 1)
-    log_in = jnp.sum(
-        jnp.where(diagonal, jnp.broadcast_to(in_ref[...], (n, n)), 0.0), axis=1, keepdims=True
-    )
+    log_in = column_of(in_ref[...])
     total = column[n - 1 :, :]
     weight_log = total - column + log_in
     top = jnp.max(weight_log, axis=0, keepdims=True)
@@ -93,20 +108,6 @@
     )
 
 
-def fold(first, second):
-    memory_1, normal_1, decay_1, max_1 = first
-    memory_2, normal_2, decay_2, max_2 = second
-    top = jnp.maximum(decay_2 + max_1, max_2)
-    keep_1 = jnp.exp(decay_2 + max_1 - top)
-    keep_2 = jnp.exp(max_2 - top)
-    return (
-        keep_1 * memory_1 + keep_2 * memory_2,
-        keep_1 * normal_1 + keep_2 * normal_2,
-        decay_1 + decay_2,
-        top,
-    )
-
-
 def split3(x):
     high = x.astype(BF16)
     rest = x - high.astype(F32)
@@ -125,22 +126,28 @@
     out_ref[dk:, :] = jnp.concatenate(rows, axis=0).astype(BF16)
 
 
-def unpack(item, dk):
-    item = item.astype(F32)
-    rows = [
-        item[dk + i : dk + i + 1] + item[dk + i + 1 : dk + i + 2] + item[dk + i + 2 : dk + i + 3]
-        for i in (0, 3, 6)
-    ]
-    return (item[0:dk], *rows)
-
-
-def first_state(dk, width):
-    return (
-        jnp.zeros((dk, width), F32),
-        jnp.zeros((1, width), F32),
-        jnp.zeros((1, width), F32),
-        jnp.full((1, width), LOG_FLOOR, F32),
-    )
+def earlier_state(all_ref, here, dk):
+    count, _, width = all_ref.shape
+    decay = jnp.zeros((1, width), F32)
+    logs, normals = [], []
+    for k in reversed(range(count)):
+        lines = all_ref[k, dk : dk + 16, :].astype(F32)
+        normal, own_decay, top = [
+            lines[i : i + 1] + lines[i + 1 : i + 2] + lines[i + 2 : i + 3] for i in (0, 3, 6)
+        ]
+        logs.append(jnp.where(k < here, top + decay, MASKED))
+        normals.append(normal)
+        decay = decay + jnp.where(k < here, own_decay, 0.0)
+    top = jnp.full((1, width), LOG_FLOOR, F32)
+    for log in logs:
+        top = jnp.maximum(top, log)
+    memory = jnp.zeros((dk, width), F32)
+    normal = jnp.zeros((1, width), F32)
+    for k, log, own in zip(reversed(range(count)), logs, normals):
+        weight = jnp.exp(log - top)
+        memory = memory + weight * all_ref[k, 0:dk, :].astype(F32)
+        normal = normal + weight * own
+    return memory, normal, top
 
 
 def output_kernel(
@@ -149,12 +156,7 @@
     n, dk = q_ref.shape
     scale = dk ** (-0.5)
     column, row = cumulative_forms(forget_ref[...])
-    memory, normal, _, top_before = lax.fori_loop(
-        0,
-        at_ref[0],
-        lambda k, state: fold(state, unpack(all_ref[k], dk)),
-        first_state(dk, all_ref.shape[2]),
-    )
+    memory, normal, top_before = earlier_state(all_ref, at_ref[0], dk)
     normal = normal[:, :dk]
     top_before = top_before[:, 0:1]
     log_in = in_ref[...]

time: 283 us -> 284 us (level)
  no operation moved by 1% of the time
where the time goes in v7:
time: 284 us; the launch traced here: 283 us
  waiting for transfers between devices  139 us (49%)
  starting transfers between devices  55.9 us (20%)
  blocking collectives  45.6 us (16%)
  Pallas kernels  22.2 us (8%)
  between operations  14.2 us (5%)
  local copies, waits for them, and re-layouts  4.88 us (2%)
    all_gather x1, waiting for transfers between devices, body(): states = lax.all_gather(mine, EP, axis=0)  78 us
    all_to_all x1, blocking collectives, exchange(): return lax.all_to_all(x, axis, split_axis=0, concat_axis=0, tiled=True)  45.6 us
    ppermute x9, waiting for transfers between devices, from_next(): return lax.ppermute(x, axis, [((i + k) % n, i) for i in range(n)])  31.2 us
    all_to_all x3, waiting for transfers between devices, exchange(): return lax.all_to_all(x, axis, split_axis=0, concat_axis=0, tiled=True)  30.2 us
    all_to_all x3, starting transfers between devices, exchange(): return lax.all_to_all(x, axis, split_axis=0, concat_axis=0, tiled=True)  29.3 us
    ppermute x9, starting transfers between devices, from_next(): return lax.ppermute(x, axis, [((i + k) % n, i) for i in range(n)])  26.5 us
    pallas_call x8, Pallas kernels, call(): pl.pallas_call(kernel, out_shape=out, in_specs=in_specs, out_specs=out_sp...  22.2 us
  transfers between devices with their start and end apart: 14, of which 8 were waited for; matrix products, arithmetic and copies ran while one was open for 2% of the time, Pallas kernels for 4%

profile of v7, /device:TPU:1, one launch (start us, length us, event | category | flops | bytes accessed | tf_op | source)
XLA Modules:
  0.0 282.8 jit_solution(4270631178890536711)
XLA Ops:
  7.2 2.2 shard_map.149
  10.1 78.0 %all-gather.5.cloned.1.call-done = bf16[4608,256]{1,0:T(8,128)(2,1)} async-done(((bf16[144,256]{1,0:T(8,128)(2,1)}), bf16[4608,256]{1,0:T(8,128)(2,1)}) %all-gather.5.cloned.1.call-update) | async-done | bytes 2359312 | tf_op jit(solution)/shard_map/all_gather | solution.py:345
  88.1 4.8 %shard_map.150 = bf16[512,256]{1,0:T(8,128)(2,1)} custom-call(s32[2]{0:T(128)} %pad_add_fusion.at_ref, bf16[512,128]{1,0:T(8,128)(2,1)} %q_ref.1, bf16[512,128]{1,0:T(8,128)(2,1)} %k_ref.3, bf16[512,256]{1,0:T(8,128)(2,1)} %v_ref.3, f32[1,512]{1,0:T(1,128)} %in_ref.3, f32[1,512]{1,0:T(1,128)} %forget_ref.3, bf16[512,256]{1,0:T(8,128)(2,1)} %gate_ref.1, ...), custom_call_target="tpu_custom_call" | custom-call | tf_op jit(solution)/shard_map/pallas_call | solution.py:44
  94.5 45.6 %all_to_all.20 = bf16[128,8,256]{2,1,0:T(8,128)(2,1)S(1)} all-to-all(bf16[128,8,256]{2,1,0:T(8,128)(2,1)S(1)} %bitcast.21), channel_id=1, replica_groups=mesh['z'=16,'c'=2,'y'=4,'x'=4] {'z','c','y'}, dimensions={0} | all-to-all | bytes 1048576 | tf_op jit(solution)/shard_map/all_to_all | solution.py:313
  141.6 4.1 %all-to-all-start.1 = ((bf16[4,1024,256]{2,1,0:T(8,128)(2,1)}), bf16[4,1024,256]{2,1,0:T(8,128)(2,1)S(1)}, u32[]{:S(2)}, u32[]{:S(2)}) async-start(bf16[4,1024,256]{2,1,0:T(8,128)(2,1)} %broadcast_in_dim.12), calls=%async_computation.1 | async-start | bytes 4194304 | tf_op jit(solution)/shard_map/all_to_all | solution.py:313
  147.8 3.2 %collective-permute-start.4 = (bf16[64,4096]{1,0:T(8,128)(2,1)}, bf16[64,4096]{1,0:T(8,128)(2,1)S(1)}, u32[]{:S(2)}, u32[]{:S(2)}) collective-permute-start(bf16[64,4096]{1,0:T(8,128)(2,1)} %bitcast.12.u0_ref), channel_id=1, source_target_pairs={{12,0},{0,4},{4,8},{8,12},{13,1},{1,5},{5,9},{9,13},{14,2},{2,6},{... | collective-permute-start | bytes 1572872 | tf_op jit(solution)/shard_map/ppermute | solution.py:309
  151.0 3.1 %collective-permute-start.2 = (bf16[64,4096]{1,0:T(8,128)(2,1)}, bf16[64,4096]{1,0:T(8,128)(2,1)S(1)}, u32[]{:S(2)}, u32[]{:S(2)}) collective-permute-start(bf16[64,4096]{1,0:T(8,128)(2,1)} %bitcast.11.g0_ref), channel_id=1, source_target_pairs={{12,0},{0,4},{4,8},{8,12},{13,1},{1,5},{5,9},{9,13},{14,2},{2,6},{... | collective-permute-start | bytes 1572872 | tf_op jit(solution)/shard_map/ppermute | solution.py:309
  154.1 3.4 %collective-permute-start.3 = (bf16[64,4096]{1,0:T(8,128)(2,1)}, bf16[64,4096]{1,0:T(8,128)(2,1)S(1)}, u32[]{:S(2)}, u32[]{:S(2)}) collective-permute-start(bf16[64,4096]{1,0:T(8,128)(2,1)} %bitcast.12.u0_ref), channel_id=1, source_target_pairs={{4,0},{8,4},{12,8},{0,12},{5,1},{9,5},{13,9},{1,13},{6,2},{10,6},{... | collective-permute-start | bytes 1572872 | tf_op jit(solution)/shard_map/ppermute | solution.py:309
  157.5 9.7 %collective-permute-done.g1_ref = bf16[64,4096]{1,0:T(8,128)(2,1)S(1)} collective-permute-done((bf16[64,4096]{1,0:T(8,128)(2,1)}, bf16[64,4096]{1,0:T(8,128)(2,1)S(1)}, u32[]{:S(2)}, u32[]{:S(2)}) %collective-permute-start) | collective-permute-done | bytes 524320 | tf_op jit(solution)/shard_map/ppermute | solution.py:309
  167.3 2.4 collective-permute-start.1
  169.7 2.9 %collective-permute-start.5 = (bf16[64,4096]{1,0:T(8,128)(2,1)S(1)}, bf16[64,4096]{1,0:T(8,128)(2,1)}, u32[]{:S(2)}, u32[]{:S(2)}) collective-permute-start(bf16[64,4096]{1,0:T(8,128)(2,1)S(1)} %collective-permute-done.4.u3_ref), channel_id=1, source_target_pairs={{12,0},{0,4},{4,8},{8,12},{13,1},{1,5},{5,9},{9,13},{14,2},{2,6},{... | collective-permute-start | bytes 1572872 | tf_op jit(solution)/shard_map/ppermute | solution.py:309
  172.6 3.6 %collective-permute-start.6 = (bf16[1024,256]{1,0:T(8,128)(2,1)S(1)}, bf16[1024,256]{1,0:T(8,128)(2,1)S(1)}, u32[]{:S(2)}, u32[]{:S(2)}) collective-permute-start(bf16[1024,256]{1,0:T(8,128)(2,1)S(1)} %bitcast.29), channel_id=1, source_target_pairs={{4,0},{8,4},{12,8},{0,12},{5,1},{9,5},{13,9},{1,13},{6,2},{10,6},{... | collective-permute-start | bytes 1572872 | tf_op jit(solution)/shard_map/ppermute | solution.py:309
  176.3 2.4 collective-permute-done.2.g3_ref
  178.7 3.7 %collective-permute-start.7 = (bf16[1024,256]{1,0:T(8,128)(2,1)S(1)}, bf16[1024,256]{1,0:T(8,128)(2,1)}, u32[]{:S(2)}, u32[]{:S(2)}) collective-permute-start(bf16[1024,256]{1,0:T(8,128)(2,1)S(1)} %bitcast.30), channel_id=1, source_target_pairs={{8,0},{12,4},{0,8},{4,12},{9,1},{13,5},{1,9},{5,13},{10,2},{14,6},... | collective-permute-start | bytes 1572872 | tf_op jit(solution)/shard_map/ppermute | solution.py:309
  182.4 2.1 collective-permute-start.8
  184.5 5.3 %collective-permute-done.1.g2_ref = bf16[64,4096]{1,0:T(8,128)(2,1)S(1)} collective-permute-done((bf16[64,4096]{1,0:T(8,128)(2,1)S(1)}, bf16[64,4096]{1,0:T(8,128)(2,1)S(1)}, u32[]{:S(2)}, u32[]{:S(2)}) %collective-permute-start.1) | collective-permute-done | bytes 524320 | tf_op jit(solution)/shard_map/ppermute | solution.py:309
  190.7 4.2 %shard_map.154 = bf16[4,256,256]{2,1,0:T(8,128)(2,1)} custom-call(bf16[16,256,256]{2,1,0:T(8,128)(2,1)S(1)} %bitcast.20, bf16[64,4096]{1,0:T(8,128)(2,1)} %bitcast.11.g0_ref, bf16[64,4096]{1,0:T(8,128)(2,1)} %copy-done.2, bf16[64,4096]{1,0:T(8,128)(2,1)} %copy-done.6, bf16[64,4096]{1,0:T(8,128)(2,1)} %copy-done.4, bf16[64,4096]{1,0:T(8,128)(2,1)} %bitcast.12.u0_ref, ...), custom_call_target="tpu_custom_call" | custom-call | tf_op jit(solution)/shard_map/pallas_call | solution.py:44
  194.9 3.9 %all-to-all-start.2 = ((bf16[4,256,256]{2,1,0:T(8,128)(2,1)}), bf16[4,256,256]{2,1,0:T(8,128)(2,1)S(1)}, u32[]{:S(2)}, u32[]{:S(2)}) async-start(bf16[4,256,256]{2,1,0:T(8,128)(2,1)} %shard_map.154), calls=%async_computation.2 | async-start | bytes 1048576 | tf_op jit(solution)/shard_map/all_to_all | solution.py:313
  198.8 2.3 collective-permute-done.6.w1_ref
  202.4 10.1 %collective-permute-done.8.w3_ref = bf16[1024,256]{1,0:T(8,128)(2,1)} collective-permute-done((bf16[1024,256]{1,0:T(8,128)(2,1)S(1)}, bf16[1024,256]{1,0:T(8,128)(2,1)}, u32[]{:S(2)}, u32[]{:S(2)}) %collective-permute-start.8) | collective-permute-done | bytes 524320 | tf_op jit(solution)/shard_map/ppermute | solution.py:309
  212.5 2.2 shard_map.155
  215.6 21.3 %all-to-all-start.3 = ((bf16[128,8,256]{2,1,0:T(8,128)(2,1)}), bf16[128,8,256]{2,1,0:T(8,128)(2,1)S(1)}, u32[]{:S(2)}, u32[]{:S(2)}) async-start(bf16[128,8,256]{2,1,0:T(8,128)(2,1)} %bitcast.16), calls=%async_computation.3 | async-start | bytes 1048576 | tf_op jit(solution)/shard_map/all_to_all | solution.py:313
  240.4 30.2 %all-to-all-done.3 = bf16[128,8,256]{2,1,0:T(8,128)(2,1)S(1)} async-done(((bf16[128,8,256]{2,1,0:T(8,128)(2,1)}), bf16[128,8,256]{2,1,0:T(8,128)(2,1)S(1)}, u32[]{:S(2)}, u32[]{:S(2)}) %all-to-all-start.3) | async-done | bytes 524320 | tf_op jit(solution)/shard_map/all_to_all | solution.py:313
  271.7 4.3 %shard_map.151 = bf16[512,256]{1,0:T(8,128)(2,1)} custom-call(bf16[16,512,256]{2,1,0:T(8,128)(2,1)} %bitcast.24, bf16[4096,256]{1,0:T(8,128)(2,1)} %w_ref.1), custom_call_target="tpu_custom_call" | custom-call | tf_op jit(solution)/shard_map/pallas_call | solution.py:44
  (39 shorter events, 13.5 us)
Async XLA Ops:
  7.2 81.0 %all-gather.5.cloned.1.call-start = ((), (), s32[]{:S(2)}) async-start(), calls=%async_computation.4 | async-start | bytes 2433024 | tf_op jit(solution)/shard_map/all_gather | solution.py:345
  9.5 262.2 %all-gather.7.cloned.1.call-start = ((), (), s32[]{:S(2)}) async-start(), calls=%async_computation.5 | async-start | bytes 4456448 | tf_op jit(solution)/shard_map/all_gather | solution.py:399
  141.6 31.0 %copy-start = (bf16[1,1024,256]{2,1,0:T(8,128)(2,1)S(1)}, bf16[1,1024,256]{2,1,0:T(8,128)(2,1)}, u32[]{:S(2)}) copy-start(bf16[1,1024,256]{2,1,0:T(8,128)(2,1)} %param.27) | copy-start | bytes 1572868
  141.6 49.1 %all-to-all-start.1 = ((bf16[4,1024,256]{2,1,0:T(8,128)(2,1)}), bf16[4,1024,256]{2,1,0:T(8,128)(2,1)S(1)}, u32[]{:S(2)}, u32[]{:S(2)}) async-start(bf16[4,1024,256]{2,1,0:T(8,128)(2,1)} %broadcast_in_dim.12), calls=%async_computation.1 | async-start | bytes 4194304 | tf_op jit(solution)/shard_map/all_to_all | solution.py:313
  145.7 21.6 %collective-permute-start = (bf16[64,4096]{1,0:T(8,128)(2,1)}, bf16[64,4096]{1,0:T(8,128)(2,1)S(1)}, u32[]{:S(2)}, u32[]{:S(2)}) collective-permute-start(bf16[64,4096]{1,0:T(8,128)(2,1)} %bitcast.11.g0_ref), channel_id=1, source_target_pairs={{4,0},{8,4},{12,8},{0,12},{5,1},{9,5},{13,9},{1,13},{6,2},{10,6},{... | collective-permute-start | bytes 1572872 | tf_op jit(solution)/shard_map/ppermute | solution.py:309
  147.8 21.9 %collective-permute-start.4 = (bf16[64,4096]{1,0:T(8,128)(2,1)}, bf16[64,4096]{1,0:T(8,128)(2,1)S(1)}, u32[]{:S(2)}, u32[]{:S(2)}) collective-permute-start(bf16[64,4096]{1,0:T(8,128)(2,1)} %bitcast.12.u0_ref), channel_id=1, source_target_pairs={{12,0},{0,4},{4,8},{8,12},{13,1},{1,5},{5,9},{9,13},{14,2},{2,6},{... | collective-permute-start | bytes 1572872 | tf_op jit(solution)/shard_map/ppermute | solution.py:309
  151.0 27.7 %collective-permute-start.2 = (bf16[64,4096]{1,0:T(8,128)(2,1)}, bf16[64,4096]{1,0:T(8,128)(2,1)S(1)}, u32[]{:S(2)}, u32[]{:S(2)}) collective-permute-start(bf16[64,4096]{1,0:T(8,128)(2,1)} %bitcast.11.g0_ref), channel_id=1, source_target_pairs={{12,0},{0,4},{4,8},{8,12},{13,1},{1,5},{5,9},{9,13},{14,2},{2,6},{... | collective-permute-start | bytes 1572872 | tf_op jit(solution)/shard_map/ppermute | solution.py:309
  154.1 28.3 %collective-permute-start.3 = (bf16[64,4096]{1,0:T(8,128)(2,1)}, bf16[64,4096]{1,0:T(8,128)(2,1)S(1)}, u32[]{:S(2)}, u32[]{:S(2)}) collective-permute-start(bf16[64,4096]{1,0:T(8,128)(2,1)} %bitcast.12.u0_ref), channel_id=1, source_target_pairs={{4,0},{8,4},{12,8},{0,12},{5,1},{9,5},{13,9},{1,13},{6,2},{10,6},{... | collective-permute-start | bytes 1572872 | tf_op jit(solution)/shard_map/ppermute | solution.py:309
  167.3 22.6 %copy-start.2 = (bf16[64,4096]{1,0:T(8,128)(2,1)}, bf16[64,4096]{1,0:T(8,128)(2,1)S(1)}, u32[]{:S(2)}) copy-start(bf16[64,4096]{1,0:T(8,128)(2,1)S(1)} %collective-permute-done.g1_ref) | copy-start | bytes 1572868
  167.3 22.6 %collective-permute-start.1 = (bf16[64,4096]{1,0:T(8,128)(2,1)S(1)}, bf16[64,4096]{1,0:T(8,128)(2,1)S(1)}, u32[]{:S(2)}, u32[]{:S(2)}) collective-permute-start(bf16[64,4096]{1,0:T(8,128)(2,1)S(1)} %collective-permute-done.g1_ref), channel_id=1, source_target_pairs={{4,0},{8,4},{12,8},{0,12},{5,1},{9,5},{13,9},{1,13},{6,2},{10,6},{... | collective-permute-start | bytes 1572872 | tf_op jit(solution)/shard_map/ppermute | solution.py:309
  169.7 20.1 %copy-start.3 = (bf16[64,4096]{1,0:T(8,128)(2,1)}, bf16[64,4096]{1,0:T(8,128)(2,1)S(1)}, u32[]{:S(2)}) copy-start(bf16[64,4096]{1,0:T(8,128)(2,1)S(1)} %collective-permute-done.4.u3_ref) | copy-start | bytes 1572868
  169.7 21.0 %collective-permute-start.5 = (bf16[64,4096]{1,0:T(8,128)(2,1)S(1)}, bf16[64,4096]{1,0:T(8,128)(2,1)}, u32[]{:S(2)}, u32[]{:S(2)}) collective-permute-start(bf16[64,4096]{1,0:T(8,128)(2,1)S(1)} %collective-permute-done.4.u3_ref), channel_id=1, source_target_pairs={{12,0},{0,4},{4,8},{8,12},{13,1},{1,5},{5,9},{9,13},{14,2},{2,6},{... | collective-permute-start | bytes 1572872 | tf_op jit(solution)/shard_map/ppermute | solution.py:309
  172.6 28.5 %collective-permute-start.6 = (bf16[1024,256]{1,0:T(8,128)(2,1)S(1)}, bf16[1024,256]{1,0:T(8,128)(2,1)S(1)}, u32[]{:S(2)}, u32[]{:S(2)}) collective-permute-start(bf16[1024,256]{1,0:T(8,128)(2,1)S(1)} %bitcast.29), channel_id=1, source_target_pairs={{4,0},{8,4},{12,8},{0,12},{5,1},{9,5},{13,9},{1,13},{6,2},{10,6},{... | collective-permute-start | bytes 1572872 | tf_op jit(solution)/shard_map/ppermute | solution.py:309
  178.7 11.2 %copy-start.4 = (bf16[64,4096]{1,0:T(8,128)(2,1)}, bf16[64,4096]{1,0:T(8,128)(2,1)S(1)}, u32[]{:S(2)}) copy-start(bf16[64,4096]{1,0:T(8,128)(2,1)S(1)} %collective-permute-done.2.g3_ref) | copy-start | bytes 1572868
  178.7 23.7 %collective-permute-start.7 = (bf16[1024,256]{1,0:T(8,128)(2,1)S(1)}, bf16[1024,256]{1,0:T(8,128)(2,1)}, u32[]{:S(2)}, u32[]{:S(2)}) collective-permute-start(bf16[1024,256]{1,0:T(8,128)(2,1)S(1)} %bitcast.30), channel_id=1, source_target_pairs={{8,0},{12,4},{0,8},{4,12},{9,1},{13,5},{1,9},{5,13},{10,2},{14,6},... | collective-permute-start | bytes 1572872 | tf_op jit(solution)/shard_map/ppermute | solution.py:309
  182.4 7.4 %copy-start.5 = (bf16[64,4096]{1,0:T(8,128)(2,1)}, bf16[64,4096]{1,0:T(8,128)(2,1)S(1)}, u32[]{:S(2)}) copy-start(bf16[64,4096]{1,0:T(8,128)(2,1)S(1)} %collective-permute-done.3.u1_ref) | copy-start | bytes 1572868
  182.4 30.0 %collective-permute-start.8 = (bf16[1024,256]{1,0:T(8,128)(2,1)S(1)}, bf16[1024,256]{1,0:T(8,128)(2,1)}, u32[]{:S(2)}, u32[]{:S(2)}) collective-permute-start(bf16[1024,256]{1,0:T(8,128)(2,1)S(1)} %bitcast.31), channel_id=1, source_target_pairs={{12,0},{0,4},{4,8},{8,12},{13,1},{1,5},{5,9},{9,13},{14,2},{2,6},{... | collective-permute-start | bytes 1572872 | tf_op jit(solution)/shard_map/ppermute | solution.py:309
  189.9 0.8 copy-start.6
  194.9 17.6 %all-to-all-start.2 = ((bf16[4,256,256]{2,1,0:T(8,128)(2,1)}), bf16[4,256,256]{2,1,0:T(8,128)(2,1)S(1)}, u32[]{:S(2)}, u32[]{:S(2)}) async-start(bf16[4,256,256]{2,1,0:T(8,128)(2,1)} %shard_map.154), calls=%async_computation.2 | async-start | bytes 1048576 | tf_op jit(solution)/shard_map/all_to_all | solution.py:313
  198.8 38.1 %copy-start.7 = (s32[256,2]{0,1:T(2,128)S(1)}, s32[256,2]{0,1:T(2,128)}, u32[]{:S(2)}) copy-start(s32[256,2]{0,1:T(2,128)} %param.23) | copy-start | bytes 6148
  198.8 38.9 %copy-start.8 = (f32[256,2]{0,1:T(2,128)S(1)}, f32[256,2]{0,1:T(2,128)}, u32[]{:S(2)}) copy-start(f32[256,2]{0,1:T(2,128)} %param.24) | copy-start | bytes 6148
  201.1 11.4 %copy-start.1 = (bf16[1024,256]{1,0:T(8,128)(2,1)}, bf16[1024,256]{1,0:T(8,128)(2,1)S(1)}, u32[]{:S(2)}) copy-start(bf16[1024,256]{1,0:T(8,128)(2,1)S(1)} %collective-permute-done.6.w1_ref) | copy-start | bytes 1572868
  215.6 54.9 %all-to-all-start.3 = ((bf16[128,8,256]{2,1,0:T(8,128)(2,1)}), bf16[128,8,256]{2,1,0:T(8,128)(2,1)S(1)}, u32[]{:S(2)}, u32[]{:S(2)}) async-start(bf16[128,8,256]{2,1,0:T(8,128)(2,1)} %bitcast.16), calls=%async_computation.3 | async-start | bytes 1048576 | tf_op jit(solution)/shard_map/all_to_all | solution.py:313
Sparse Core Ops, SparseCore 0:
  10.7 77.4 all-gather.4
  93.0 70.7 all-gather.6

commit v8 on v6

--- a/solution.py
+++ b/solution.py
@@ -83,14 +83,14 @@
     )
     normal = jnp.sum(weighted, axis=0, keepdims=True)
     width = out_ref.shape[1]
-    normal = jnp.concatenate([normal] * (width // dk), axis=1)
-    pack(
-        out_ref,
-        memory,
-        normal,
+    out_ref[0:dk, :] = memory
+    rows = [
+        jnp.concatenate([normal] * (width // dk), axis=1),
         jnp.broadcast_to(total, (1, width)),
         jnp.broadcast_to(top, (1, width)),
-    )
+        jnp.zeros((out_ref.shape[0] - dk - 3, width), F32),
+    ]
+    out_ref[dk:, :] = jnp.concatenate(rows, axis=0)
 
 
 def fold(first, second):
@@ -115,23 +115,8 @@
     return high, middle, low
 
 
-def pack(out_ref, memory, normal, decay, top):
-    dk, width = memory.shape
-    out_ref[0:dk, :] = memory.astype(BF16)
-    rows = []
-    for value in (normal, decay, top):
-        rows += [part.astype(F32) for part in split3(value)]
-    rows.append(jnp.zeros((out_ref.shape[0] - dk - len(rows), width), F32))
-    out_ref[dk:, :] = jnp.concatenate(rows, axis=0).astype(BF16)
-
-
 def unpack(item, dk):
-    item = item.astype(F32)
-    rows = [
-        item[dk + i : dk + i + 1] + item[dk + i + 1 : dk + i + 2] + item[dk + i + 2 : dk + i + 3]
-        for i in (0, 3, 6)
-    ]
-    return (item[0:dk], *rows)
+    return (item[0:dk], item[dk : dk + 1], item[dk + 1 : dk + 2], item[dk + 2 : dk + 3])
 
 
 def first_state(dk, width):
@@ -338,7 +323,7 @@
     at = jnp.stack([lax.axis_index(EP), lax.axis_index("y")]).astype(jnp.int32)
 
     mine = call(
-        summary_kernel, sds((dk + 16, dv), BF16), (key_rows, value_rows, in_gate, forget_gate)
+        summary_kernel, sds((dk + 8, dv), F32), (key_rows, value_rows, in_gate, forget_gate)
     )
     states = lax.all_gather(mine, EP, axis=0)
     table = call(dispatch_kernel, pltpu.VMEM((slots, columns), BF16), (routes.T, expert_input))

time: 283 us -> 286 us (1.011)
  no operation moved by 1% of the time
where the time goes in v8:
time: 286 us; the launch traced here: 285 us
  waiting for transfers between devices  142 us (50%)
  starting transfers between devices  55.9 us (20%)
  blocking collectives  46.2 us (16%)
  Pallas kernels  22 us (8%)
  between operations  14.2 us (5%)
  local copies, waits for them, and re-layouts  4.88 us (2%)
    all_gather x1, waiting for transfers between devices, body(): states = lax.all_gather(mine, EP, axis=0)  80.2 us
    all_to_all x1, blocking collectives, exchange(): return lax.all_to_all(x, axis, split_axis=0, concat_axis=0, tiled=True)  46.2 us
    ppermute x9, waiting for transfers between devices, from_next(): return lax.ppermute(x, axis, [((i + k) % n, i) for i in range(n)])  31.2 us
    all_to_all x3, waiting for transfers between devices, exchange(): return lax.all_to_all(x, axis, split_axis=0, concat_axis=0, tiled=True)  30.2 us
    all_to_all x3, starting transfers between devices, exchange(): return lax.all_to_all(x, axis, split_axis=0, concat_axis=0, tiled=True)  29.3 us
    ppermute x9, starting transfers between devices, from_next(): return lax.ppermute(x, axis, [((i + k) % n, i) for i in range(n)])  26.5 us
    pallas_call x8, Pallas kernels, call(): pl.pallas_call(kernel, out_shape=out, in_specs=in_specs, out_specs=out_sp...  22 us
  transfers between devices with their start and end apart: 14, of which 8 were waited for; matrix products, arithmetic and copies ran while one was open for 2% of the time, Pallas kernels for 4%

profile of v8, /device:TPU:1, one launch (start us, length us, event | category | flops | bytes accessed | tf_op | source)
XLA Modules:
  0.0 285.4 jit_solution(12696646864492454058)
XLA Ops:
  7.2 2.1 shard_map.149
  10.0 80.2 %all-gather.5.cloned.1.call-done = f32[4352,256]{1,0:T(8,128)} async-done(((f32[136,256]{1,0:T(8,128)}), f32[4352,256]{1,0:T(8,128)}) %all-gather.5.cloned.1.call-update) | async-done | bytes 4456464 | tf_op jit(solution)/shard_map/all_gather | solution.py:328
  90.2 4.7 %shard_map.150 = bf16[512,256]{1,0:T(8,128)(2,1)} custom-call(s32[2]{0:T(128)} %pad_add_fusion.at_ref, bf16[512,128]{1,0:T(8,128)(2,1)} %q_ref.1, bf16[512,128]{1,0:T(8,128)(2,1)} %k_ref.3, bf16[512,256]{1,0:T(8,128)(2,1)} %v_ref.3, f32[1,512]{1,0:T(1,128)} %in_ref.3, f32[1,512]{1,0:T(1,128)} %forget_ref.3, bf16[512,256]{1,0:T(8,128)(2,1)} %gate_ref.1, ...), custom_call_target="tpu_custom_call" | custom-call | tf_op jit(solution)/shard_map/pallas_call | solution.py:44
  96.5 46.2 %all_to_all.20 = bf16[128,8,256]{2,1,0:T(8,128)(2,1)S(1)} all-to-all(bf16[128,8,256]{2,1,0:T(8,128)(2,1)S(1)} %bitcast.21), channel_id=1, replica_groups=mesh['z'=16,'c'=2,'y'=4,'x'=4] {'z','c','y'}, dimensions={0} | all-to-all | bytes 1048576 | tf_op jit(solution)/shard_map/all_to_all | solution.py:296
  144.2 4.1 %all-to-all-start.1 = ((bf16[4,1024,256]{2,1,0:T(8,128)(2,1)}), bf16[4,1024,256]{2,1,0:T(8,128)(2,1)S(1)}, u32[]{:S(2)}, u32[]{:S(2)}) async-start(bf16[4,1024,256]{2,1,0:T(8,128)(2,1)} %broadcast_in_dim.12), calls=%async_computation.1 | async-start | bytes 4194304 | tf_op jit(solution)/shard_map/all_to_all | solution.py:296
  150.4 3.2 %collective-permute-start.4 = (bf16[64,4096]{1,0:T(8,128)(2,1)}, bf16[64,4096]{1,0:T(8,128)(2,1)S(1)}, u32[]{:S(2)}, u32[]{:S(2)}) collective-permute-start(bf16[64,4096]{1,0:T(8,128)(2,1)} %bitcast.12.u0_ref), channel_id=1, source_target_pairs={{12,0},{0,4},{4,8},{8,12},{13,1},{1,5},{5,9},{9,13},{14,2},{2,6},{... | collective-permute-start | bytes 1572872 | tf_op jit(solution)/shard_map/ppermute | solution.py:292
  153.6 3.1 %collective-permute-start.2 = (bf16[64,4096]{1,0:T(8,128)(2,1)}, bf16[64,4096]{1,0:T(8,128)(2,1)S(1)}, u32[]{:S(2)}, u32[]{:S(2)}) collective-permute-start(bf16[64,4096]{1,0:T(8,128)(2,1)} %bitcast.11.g0_ref), channel_id=1, source_target_pairs={{12,0},{0,4},{4,8},{8,12},{13,1},{1,5},{5,9},{9,13},{14,2},{2,6},{... | collective-permute-start | bytes 1572872 | tf_op jit(solution)/shard_map/ppermute | solution.py:292
  156.7 3.4 %collective-permute-start.3 = (bf16[64,4096]{1,0:T(8,128)(2,1)}, bf16[64,4096]{1,0:T(8,128)(2,1)S(1)}, u32[]{:S(2)}, u32[]{:S(2)}) collective-permute-start(bf16[64,4096]{1,0:T(8,128)(2,1)} %bitcast.12.u0_ref), channel_id=1, source_target_pairs={{4,0},{8,4},{12,8},{0,12},{5,1},{9,5},{13,9},{1,13},{6,2},{10,6},{... | collective-permute-start | bytes 1572872 | tf_op jit(solution)/shard_map/ppermute | solution.py:292
  160.1 9.7 %collective-permute-done.g1_ref = bf16[64,4096]{1,0:T(8,128)(2,1)S(1)} collective-permute-done((bf16[64,4096]{1,0:T(8,128)(2,1)}, bf16[64,4096]{1,0:T(8,128)(2,1)S(1)}, u32[]{:S(2)}, u32[]{:S(2)}) %collective-permute-start) | collective-permute-done | bytes 524320 | tf_op jit(solution)/shard_map/ppermute | solution.py:292
  169.8 2.4 collective-permute-start.1
  172.3 2.9 %collective-permute-start.5 = (bf16[64,4096]{1,0:T(8,128)(2,1)S(1)}, bf16[64,4096]{1,0:T(8,128)(2,1)}, u32[]{:S(2)}, u32[]{:S(2)}) collective-permute-start(bf16[64,4096]{1,0:T(8,128)(2,1)S(1)} %collective-permute-done.4.u3_ref), channel_id=1, source_target_pairs={{12,0},{0,4},{4,8},{8,12},{13,1},{1,5},{5,9},{9,13},{14,2},{2,6},{... | collective-permute-start | bytes 1572872 | tf_op jit(solution)/shard_map/ppermute | solution.py:292
  175.2 3.6 %collective-permute-start.6 = (bf16[1024,256]{1,0:T(8,128)(2,1)S(1)}, bf16[1024,256]{1,0:T(8,128)(2,1)S(1)}, u32[]{:S(2)}, u32[]{:S(2)}) collective-permute-start(bf16[1024,256]{1,0:T(8,128)(2,1)S(1)} %bitcast.29), channel_id=1, source_target_pairs={{4,0},{8,4},{12,8},{0,12},{5,1},{9,5},{13,9},{1,13},{6,2},{10,6},{... | collective-permute-start | bytes 1572872 | tf_op jit(solution)/shard_map/ppermute | solution.py:292
  178.8 2.4 collective-permute-done.2.g3_ref
  181.2 3.7 %collective-permute-start.7 = (bf16[1024,256]{1,0:T(8,128)(2,1)S(1)}, bf16[1024,256]{1,0:T(8,128)(2,1)}, u32[]{:S(2)}, u32[]{:S(2)}) collective-permute-start(bf16[1024,256]{1,0:T(8,128)(2,1)S(1)} %bitcast.30), channel_id=1, source_target_pairs={{8,0},{12,4},{0,8},{4,12},{9,1},{13,5},{1,9},{5,13},{10,2},{14,6},... | collective-permute-start | bytes 1572872 | tf_op jit(solution)/shard_map/ppermute | solution.py:292
  185.0 2.1 collective-permute-start.8
  187.1 5.3 %collective-permute-done.1.g2_ref = bf16[64,4096]{1,0:T(8,128)(2,1)S(1)} collective-permute-done((bf16[64,4096]{1,0:T(8,128)(2,1)S(1)}, bf16[64,4096]{1,0:T(8,128)(2,1)S(1)}, u32[]{:S(2)}, u32[]{:S(2)}) %collective-permute-start.1) | collective-permute-done | bytes 524320 | tf_op jit(solution)/shard_map/ppermute | solution.py:292
  193.3 4.2 %shard_map.154 = bf16[4,256,256]{2,1,0:T(8,128)(2,1)} custom-call(bf16[16,256,256]{2,1,0:T(8,128)(2,1)S(1)} %bitcast.20, bf16[64,4096]{1,0:T(8,128)(2,1)} %bitcast.11.g0_ref, bf16[64,4096]{1,0:T(8,128)(2,1)} %copy-done.2, bf16[64,4096]{1,0:T(8,128)(2,1)} %copy-done.6, bf16[64,4096]{1,0:T(8,128)(2,1)} %copy-done.4, bf16[64,4096]{1,0:T(8,128)(2,1)} %bitcast.12.u0_ref, ...), custom_call_target="tpu_custom_call" | custom-call | tf_op jit(solution)/shard_map/pallas_call | solution.py:44
  197.5 3.9 %all-to-all-start.2 = ((bf16[4,256,256]{2,1,0:T(8,128)(2,1)}), bf16[4,256,256]{2,1,0:T(8,128)(2,1)S(1)}, u32[]{:S(2)}, u32[]{:S(2)}) async-start(bf16[4,256,256]{2,1,0:T(8,128)(2,1)} %shard_map.154), calls=%async_computation.2 | async-start | bytes 1048576 | tf_op jit(solution)/shard_map/all_to_all | solution.py:296
  201.4 2.3 collective-permute-done.6.w1_ref
  205.0 10.1 %collective-permute-done.8.w3_ref = bf16[1024,256]{1,0:T(8,128)(2,1)} collective-permute-done((bf16[1024,256]{1,0:T(8,128)(2,1)S(1)}, bf16[1024,256]{1,0:T(8,128)(2,1)}, u32[]{:S(2)}, u32[]{:S(2)}) %collective-permute-start.8) | collective-permute-done | bytes 524320 | tf_op jit(solution)/shard_map/ppermute | solution.py:292
  215.1 2.2 shard_map.155
  218.2 21.3 %all-to-all-start.3 = ((bf16[128,8,256]{2,1,0:T(8,128)(2,1)}), bf16[128,8,256]{2,1,0:T(8,128)(2,1)S(1)}, u32[]{:S(2)}, u32[]{:S(2)}) async-start(bf16[128,8,256]{2,1,0:T(8,128)(2,1)} %bitcast.16), calls=%async_computation.3 | async-start | bytes 1048576 | tf_op jit(solution)/shard_map/all_to_all | solution.py:296
  243.0 30.2 %all-to-all-done.3 = bf16[128,8,256]{2,1,0:T(8,128)(2,1)S(1)} async-done(((bf16[128,8,256]{2,1,0:T(8,128)(2,1)}), bf16[128,8,256]{2,1,0:T(8,128)(2,1)S(1)}, u32[]{:S(2)}, u32[]{:S(2)}) %all-to-all-start.3) | async-done | bytes 524320 | tf_op jit(solution)/shard_map/all_to_all | solution.py:296
  274.2 4.3 %shard_map.151 = bf16[512,256]{1,0:T(8,128)(2,1)} custom-call(bf16[16,512,256]{2,1,0:T(8,128)(2,1)} %bitcast.25, bf16[4096,256]{1,0:T(8,128)(2,1)} %w_ref.1), custom_call_target="tpu_custom_call" | custom-call | tf_op jit(solution)/shard_map/pallas_call | solution.py:44
  (39 shorter events, 13.5 us)
Async XLA Ops:
  7.2 83.1 %all-gather.5.cloned.1.call-start = ((), (), s32[]{:S(2)}) async-start(), calls=%async_computation.4 | async-start | bytes 4595712 | tf_op jit(solution)/shard_map/all_gather | solution.py:328
  9.4 264.9 %all-gather.7.cloned.1.call-start = ((), (), s32[]{:S(2)}) async-start(), calls=%async_computation.5 | async-start | bytes 4456448 | tf_op jit(solution)/shard_map/all_gather | solution.py:382
  144.2 31.0 %copy-start = (bf16[1,1024,256]{2,1,0:T(8,128)(2,1)S(1)}, bf16[1,1024,256]{2,1,0:T(8,128)(2,1)}, u32[]{:S(2)}) copy-start(bf16[1,1024,256]{2,1,0:T(8,128)(2,1)} %param.27) | copy-start | bytes 1572868
  144.2 49.1 %all-to-all-start.1 = ((bf16[4,1024,256]{2,1,0:T(8,128)(2,1)}), bf16[4,1024,256]{2,1,0:T(8,128)(2,1)S(1)}, u32[]{:S(2)}, u32[]{:S(2)}) async-start(bf16[4,1024,256]{2,1,0:T(8,128)(2,1)} %broadcast_in_dim.12), calls=%async_computation.1 | async-start | bytes 4194304 | tf_op jit(solution)/shard_map/all_to_all | solution.py:296
  148.3 21.5 %collective-permute-start = (bf16[64,4096]{1,0:T(8,128)(2,1)}, bf16[64,4096]{1,0:T(8,128)(2,1)S(1)}, u32[]{:S(2)}, u32[]{:S(2)}) collective-permute-start(bf16[64,4096]{1,0:T(8,128)(2,1)} %bitcast.11.g0_ref), channel_id=1, source_target_pairs={{4,0},{8,4},{12,8},{0,12},{5,1},{9,5},{13,9},{1,13},{6,2},{10,6},{... | collective-permute-start | bytes 1572872 | tf_op jit(solution)/shard_map/ppermute | solution.py:292
  150.4 21.9 %collective-permute-start.4 = (bf16[64,4096]{1,0:T(8,128)(2,1)}, bf16[64,4096]{1,0:T(8,128)(2,1)S(1)}, u32[]{:S(2)}, u32[]{:S(2)}) collective-permute-start(bf16[64,4096]{1,0:T(8,128)(2,1)} %bitcast.12.u0_ref), channel_id=1, source_target_pairs={{12,0},{0,4},{4,8},{8,12},{13,1},{1,5},{5,9},{9,13},{14,2},{2,6},{... | collective-permute-start | bytes 1572872 | tf_op jit(solution)/shard_map/ppermute | solution.py:292
  153.6 27.7 %collective-permute-start.2 = (bf16[64,4096]{1,0:T(8,128)(2,1)}, bf16[64,4096]{1,0:T(8,128)(2,1)S(1)}, u32[]{:S(2)}, u32[]{:S(2)}) collective-permute-start(bf16[64,4096]{1,0:T(8,128)(2,1)} %bitcast.11.g0_ref), channel_id=1, source_target_pairs={{12,0},{0,4},{4,8},{8,12},{13,1},{1,5},{5,9},{9,13},{14,2},{2,6},{... | collective-permute-start | bytes 1572872 | tf_op jit(solution)/shard_map/ppermute | solution.py:292
  156.7 28.3 %collective-permute-start.3 = (bf16[64,4096]{1,0:T(8,128)(2,1)}, bf16[64,4096]{1,0:T(8,128)(2,1)S(1)}, u32[]{:S(2)}, u32[]{:S(2)}) collective-permute-start(bf16[64,4096]{1,0:T(8,128)(2,1)} %bitcast.12.u0_ref), channel_id=1, source_target_pairs={{4,0},{8,4},{12,8},{0,12},{5,1},{9,5},{13,9},{1,13},{6,2},{10,6},{... | collective-permute-start | bytes 1572872 | tf_op jit(solution)/shard_map/ppermute | solution.py:292
  169.8 22.6 %copy-start.2 = (bf16[64,4096]{1,0:T(8,128)(2,1)}, bf16[64,4096]{1,0:T(8,128)(2,1)S(1)}, u32[]{:S(2)}) copy-start(bf16[64,4096]{1,0:T(8,128)(2,1)S(1)} %collective-permute-done.g1_ref) | copy-start | bytes 1572868
  169.8 22.6 %collective-permute-start.1 = (bf16[64,4096]{1,0:T(8,128)(2,1)S(1)}, bf16[64,4096]{1,0:T(8,128)(2,1)S(1)}, u32[]{:S(2)}, u32[]{:S(2)}) collective-permute-start(bf16[64,4096]{1,0:T(8,128)(2,1)S(1)} %collective-permute-done.g1_ref), channel_id=1, source_target_pairs={{4,0},{8,4},{12,8},{0,12},{5,1},{9,5},{13,9},{1,13},{6,2},{10,6},{... | collective-permute-start | bytes 1572872 | tf_op jit(solution)/shard_map/ppermute | solution.py:292
  172.3 20.1 %copy-start.3 = (bf16[64,4096]{1,0:T(8,128)(2,1)}, bf16[64,4096]{1,0:T(8,128)(2,1)S(1)}, u32[]{:S(2)}) copy-start(bf16[64,4096]{1,0:T(8,128)(2,1)S(1)} %collective-permute-done.4.u3_ref) | copy-start | bytes 1572868
  172.3 21.0 %collective-permute-start.5 = (bf16[64,4096]{1,0:T(8,128)(2,1)S(1)}, bf16[64,4096]{1,0:T(8,128)(2,1)}, u32[]{:S(2)}, u32[]{:S(2)}) collective-permute-start(bf16[64,4096]{1,0:T(8,128)(2,1)S(1)} %collective-permute-done.4.u3_ref), channel_id=1, source_target_pairs={{12,0},{0,4},{4,8},{8,12},{13,1},{1,5},{5,9},{9,13},{14,2},{2,6},{... | collective-permute-start | bytes 1572872 | tf_op jit(solution)/shard_map/ppermute | solution.py:292
  175.2 28.5 %collective-permute-start.6 = (bf16[1024,256]{1,0:T(8,128)(2,1)S(1)}, bf16[1024,256]{1,0:T(8,128)(2,1)S(1)}, u32[]{:S(2)}, u32[]{:S(2)}) collective-permute-start(bf16[1024,256]{1,0:T(8,128)(2,1)S(1)} %bitcast.29), channel_id=1, source_target_pairs={{4,0},{8,4},{12,8},{0,12},{5,1},{9,5},{13,9},{1,13},{6,2},{10,6},{... | collective-permute-start | bytes 1572872 | tf_op jit(solution)/shard_map/ppermute | solution.py:292
  181.2 11.2 %copy-start.4 = (bf16[64,4096]{1,0:T(8,128)(2,1)}, bf16[64,4096]{1,0:T(8,128)(2,1)S(1)}, u32[]{:S(2)}) copy-start(bf16[64,4096]{1,0:T(8,128)(2,1)S(1)} %collective-permute-done.2.g3_ref) | copy-start | bytes 1572868
  181.2 23.7 %collective-permute-start.7 = (bf16[1024,256]{1,0:T(8,128)(2,1)S(1)}, bf16[1024,256]{1,0:T(8,128)(2,1)}, u32[]{:S(2)}, u32[]{:S(2)}) collective-permute-start(bf16[1024,256]{1,0:T(8,128)(2,1)S(1)} %bitcast.30), channel_id=1, source_target_pairs={{8,0},{12,4},{0,8},{4,12},{9,1},{13,5},{1,9},{5,13},{10,2},{14,6},... | collective-permute-start | bytes 1572872 | tf_op jit(solution)/shard_map/ppermute | solution.py:292
  185.0 7.4 %copy-start.5 = (bf16[64,4096]{1,0:T(8,128)(2,1)}, bf16[64,4096]{1,0:T(8,128)(2,1)S(1)}, u32[]{:S(2)}) copy-start(bf16[64,4096]{1,0:T(8,128)(2,1)S(1)} %collective-permute-done.3.u1_ref) | copy-start | bytes 1572868
  185.0 30.0 %collective-permute-start.8 = (bf16[1024,256]{1,0:T(8,128)(2,1)S(1)}, bf16[1024,256]{1,0:T(8,128)(2,1)}, u32[]{:S(2)}, u32[]{:S(2)}) collective-permute-start(bf16[1024,256]{1,0:T(8,128)(2,1)S(1)} %bitcast.31), channel_id=1, source_target_pairs={{12,0},{0,4},{4,8},{8,12},{13,1},{1,5},{5,9},{9,13},{14,2},{2,6},{... | collective-permute-start | bytes 1572872 | tf_op jit(solution)/shard_map/ppermute | solution.py:292
  192.4 0.8 copy-start.6
  197.5 17.6 %all-to-all-start.2 = ((bf16[4,256,256]{2,1,0:T(8,128)(2,1)}), bf16[4,256,256]{2,1,0:T(8,128)(2,1)S(1)}, u32[]{:S(2)}, u32[]{:S(2)}) async-start(bf16[4,256,256]{2,1,0:T(8,128)(2,1)} %shard_map.154), calls=%async_computation.2 | async-start | bytes 1048576 | tf_op jit(solution)/shard_map/all_to_all | solution.py:296
  201.3 38.1 %copy-start.7 = (s32[256,2]{0,1:T(2,128)S(1)}, s32[256,2]{0,1:T(2,128)}, u32[]{:S(2)}) copy-start(s32[256,2]{0,1:T(2,128)} %param.23) | copy-start | bytes 6148
  201.4 38.9 %copy-start.8 = (f32[256,2]{0,1:T(2,128)S(1)}, f32[256,2]{0,1:T(2,128)}, u32[]{:S(2)}) copy-start(f32[256,2]{0,1:T(2,128)} %param.24) | copy-start | bytes 6148
  203.7 11.4 %copy-start.1 = (bf16[1024,256]{1,0:T(8,128)(2,1)}, bf16[1024,256]{1,0:T(8,128)(2,1)S(1)}, u32[]{:S(2)}) copy-start(bf16[1024,256]{1,0:T(8,128)(2,1)S(1)} %collective-permute-done.6.w1_ref) | copy-start | bytes 1572868
  218.2 54.9 %all-to-all-start.3 = ((bf16[128,8,256]{2,1,0:T(8,128)(2,1)}), bf16[128,8,256]{2,1,0:T(8,128)(2,1)S(1)}, u32[]{:S(2)}, u32[]{:S(2)}) async-start(bf16[128,8,256]{2,1,0:T(8,128)(2,1)} %bitcast.16), calls=%async_computation.3 | async-start | bytes 1048576 | tf_op jit(solution)/shard_map/all_to_all | solution.py:296
Sparse Core Ops, SparseCore 0:
  10.7 79.5 all-gather.4
  95.0 71.2 all-gather.6
